TPU v7x, 128 devices: a whole 4x4x4 slice. The times are simulated.
128 devices in a mesh: sp: 32 (over z, y, core), tp: 4 (over x).
Axes of the slice: x: 4, y: 4, z: 4, core: 2. Of those that a mesh axis runs over, the one named last changes fastest.
Arguments:
- input_activations: bfloat16 [32768, 2048], P(('sp', 'tp')), may hold values from -6 to 6
- norm_gain: float32 [2048], replicated, may hold values from 0.5 to 1.5
- w_gate: bfloat16 [2048, 2048], P('sp', 'tp'), may hold values from -0.125 to 0.125
- w_value: bfloat16 [2048, 2048], P('sp', 'tp'), may hold values from -0.125 to 0.125
- w_state_in: bfloat16 [2048, 1024], P('sp', 'tp'), may hold values from -0.125 to 0.125
- w_state_out: bfloat16 [2048, 1024], P('sp', 'tp'), may hold values from -0.125 to 0.125
- w_step_forward: bfloat16 [2048, 32], P('sp', 'tp'), may hold values from -0.03125 to 0.03125
- w_step_backward: bfloat16 [2048, 32], P('sp', 'tp'), may hold values from -0.03125 to 0.03125
- step_offset: float32 [2, 32], P(None, 'tp'), may hold values from -0.5 to 0.5
- fading_speed: float32 [2, 32], P(None, 'tp'), may hold values from 0.3 to 1
- conv_value: float32 [3, 2048], P(None, 'tp'), may hold values from -3.5 to 3.5
- conv_state_in: float32 [3, 1024], P(None, 'tp'), may hold values from -3.5 to 3.5
- conv_state_out: float32 [3, 1024], P(None, 'tp'), may hold values from -3.5 to 3.5
- out_gain: float32 [2048], P('tp'), may hold values from 0.5 to 1.5
- w_out: bfloat16 [2048, 2048], P('tp', 'sp'), may hold values from -0.125 to 0.125
Outputs:
- mixer_out: bfloat16 [32768, 2048], P(('sp', 'tp'))
All inputs are finite; a program needn't handle non-finite values.
Results may differ from a plain program's by a relative error of at most 0.015.
Values may be sent and summed in bfloat16 or wider, within the bound.
A program may use at most 128 MiB of HBM per device.

v0:
```python
import functools
import math

import jax
import jax.numpy as jnp
from jax import lax
from jax.experimental import pallas as pl
from jax.experimental.pallas import tpu as pltpu
from jax.sharding import Mesh
from jax.sharding import PartitionSpec as P

HEAD_DIM = 64
STATE = 128
BLOCK = 128
SP = ("z", "y", "c")
SP_TP = ("z", "y", "c", "x")
EPSILON = 1e-06
MESH = pl.DeviceIdType.MESH
HALO = 16


def place():
    return [lax.axis_index(name) for name in ("z", "y", "c", "x")]


def step(at, by):
    return lax.rem(at + by + 4, 4)


def stretch_at(z, y, c, by):
    n = lax.rem(z * 8 + y * 2 + c + by + 32, 32)
    return {"z": n // 8, "y": lax.rem(n // 2, 4), "c": lax.rem(n, 2)}


class Wire:
    def __init__(self, send, recv):
        self.send, self.recv, self.count, self.sent = send, recv, 0, []

    def describe(self, ref, to):
        k = self.count
        self.count += 1
        return pltpu.make_async_remote_copy(
            src_ref=ref,
            dst_ref=ref,
            send_sem=self.send.at[k],
            recv_sem=self.recv.at[k],
            device_id=to,
            device_id_type=MESH,
        )

    def go(self, ref, to):
        copy = self.describe(ref, to)
        copy.start()
        self.sent.append(copy)
        return copy

    def drain(self):
        for copy in self.sent:
            copy.wait_send()


class Ring:
    def __init__(self, wire, axis, at, block, low, high):
        self.wire, self.at = wire, at
        self.up, self.down = {axis: step(at, 1)}, {axis: step(at, 3)}
        self.block, self.low, self.high = block, low, high

    def start(self):
        self.a = self.wire.go(self.block(self.at), self.up)
        self.b = self.wire.go(self.block(self.at), self.down)

    def forward(self):
        self.a.wait_recv()
        self.c = self.wire.go(self.low(step(self.at, 3)), self.up)
        self.b.wait_recv()
        self.d = self.wire.go(self.high(step(self.at, 1)), self.down)

    def finish(self):
        self.c.wait_recv()
        self.d.wait_recv()


def greet(others):
    barrier = pltpu.get_barrier_semaphore()
    for other in others:
        pl.semaphore_signal(barrier, inc=1, device_id=other, device_id_type=MESH)
    pl.semaphore_wait(barrier, len(others))


def ring_peers(z, y, c, x):
    return [
        {"x": step(x, 1)},
        {"x": step(x, 3)},
        {"y": step(y, 1)},
        {"y": step(y, 3)},
        {"z": step(z, 1)},
        {"z": step(z, 3)},
        {"c": 1 - c},
    ]


def project_kernel(
    tokens_ref,
    gain_ref,
    a_ref,
    g_ref,
    o_ref,
    mixed_ref,
    gate_ref,
    steps_ref,
    wo_ref,
    tokens,
    edges,
    normed,
    wa,
    wg,
    wo,
    send,
    recv,
    halo_send,
    halo_recv,
    local_sem,
):
    z, y, c, x = place()
    wire = Wire(send, recv)
    rows = tokens_ref.shape[0]
    half = rows // 2
    own = [
        pltpu.make_async_copy(tokens_ref, tokens.at[x], local_sem.at[0]),
        pltpu.make_async_copy(a_ref, wa.at[z, y, c], local_sem.at[1]),
        pltpu.make_async_copy(g_ref, wg.at[z, y, c], local_sem.at[2]),
        pltpu.make_async_copy(o_ref, wo.at[z, y, c, x], local_sem.at[3]),
    ]
    for copy in own:
        copy.start()
    ahead = [dict(stretch_at(z, y, c, 1), x=k) for k in range(4)]
    behind = [dict(stretch_at(z, y, c, 31), x=k) for k in range(4)]
    greet(ring_peers(z, y, c, x) + ahead + behind)
    for copy in own:
        copy.wait()

    halos = [
        [
            pltpu.make_async_remote_copy(
                src_ref=tokens.at[x, pl.ds(offset, HALO)],
                dst_ref=edges.at[slot],
                send_sem=halo_send.at[4 * slot + k],
                recv_sem=halo_recv.at[slot],
                device_id=to,
                device_id_type=MESH,
            )
            for k, to in enumerate(group)
        ]
        for slot, (group, offset) in enumerate(((ahead, rows - HALO), (behind, 0)))
    ]

    @pl.when(x == 3)
    def _():
        for copy in halos[0]:
            copy.start()

    @pl.when(x == 0)
    def _():
        for copy in halos[1]:
            copy.start()

    wo_x = Ring(
        wire,
        "x",
        x,
        lambda at: wo.at[z, y, c, at],
        lambda at: wo.at[z, y, c, at, pl.ds(0, 32)],
        lambda at: wo.at[z, y, c, at, pl.ds(32, 32)],
    )
    wo_x.start()
    low, high = pl.ds(0, half), pl.ds(half, half)
    up, down = {"x": step(x, 1)}, {"x": step(x, 3)}
    up_low = wire.go(tokens.at[x, low], up)
    down_high = wire.go(tokens.at[x, high], down)
    up_high = wire.go(tokens.at[x, high], up)
    down_low = wire.go(tokens.at[x, low], down)

    a_first = Ring(
        wire,
        "y",
        y,
        lambda at: wa.at[z, at, c],
        lambda at: wa.at[z, at, c, pl.ds(0, 32)],
        lambda at: wa.at[z, at, c, pl.ds(32, 32)],
    )
    g_first = Ring(
        wire,
        "z",
        z,
        lambda at: wg.at[at, y, c],
        lambda at: wg.at[at, y, c, pl.ds(0, 32)],
        lambda at: wg.at[at, y, c, pl.ds(32, 32)],
    )
    a_first.start()
    g_first.start()

    def normalize(ref, count, to):
        @pl.loop(0, count // 16)
        def _(k):
            start = pl.multiple_of(k * 16, 16)
            wide = ref[pl.ds(start, 16), :].astype(jnp.float32)
            scale = lax.rsqrt(jnp.mean(wide * wide, axis=-1, keepdims=True) + EPSILON)
            normed[pl.ds(pl.multiple_of(to + start, 16), 16), :] = (
                wide * scale * gain_ref[...]
            ).astype(jnp.bfloat16)

    def main_row(shard):
        return HALO + shard * rows

    normalize(tokens.at[x], rows, main_row(x))

    a_first.forward()
    g_first.forward()
    wo_x.forward()
    a_first.finish()
    a_second = Ring(
        wire,
        "z",
        z,
        lambda at: wa.at[at, :, c],
        lambda at: wa.at[at, pl.ds(0, 2), c],
        lambda at: wa.at[at, pl.ds(2, 2), c],
    )
    a_second.start()
    partner = {"c": 1 - c}
    a_pair = [wire.go(wa.at[z, :, c], partner)]
    g_first.finish()
    g_second = Ring(
        wire,
        "y",
        y,
        lambda at: wg.at[:, at, c],
        lambda at: wg.at[pl.ds(0, 2), at, c],
        lambda at: wg.at[pl.ds(2, 2), at, c],
    )
    g_second.start()
    g_pair = [wire.go(wg.at[:, y, c], partner)]
    wo_x.finish()
    lo_first = Ring(
        wire,
        "y",
        y,
        lambda at: wo.at[z, at, c, pl.ds(0, 2)],
        lambda at: wo.at[z, at, c, 0],
        lambda at: wo.at[z, at, c, 1],
    )
    hi_first = Ring(
        wire,
        "z",
        z,
        lambda at: wo.at[at, y, c, pl.ds(2, 2)],
        lambda at: wo.at[at, y, c, 2],
        lambda at: wo.at[at, y, c, 3],
    )
    lo_first.start()
    hi_first.start()

    for slot in range(2):
        halos[slot][0].wait_recv()
    normalize(edges.at[0], HALO, 0)
    normalize(edges.at[1], HALO, main_row(4))

    up_low.wait_recv()
    far_low = wire.go(tokens.at[step(x, 3), low], up)
    down_high.wait_recv()
    far_high = wire.go(tokens.at[step(x, 1), high], down)
    normalize(tokens.at[step(x, 3), low], half, main_row(step(x, 3)))
    normalize(tokens.at[step(x, 1), high], half, main_row(step(x, 1)) + half)

    a_second.forward()
    a_pair.append(wire.go(wa.at[step(z, 3), :, c], partner))
    a_pair.append(wire.go(wa.at[step(z, 1), :, c], partner))
    g_second.forward()
    g_pair.append(wire.go(wg.at[:, step(y, 3), c], partner))
    g_pair.append(wire.go(wg.at[:, step(y, 1), c], partner))
    lo_first.forward()
    hi_first.forward()
    lo_first.finish()
    lo_second = Ring(
        wire,
        "z",
        z,
        lambda at: wo.at[at, :, c, pl.ds(0, 2)],
        lambda at: wo.at[at, pl.ds(0, 2), c, pl.ds(0, 2)],
        lambda at: wo.at[at, pl.ds(2, 2), c, pl.ds(0, 2)],
    )
    lo_second.start()
    hi_first.finish()
    hi_second = Ring(
        wire,
        "y",
        y,
        lambda at: wo.at[:, at, c, pl.ds(2, 2)],
        lambda at: wo.at[pl.ds(0, 2), at, c, pl.ds(2, 2)],
        lambda at: wo.at[pl.ds(2, 2), at, c, pl.ds(2, 2)],
    )
    hi_second.start()
    wo_pair = [
        wire.go(wo.at[z, :, c, pl.ds(0, 2)], partner),
        wire.go(wo.at[:, y, c, pl.ds(2, 2)], partner),
    ]

    up_high.wait_recv()
    down_low.wait_recv()
    normalize(tokens.at[step(x, 3), high], half, main_row(step(x, 3)) + half)
    normalize(tokens.at[step(x, 1), low], half, main_row(step(x, 1)))

    a_second.finish()
    a_pair.append(wire.go(wa.at[step(z, 2), :, c], partner))
    g_second.finish()
    g_pair.append(wire.go(wg.at[:, step(y, 2), c], partner))
    for copy in a_pair + g_pair:
        copy.wait_recv()

    lead = wa.shape[4] - 128

    def project(start, count):
        taken = pl.ds(start, count)

        @pl.loop(0, lead // 256)
        def _(k):
            columns = pl.ds(pl.multiple_of(k * 256, 256), 256)
            weight = wa[:, :, :, :, columns].reshape(-1, 256)
            mixed_ref[taken, columns] = jnp.dot(
                normed[taken, :], weight, preferred_element_type=jnp.float32
            ).astype(jnp.bfloat16)

    def project_rest(shard):
        taken = pl.ds(main_row(shard), rows)
        kept = pl.ds(pl.multiple_of(shard * rows, rows), rows)

        @pl.loop(0, wg.shape[4] // 256)
        def _(k):
            columns = pl.ds(pl.multiple_of(k * 256, 256), 256)
            weight = wg[:, :, :, :, columns].reshape(-1, 256)
            gate_ref[kept, columns] = jnp.dot(
                normed[taken, :], weight, preferred_element_type=jnp.float32
            ).astype(jnp.bfloat16)

        weight = wa[:, :, :, :, lead:].reshape(-1, 128)
        steps_ref[kept, :] = jnp.dot(
            normed[taken, :], weight, preferred_element_type=jnp.float32
        ).astype(jnp.bfloat16)

    def whole(shard):
        project(pl.multiple_of(main_row(shard), 16), rows)
        project_rest(shard)

    @pl.loop(0, 3)
    def _(k):
        whole(lax.rem(x + 3 + k, 4))

    project(0, HALO)
    project(main_row(4), HALO)

    lo_second.forward()
    hi_second.forward()
    for by in (3, 1):
        wo_pair.append(wire.go(wo.at[step(z, by), :, c, pl.ds(0, 2)], partner))
        wo_pair.append(wire.go(wo.at[:, step(y, by), c, pl.ds(2, 2)], partner))

    far_low.wait_recv()
    far_high.wait_recv()
    normalize(tokens.at[step(x, 2)], rows, main_row(step(x, 2)))
    whole(step(x, 2))

    lo_second.finish()
    hi_second.finish()
    wo_pair.append(wire.go(wo.at[step(z, 2), :, c, pl.ds(0, 2)], partner))
    wo_pair.append(wire.go(wo.at[:, step(y, 2), c, pl.ds(2, 2)], partner))
    for copy in wo_pair:
        copy.wait_recv()
    out = pltpu.make_async_copy(wo, wo_ref, local_sem.at[0])
    out.start()
    wire.drain()

    @pl.when(x == 3)
    def _():
        for copy in halos[0]:
            copy.wait_send()

    @pl.when(x == 0)
    def _():
        for copy in halos[1]:
            copy.wait_send()

    out.wait()


COPIES = 80


def gather_and_project(tokens, gain, a, g, o):
    rows, width = tokens.shape
    return pl.pallas_call(
        project_kernel,
        out_shape=(
            jax.ShapeDtypeStruct((4 * rows + 2 * HALO, a.shape[1] - 128), jnp.bfloat16),
            jax.ShapeDtypeStruct((4 * rows, g.shape[1]), jnp.bfloat16),
            jax.ShapeDtypeStruct((4 * rows, 128), jnp.bfloat16),
            jax.ShapeDtypeStruct((4, 4, 2, 4, *o.shape), jnp.bfloat16),
        ),
        in_specs=[
            pl.BlockSpec(memory_space=pl.ANY),
            pl.BlockSpec(memory_space=pltpu.VMEM),
            pl.BlockSpec(memory_space=pl.ANY),
            pl.BlockSpec(memory_space=pl.ANY),
            pl.BlockSpec(memory_space=pl.ANY),
        ],
        out_specs=(
            pl.BlockSpec(memory_space=pltpu.VMEM),
            pl.BlockSpec(memory_space=pltpu.VMEM),
            pl.BlockSpec(memory_space=pltpu.VMEM),
            pl.BlockSpec(memory_space=pl.ANY),
        ),
        scratch_shapes=[
            pltpu.VMEM((4, rows, width), jnp.bfloat16),
            pltpu.VMEM((2, HALO, width), jnp.bfloat16),
            pltpu.VMEM((4 * rows + 2 * HALO, width), jnp.bfloat16),
            pltpu.VMEM((4, 4, 2, *a.shape), jnp.bfloat16),
            pltpu.VMEM((4, 4, 2, *g.shape), jnp.bfloat16),
            pltpu.VMEM((4, 4, 2, 4, *o.shape), jnp.bfloat16),
            pltpu.SemaphoreType.DMA((COPIES,)),
            pltpu.SemaphoreType.DMA((COPIES,)),
            pltpu.SemaphoreType.DMA((8,)),
            pltpu.SemaphoreType.DMA((2,)),
            pltpu.SemaphoreType.DMA((4,)),
        ],
        compiler_params=pltpu.CompilerParams(
            collective_id=0, has_side_effects=True, vmem_limit_bytes=60 * 2**20
        ),
        name="gather_project",
    )(tokens, gain.reshape(1, -1), a, g, o)


def prefix(shard, axis, combine, identity, reverse):
    length, place = lax.axis_size(axis), lax.axis_index(axis)
    everything = jax.tree.map(lambda part: lax.all_gather(part, axis), shard)
    start = jax.tree.map(
        lambda part, zero: jnp.broadcast_to(jnp.asarray(zero, part.dtype), part.shape),
        shard,
        identity,
    )

    def hop(k, before):
        at = length - 1 - k if reverse else k
        reached = at > place if reverse else at < place
        new = combine(before, jax.tree.map(lambda part: part[at], everything))
        return jax.tree.map(lambda a, b: jnp.where(reached, a, b), new, before)

    return lax.fori_loop(0, length, hop, start)


def nothing_yet(shard, identity):
    return jax.tree.map(
        lambda a, e: jnp.broadcast_to(jnp.asarray(e, a.dtype), a.shape), shard, identity
    )


def carried_in(shard, axes, combine, identity, reverse):
    before = start = nothing_yet(shard, identity)
    subtotal = shard
    for axis in reversed(axes):
        length, place = lax.axis_size(axis), lax.axis_index(axis)
        pieces = jax.tree.map(lambda part: lax.all_gather(part, axis), subtotal)
        inside, subtotal = start, start
        for k in reversed(range(length)) if reverse else range(length):
            passed = k > place if reverse else k < place
            subtotal = combine(subtotal, jax.tree.map(lambda part: part[k], pieces))
            inside = jax.tree.map(lambda new, old: jnp.where(passed, new, old), subtotal, inside)
        before = combine(inside, before)
    return before


def rms_rows(values):
    wide = values.astype(jnp.float32)
    return wide * lax.rsqrt(jnp.mean(wide * wide, axis=-1, keepdims=True) + EPSILON)


def short_filter(padded, taps):
    wide = padded.astype(jnp.float32)
    mixed = taps[0] * wide[:-2] + taps[1] * wide[1:-1] + taps[2] * wide[2:]
    return jax.nn.silu(mixed).astype(jnp.bfloat16)


def one_way(signal, step_size, rate, inward, outward, intersect):
    sequence_extent, groups, ratio, width = signal.shape
    states = inward.shape[2]
    count = sequence_extent // BLOCK
    blocks = signal.reshape(count, BLOCK, groups, ratio, width).astype(jnp.float32)
    step_blocks = step_size.reshape(count, BLOCK, groups, ratio)
    within = jnp.cumsum(-step_blocks * rate, axis=1)
    final = within[:, -1]
    scaling_factor = jnp.exp(final[:, None] - within) * step_blocks
    inward_blocks = inward.reshape(count, BLOCK, groups, states).astype(jnp.float32)
    outward_blocks = outward.reshape(count, BLOCK, groups, states).astype(jnp.float32)
    block_states = jnp.einsum(
        "cqgn,cqgrp->cgrpn",
        inward_blocks,
        blocks * scaling_factor[..., None],
        precision=lax.Precision.HIGHEST,
    )

    def advance(state, inputs):
        return (state * inputs[1][..., None, None] + inputs[0], state)

    start_state = jnp.zeros((groups, ratio, width, states), jnp.float32)
    last_state, before = lax.scan(advance, start_state, (block_states, jnp.exp(final)))
    lower = (jnp.arange(BLOCK)[:, None] >= jnp.arange(BLOCK)[None, :])[None, :, :, None, None]
    gaps = within[:, :, None] - within[:, None]
    decay = jnp.where(lower, jnp.exp(jnp.where(lower, gaps, 0.0)), 0.0)
    weights_mix = intersect[..., None] * decay * step_blocks[:, None]
    diagonal = jnp.einsum("cqkgr,ckgrp->cqgrp", weights_mix, blocks, precision=lax.Precision.HIGHEST)
    carried = (
        jnp.einsum("cqgn,cgrpn->cqgrp", outward_blocks, before, precision=lax.Precision.HIGHEST)
        * jnp.exp(within)[..., None]
    )
    running = jnp.cumsum(final, axis=0)
    from_start = (within + (running - final)[:, None]).reshape(sequence_extent, groups, ratio)
    outputs = (diagonal + carried).reshape(sequence_extent, groups, ratio, width)
    return (
        outputs,
        from_start,
        jnp.exp(running[-1]),
        last_state,
        outward_blocks.reshape(sequence_extent, groups, states),
    )


def read_in(outward_wide, incoming, from_start):
    return (
        jnp.einsum("lgn,grpn->lgrp", outward_wide, incoming, precision=lax.Precision.HIGHEST)
        * jnp.exp(from_start)[..., None]
    )


def link(earlier, later):
    return (earlier[0] * later[0], earlier[1] * later[0][..., None, None] + later[1])


def combine_ways(ahead, behind, ahead_state, behind_state):
    forward = ahead[0] + read_in(ahead[4], ahead_state, ahead[1])
    backward = behind[0] + read_in(behind[4], behind_state, behind[1])
    return forward + backward[::-1]


def local(
    input_activations,
    norm_gain,
    w_gate,
    w_value,
    w_state_in,
    w_state_out,
    w_step_forward,
    w_step_backward,
    step_offset,
    fading_speed,
    conv_value,
    conv_state_in,
    conv_state_out,
    out_gain,
    w_out,
):
    heads_local = w_step_forward.shape[1]
    a = jnp.concatenate(
        [
            w_value,
            w_state_in,
            w_state_out,
            w_step_forward,
            w_step_backward,
            jnp.zeros((w_value.shape[0], 128 - 2 * heads_local), jnp.bfloat16),
        ],
        axis=1,
    )
    mixed_in, gate, raw, wo = gather_and_project(input_activations, norm_gain, a, w_gate, w_out.T)
    sequence_extent = gate.shape[0]
    stretch = lax.axis_index(SP)
    row = lax.broadcasted_iota(jnp.int32, (sequence_extent + 2, 1), 0)
    outside = ((row == 0) & (stretch == 0)) | (
        (row == sequence_extent + 1) & (stretch == lax.axis_size(SP) - 1)
    )
    padded = jnp.where(outside, 0, mixed_in[HALO - 1 : 1 - HALO])
    raw_forward, raw_backward = raw[:, :heads_local], raw[:, heads_local : 2 * heads_local]
    taps = jnp.concatenate([conv_value, conv_state_in, conv_state_out], axis=1)
    filtered = short_filter(padded, taps)
    content_breadth = w_value.shape[1]
    state_width = w_state_in.shape[1]
    groups_local = state_width // STATE
    ratio = heads_local // groups_local
    signal = filtered[:, :content_breadth].reshape(sequence_extent, groups_local, ratio, HEAD_DIM)
    inward = filtered[:, content_breadth : content_breadth + state_width].reshape(
        sequence_extent, groups_local, STATE
    )
    outward = filtered[:, content_breadth + state_width :].reshape(
        sequence_extent, groups_local, STATE
    )
    shift = math.log(sequence_extent * lax.axis_size(SP))
    forward_step = jax.nn.softplus(
        raw_forward.astype(jnp.float32) + step_offset[0] - shift
    ).reshape(sequence_extent, groups_local, ratio)
    backward_step = jax.nn.softplus(
        raw_backward.astype(jnp.float32) + step_offset[1] - shift
    ).reshape(sequence_extent, groups_local, ratio)
    rates = fading_speed.reshape(2, groups_local, ratio)
    count = sequence_extent // BLOCK
    intersect = jnp.einsum(
        "cqgn,ckgn->cqkg",
        outward.reshape(count, BLOCK, groups_local, STATE),
        inward.reshape(count, BLOCK, groups_local, STATE),
        preferred_element_type=jnp.float32,
    )
    flipped = intersect[::-1, ::-1, ::-1]
    ahead = one_way(signal, forward_step, rates[0], inward, outward, intersect)
    behind = one_way(
        signal[::-1], backward_step[::-1], rates[1], inward[::-1], outward[::-1], flipped
    )
    ahead_in = carried_in(
        (ahead[2], ahead[3]),
        SP,
        link,
        (jnp.ones_like(ahead[2]), jnp.zeros_like(ahead[3])),
        False,
    )
    behind_in = carried_in(
        (behind[2], behind[3]),
        SP,
        link,
        (jnp.ones_like(behind[2]), jnp.zeros_like(behind[3])),
        True,
    )
    combined = combine_ways(ahead, behind, ahead_in[1], behind_in[1])
    gated = combined.reshape(sequence_extent, content_breadth) * jax.nn.silu(
        gate.astype(jnp.float32)
    )
    grouped = rms_rows(
        gated.reshape(sequence_extent, groups_local, content_breadth // groups_local)
    ).reshape(sequence_extent, content_breadth)
    mixed = (grouped * out_gain).astype(jnp.bfloat16)
    everything = lax.all_to_all(
        mixed.reshape(4, sequence_extent // 4, content_breadth), "x", split_axis=0, concat_axis=0
    )
    whole = wo.reshape(-1, 4, HEAD_DIM, content_breadth)
    result = jnp.einsum("xtk,sxnk->tsn", everything, whole, preferred_element_type=jnp.float32)
    return result.reshape(sequence_extent // 4, -1).astype(jnp.bfloat16)


def solution(mesh):
    torus = Mesh(mesh.devices.reshape(4, 4, 2, 4), SP_TP)
    return jax.shard_map(
        local,
        mesh=torus,
        in_specs=(
            P(SP_TP, None),
            P(),
            P(SP, "x"),
            P(SP, "x"),
            P(SP, "x"),
            P(SP, "x"),
            P(SP, "x"),
            P(SP, "x"),
            P(None, "x"),
            P(None, "x"),
            P(None, "x"),
            P(None, "x"),
            P(None, "x"),
            P("x"),
            P("x", SP),
        ),
        out_specs=P(SP_TP, None),
        check_vma=False,
    )
```

profile of v0, /device:TPU:1, one launch (start us, length us, event | category | flops | bytes accessed | tf_op | source)
XLA Modules:
  0.0 367.8 jit_solution(18094292623840958930)
XLA Ops:
  9.7 1.6 concatenate.7.a_ref
  11.3 80.6 %gather_project.1 = (bf16[1056,1024]{1,0:T(8,128)(2,1)}, bf16[1024,512]{1,0:T(8,128)(2,1)}, bf16[1024,128]{1,0:T(8,128)(2,1)}, bf16[4,4,2,4,64,512]{5,4,3,2,1,0:T(8,128)(2,1)}) custom-call(bf16[256,2048]{1,0:T(8,128)(2,1)} %tokens_ref.1, f32[1,2048]{1,0:T(1,128)} %bitcast.427, bf16[64,1152]{1,0:T(8,128)(2,1)} %concatenate.7.a_ref, bf16[64,512]{1,0:T(8,128)(2,1)} %g_ref.1, ...), custom_call_target="tpu_custom_call" | custom-call | tf_op jit(solution)/shard_map/gather_project/pallas_call | solution.py:400
  91.9 2.5 compare_select_fusion.1
  96.4 47.4 %fusion.204 = f32[8,128,2,4]{3,0,1,2:T(8,128)S(1)} fusion(f32[8,128,2,4]{3,0,1,2:T(8,128)S(1)} %copy.254), kind=kOutput, calls=%fused_computation.300 | output fusion | flops 1040384 | bytes 65536 | tf_op jit(solution)/shard_map/jit(cumsum)/reduce_window_sum | solution.py:497
  144.2 2.3 select_convert_fusion
  146.5 2.0 multiply_convert_fusion
  148.6 1.1 slice.252
  149.6 1.5 slice_bitcast_fusion.24
  151.2 2.5 all_gather.59
  153.7 6.6 %all_gather.60 = f32[4,2,4]{2,1,0:T(2,128)S(1)} all-gather(f32[1,2,4]{2,1,0:T(2,128)S(1)} %get-tuple-element.222), channel_id=1, replica_groups=mesh['z'=4,'y'=4,'c'=2,'x'=4] {'y'}, dimensions={0}, use_global_device_ids=true | all-gather | bytes 160 | tf_op jit(solution)/shard_map/all_gather | solution.py:470
  160.3 1.7 add_exponential_fusion
  162.4 1.5 copy.224
  164.7 6.3 %rev.21 = bf16[1024,2,128]{2,0,1:T(8,128)(2,1)S(1)} reverse(bf16[1024,2,128]{2,0,1:T(8,128)(2,1)} %bitcast.411), dimensions={0} | reverse | bytes 1048576 | tf_op jit(solution)/shard_map/rev | solution.py:621
  171.0 3.4 rev.18
  174.5 1.5 copy.311
  176.2 2.6 fusion.26
  178.7 1.6 broadcast.188.clone
  180.3 14.4 %while.27 = (s32[]{:T(128)}, f32[2,4,64,128]{3,2,1,0:T(8,128)S(1)}, f32[8,2,4,64,128]{4,3,2,1,0:T(8,128)}, f32[8,2,4]{2,1,0:T(2,128)S(1)}, f32[8,2,4,64,128]{4,3,2,1,0:T(8,128)}, /*index=5*/s32[]{:T(128)}, s32[]{:T(128)}) while((s32[]{:T(128)}, f32[2,4,64,128]{3,2,1,0:T(8,128)S(1)}, f32[8,2,4,64,128]{4,3,2,1,0:T(8,128)}, ...), condition=%wide.region_6.7_spmd.clone, body=%wide.region_5.6_spmd.clone.sunk | while | flops 262147 | bytes 1310924 | solution.py:513
  182.9 1.0 bitcast_add_fusion.25
  186.5 1.0 bitcast_add_fusion.25
  191.9 1.0 bitcast_add_fusion.25
  194.7 4.2 %all-gather.1 = f32[4,4,64,128]{3,2,1,0:T(8,128)S(1)} all-gather(f32[2,4,64,128]{3,2,1,0:T(8,128)S(1)} %get-tuple-element.70), channel_id=3, replica_groups=mesh['z'=4,'y'=4,'c'=2,'x'=4] {'c'}, dimensions={0}, use_global_device_ids=true | all-gather | bytes 786432 | tf_op jit(solution)/shard_map/all_gather | solution.py:470
  200.2 1.2 copy.228
  201.4 1.4 copy.236
  202.9 1.3 copy.229
  204.2 1.4 fusion.202
  206.0 3.0 add_exponential_fusion.1
  209.0 1.6 copy.237
  210.6 2.0 reshape_reshape.15
  214.2 2.7 fusion.28
  216.9 1.6 broadcast.188.clone.1
  218.5 14.4 %while.26 = (s32[]{:T(128)}, f32[2,4,64,128]{3,2,1,0:T(8,128)S(1)}, f32[8,2,4,64,128]{4,3,2,1,0:T(8,128)}, f32[8,2,4]{2,1,0:T(2,128)S(1)}, f32[8,2,4,64,128]{4,3,2,1,0:T(8,128)}, /*index=5*/s32[]{:T(128)}, s32[]{:T(128)}) while((s32[]{:T(128)}, f32[2,4,64,128]{3,2,1,0:T(8,128)S(1)}, f32[8,2,4,64,128]{4,3,2,1,0:T(8,128)}, ...), condition=%wide.region_2.3_spmd.clone, body=%wide.region_1.2_spmd.clone.sunk | while | flops 262147 | bytes 1310924 | solution.py:513
  232.9 1.8 all_gather.52
  234.8 5.4 %all_gather.53 = f32[4,2,4]{2,1,0:T(2,128)S(1)} all-gather(f32[1,2,4]{2,1,0:T(2,128)S(1)} %get-tuple-element.219), channel_id=1, replica_groups=mesh['z'=4,'y'=4,'c'=2,'x'=4] {'y'}, dimensions={0}, use_global_device_ids=true | all-gather | bytes 160 | tf_op jit(solution)/shard_map/all_gather | solution.py:470
  240.1 4.1 %all-gather = f32[4,4,64,128]{3,2,1,0:T(8,128)S(1)} all-gather(f32[2,4,64,128]{3,2,1,0:T(8,128)S(1)} %get-tuple-element.68), channel_id=2, replica_groups=mesh['z'=4,'y'=4,'c'=2,'x'=4] {'c'}, dimensions={0}, use_global_device_ids=true | all-gather | bytes 786432 | tf_op jit(solution)/shard_map/all_gather | solution.py:470
  246.0 2.1 multiply_add_fusion
  248.1 6.6 %all_gather.61 = f32[4,2,4]{2,1,0:T(2,128)S(1)} all-gather(f32[1,2,4]{2,1,0:T(2,128)S(1)} %get-tuple-element.213), channel_id=1, replica_groups=mesh['z'=4,'y'=4,'c'=2,'x'=4] {'z'}, dimensions={0}, use_global_device_ids=true | all-gather | bytes 160 | tf_op jit(solution)/shard_map/all_gather | solution.py:470
  254.7 5.8 %all_gather.54 = f32[4,2,4]{2,1,0:T(2,128)S(1)} all-gather(f32[1,2,4]{2,1,0:T(2,128)S(1)} %get-tuple-element.204), channel_id=1, replica_groups=mesh['z'=4,'y'=4,'c'=2,'x'=4] {'z'}, dimensions={0}, use_global_device_ids=true | all-gather | bytes 160 | tf_op jit(solution)/shard_map/all_gather | solution.py:470
  262.9 5.9 %rev.19 = f32[8,128,128,2]{1,2,3,0:T(8,128)} reverse(f32[8,128,128,2]{1,2,3,0:T(8,128)S(1)} %convolution_bitcast_fusion.1), dimensions={0,1,2} | reverse | bytes 2097152 | tf_op jit(solution)/shard_map/rev | solution.py:618
  268.8 1.3 copy.227
  270.1 1.6 copy.250
  271.8 1.5 copy.242
  274.2 1.2 copy.349
  276.0 1.3 copy.252
  277.3 7.0 %fusion.2 = f32[8,2,4,64,128]{4,3,2,1,0:T(8,128)} fusion(f32[8,128,2,4]{1,3,2,0:T(4,128)S(1)} %copy_bitcast_fusion.2, f32[8,128,2,4]{1,3,2,0:T(4,128)S(1)} %copy.255, f32[8,128,128,2]{2,1,3,0:T(8,128)} %copy.252, pred[128,128]{1,0:T(8,128)(4,1)S(1)} %iota_compare_fusion, bf16[1024,2,4,64]{0,3,2,1:T(8,128)(2,1)S(1)} %copy-done.11), kind=kOutput, calls=%fused_computation.11 | convolution fusion | flops 810549248 | bytes 4276224 | tf_op jit(solution)/shard_map/cqkgr,ckgrp->cqgrp/dot_general | solution.py:518
  284.3 2.0 multiply_add_fusion.1
  286.4 3.6 fusion.23
  290.0 4.6 %fusion.9 = f32[8,2,4,64,128]{4,3,2,1,0:T(8,128)S(1)} fusion(f32[8,128,2,4]{1,3,2,0:T(4,128)S(1)} %bitcast.416, f32[8,128,2,4]{1,3,2,0:T(4,128)S(1)} %copy.230, f32[8,128,128,2]{2,1,3,0:T(8,128)S(1)} %copy-done.18, pred[128,128]{1,0:T(8,128)(4,1)S(1)} %iota_compare_fusion, bf16[8,128,2,4,64]{1,0,4,3,2:T(8,128)(2,1)S(1)} %bitcast.405), kind=kOutput, calls=%fused_computation.18 | convolution fusion | flops 810549248 | bytes 4276224 | tf_op jit(solution)/shard_map/cqkgr,ckgrp->cqgrp/dot_general | solution.py:518
  294.7 2.6 fusion.25
  297.3 4.3 %bitcast_add_fusion.2 = f32[1024,2,4,64]{0,3,2,1:T(8,128)} fusion(f32[8,2,4,8,8,128]{5,4,3,2,1,0:T(8,128)S(1)} %fusion.23, f32[1024,2,4]{0,2,1:T(4,128)S(1)} %exp.99, bf16[1024,2,128]{2,0,1:T(8,128)(2,1)S(1)} %rev.22, f32[4,2,4,64,128]{4,3,2,1,0:T(8,128)} %all-gather.13.cloned.1.call-done, f32[4,2,4,64,128]{4,3,2,1,0:T(8,128)} %all-gather.11.cloned.1.call-done, ...), kind=kOutput, calls=%fused_computation.35 | convolution fusion | flops 808386560 | bytes 7373194 | tf_op jit(solution)/shard_map/lgn,grpn->lgrp/dot_general | solution.py:537
  301.6 6.2 %rev.23 = f32[1024,2,4,64]{0,3,2,1:T(8,128)} reverse(f32[1024,2,4,64]{0,3,2,1:T(8,128)} %bitcast_add_fusion.2), dimensions={0} | reverse | bytes 4194304 | tf_op jit(solution)/shard_map/rev | solution.py:549
  307.8 10.3 %all-gather.9.cloned.1.call-done = f32[4,2,4,64,128]{4,3,2,1,0:T(8,128)} async-done(((f32[1,2,4,64,128]{4,3,2,1,0:T(8,128)}), f32[4,2,4,64,128]{4,3,2,1,0:T(8,128)}) %all-gather.9.cloned.1.call-update) | async-done | bytes 1048592 | tf_op jit(solution)/shard_map/all_gather | solution.py:470
  318.1 5.0 %fusion.21 = f32[1024,2,4,64]{0,3,2,1:T(8,128)} fusion(f32[1024,2,4,64]{0,3,2,1:T(8,128)} %rev.23, f32[8,2,4,8,8,128]{5,4,3,2,1,0:T(8,128)S(1)} %copy-done.1, f32[1024,2,4]{0,2,1:T(4,128)S(1)} %exp.91, bf16[1024,2,128,1]{2,1,0,3:T(2,128)(2,1)S(1)} %bitcast.409, f32[4,2,4,64,128]{4,3,2,1,0:T(8,128)} %all-gather.9.cloned.1.call-done, ...), kind=kOutput, calls=%fused_computation.37 | convolution fusion | flops 808910848 | bytes 9470346 | tf_op jit(solution)/shard_map/lgn,grpn->lgrp/dot_general | solution.py:537
  323.1 2.0 copy.277
  325.1 1.9 fusion.198
  327.1 3.5 mul.705
  330.6 3.6 reduce_sum.9
  334.2 1.1 add_rsqrt_fusion
  335.3 1.2 mul.706
  337.2 1.8 multiply_convert_fusion.1
  339.0 4.0 %all-to-all-start = ((bf16[4,256,512]{2,1,0:T(8,128)(2,1)}), bf16[4,256,512]{2,1,0:T(8,128)(2,1)S(1)}, u32[]{:S(2)}, u32[]{:S(2)}) async-start(bf16[4,256,512]{2,1,0:T(8,128)(2,1)} %bitcast.408), calls=%async_computation | async-start | bytes 2097152 | tf_op jit(solution)/shard_map/all_to_all | solution.py:645
  343.0 7.7 %copy.280 = bf16[32,64,512,4]{2,1,0,3:T(8,128)(2,1)} copy(bf16[32,64,512,4]{2,1,3,0:T(8,128)(2,1)} %bitcast.397) | data formatting | bytes 16777216 | tf_op jit(solution)/shard_map/xtk,sxnk->tsn/dot_general | solution.py:649
  350.7 3.8 %all-to-all-done = bf16[4,256,512]{2,1,0:T(8,128)(2,1)S(1)} async-done(((bf16[4,256,512]{2,1,0:T(8,128)(2,1)}), bf16[4,256,512]{2,1,0:T(8,128)(2,1)S(1)}, u32[]{:S(2)}, u32[]{:S(2)}) %all-to-all-start) | async-done | bytes 1048608 | tf_op jit(solution)/shard_map/all_to_all | solution.py:645
  354.6 6.7 %fusion.16 = bf16[256,2048]{1,0:T(8,128)(2,1)} fusion(bf16[4,256,512]{2,1,0:T(8,128)(2,1)S(1)} %all-to-all-done, bf16[2048,512,4]{1,0,2:T(8,128)(2,1)} %bitcast.398), kind=kOutput, calls=%fused_computation.29 | convolution fusion | flops 2148007936 | bytes 10485760 | tf_op jit(solution)/shard_map/xtk,sxnk->tsn/dot_general | solution.py:649
  (171 shorter events, 41.8 us)
Async XLA Ops:
  6.5 239.4 %all-gather.11.cloned.1.call-start = ((), (), s32[]{:S(2)}) async-start(), calls=%async_computation.3 | async-start | bytes 1310720 | tf_op jit(solution)/shard_map/all_gather | solution.py:470
  95.4 48.7 %copy-start.19 = (f32[3,512]{1,0:T(4,128)S(1)}, f32[3,512]{1,0:T(4,128)}, u32[]{:S(2)}) copy-start(f32[3,512]{1,0:T(4,128)} %param.29) | copy-start | bytes 18436
  95.4 48.7 %copy-start.20 = (f32[3,256]{1,0:T(4,128)S(1)}, f32[3,256]{1,0:T(4,128)}, u32[]{:S(2)}) copy-start(f32[3,256]{1,0:T(4,128)} %param.30) | copy-start | bytes 9220
  95.4 48.7 %copy-start.21 = (f32[3,256]{1,0:T(4,128)S(1)}, f32[3,256]{1,0:T(4,128)}, u32[]{:S(2)}) copy-start(f32[3,256]{1,0:T(4,128)} %param.31) | copy-start | bytes 9220
  162.0 1.9 copy-start.17
  198.9 4.0 %copy-start.13 = (f32[4,4,64,128]{3,2,1,0:T(8,128)}, f32[4,4,64,128]{3,2,1,0:T(8,128)S(1)}, u32[]{:S(2)}) copy-start(f32[4,4,64,128]{3,2,1,0:T(8,128)S(1)} %all-gather.1) | copy-start | bytes 1572868
  199.9 84.5 %all-gather.7.cloned.1.call-start = ((), (), s32[]{:S(2)}) async-start(), calls=%async_computation.1 | async-start | bytes 1310720 | tf_op jit(solution)/shard_map/all_gather | solution.py:470
  212.8 1.0 copy-start.8
  212.8 1.4 copy-start.2
  244.3 0.8 copy-start.14
  245.9 15.5 %copy-start.3 = (bf16[1024,256]{1,0:T(8,128)(2,1)S(1)}, bf16[1024,256]{1,0:T(8,128)(2,1)}, u32[]{:S(2)}) copy-start(bf16[1024,256]{1,0:T(8,128)(2,1)} %get-tuple-element.187) | copy-start | bytes 1572868
  245.9 51.4 %all-gather.13.cloned.1.call-start = ((), (), s32[]{:S(2)}) async-start(), calls=%async_computation.4 | async-start | bytes 1310720 | tf_op jit(solution)/shard_map/all_gather | solution.py:470
  248.1 70.0 %all-gather.9.cloned.1.call-start = ((), (), s32[]{:S(2)}) async-start(), calls=%async_computation.2 | async-start | bytes 1310720 | tf_op jit(solution)/shard_map/all_gather | solution.py:470
  261.5 7.3 %copy-start.4 = (bf16[8,128,2,128]{3,2,1,0:T(2,128)(2,1)}, bf16[8,128,2,128]{3,2,1,0:T(2,128)(2,1)S(1)}, u32[]{:S(2)}) copy-start(bf16[8,128,2,128]{3,2,1,0:T(2,128)(2,1)S(1)} %reshape_reshape.16) | copy-start | bytes 1572868
  268.8 4.6 %copy-start.7 = (f32[8,128,2,4]{3,0,1,2:T(8,128)S(1)}, f32[8,128,2,4]{3,0,1,2:T(8,128)}, u32[]{:S(2)}) copy-start(f32[8,128,2,4]{3,0,1,2:T(8,128)} %get-tuple-element.192) | copy-start | bytes 98308
  270.1 3.6 copy-start.6
  273.7 2.2 copy-start.12
  274.2 3.2 copy-start.11
  286.4 3.6 copy-start.9
  286.4 3.6 copy-start.18
  290.0 4.7 %copy-start = (f32[8,2,4,64,128]{4,3,2,1,0:T(8,128)S(1)}, f32[8,2,4,64,128]{4,3,2,1,0:T(8,128)}, u32[]{:S(2)}) copy-start(f32[8,2,4,64,128]{4,3,2,1,0:T(8,128)} %get-tuple-element.67) | copy-start | bytes 6291460
  290.0 4.7 %copy-start.5 = (bf16[8,128,2,128]{3,2,1,0:T(2,128)(2,1)S(1)}, bf16[8,128,2,128]{3,2,1,0:T(2,128)(2,1)}, u32[]{:S(2)}) copy-start(bf16[8,128,2,128]{3,2,1,0:T(2,128)(2,1)} %copy-done.4) | copy-start | bytes 1572868
  301.6 16.6 %copy-start.1 = (f32[8,2,4,8,8,128]{5,4,3,2,1,0:T(8,128)S(1)}, f32[8,2,4,8,8,128]{5,4,3,2,1,0:T(8,128)}, u32[]{:S(2)}) copy-start(f32[8,2,4,8,8,128]{5,4,3,2,1,0:T(8,128)} %fusion.25) | copy-start | bytes 6291460
  301.6 16.6 %copy-start.15 = (f32[4,4,64,128]{3,2,1,0:T(8,128)S(1)}, f32[4,4,64,128]{3,2,1,0:T(8,128)}, u32[]{:S(2)}) copy-start(f32[4,4,64,128]{3,2,1,0:T(8,128)} %copy-done.14) | copy-start | bytes 1572868
  301.6 16.6 %copy-start.16 = (bf16[1024,2,128]{2,1,0:T(2,128)(2,1)S(1)}, bf16[1024,2,128]{2,1,0:T(2,128)(2,1)}, u32[]{:S(2)}) copy-start(bf16[1024,2,128]{2,1,0:T(2,128)(2,1)} %reshape.288) | copy-start | bytes 1572868
  323.1 2.0 copy-start.10
  336.5 0.7 copy-start.22
  339.0 15.6 %all-to-all-start = ((bf16[4,256,512]{2,1,0:T(8,128)(2,1)}), bf16[4,256,512]{2,1,0:T(8,128)(2,1)S(1)}, u32[]{:S(2)}, u32[]{:S(2)}) async-start(bf16[4,256,512]{2,1,0:T(8,128)(2,1)} %bitcast.408), calls=%async_computation | async-start | bytes 2097152 | tf_op jit(solution)/shard_map/all_to_all | solution.py:645
Sparse Core Ops, SparseCore 0:
  200.0 18.7 all-gather.10
  246.0 19.5 all-gather.6
  267.3 24.6 all-gather.12
  293.5 24.5 all-gather.8
where the time goes:
time: 373 us; the launch traced here: 368 us
  other arithmetic  104 us (28%)
  Pallas kernels  80.6 us (22%)
  local copies, waits for them, and re-layouts  74.6 us (20%)
  matrix products  39.4 us (11%)
  blocking collectives  37 us (10%)
  waiting for transfers between devices  14.2 us (4%)
  between operations  13.7 us (4%)
  starting transfers between devices  4.28 us (1%)
    pallas_call x1, Pallas kernels, gather_and_project(): pl.pallas_call(project_kernel, out_shape=(jax.ShapeDtypeStruct((4 * rows...  80.6 us
    another operation x2, other arithmetic, one_way(): within = jnp.cumsum(-step_blocks * rate, axis=1)  48.8 us
    all_gather x8, blocking collectives, carried_in(): pieces = jax.tree.map(lambda part: lax.all_gather(part, axis), subtotal)  37 us
    add x16, other arithmetic, advance(): return (state * inputs[1][..., None, None] + inputs[0], state)  16.6 us
    dynamic_update_slice x16, other arithmetic, one_way(): lax.scan(advance, start_state, (block_states, jnp.exp(final)))  11.7 us
    dot_general x2, matrix products, one_way(): jnp.einsum('cqkgr,ckgrp->cqgrp', weights_mix, blocks, precision=lax.Preci...  11.6 us
    all_gather x4, waiting for transfers between devices, carried_in(): pieces = jax.tree.map(lambda part: lax.all_gather(part, axis), subtotal)  10.3 us
    dot_general x2, matrix products, read_in(): jnp.einsum('lgn,grpn->lgrp', outward_wide, incoming, precision=lax.Precis...  9.26 us
  transfers between devices with their start and end apart: 5, of which 2 were waited for; matrix products, arithmetic and copies ran while one was open for 24% of the time, Pallas kernels for 0%

commit v1 on v0

--- a/solution.py
+++ b/solution.py
@@ -355,8 +355,21 @@
     def _(k):
         whole(lax.rem(x + 3 + k, 4))
 
-    project(0, HALO)
-    project(main_row(4), HALO)
+    @pl.when(z * 8 + y * 2 + c > 0)
+    def _():
+        project(0, HALO)
+
+    @pl.when(z * 8 + y * 2 + c == 0)
+    def _():
+        mixed_ref[0:HALO, :] = jnp.zeros((HALO, lead), jnp.bfloat16)
+
+    @pl.when(z * 8 + y * 2 + c < 31)
+    def _():
+        project(main_row(4), HALO)
+
+    @pl.when(z * 8 + y * 2 + c == 31)
+    def _():
+        mixed_ref[main_row(4) :, :] = jnp.zeros((HALO, lead), jnp.bfloat16)
 
     lo_second.forward()
     hi_second.forward()
@@ -438,115 +451,375 @@
     )(tokens, gain.reshape(1, -1), a, g, o)
 
 
-def prefix(shard, axis, combine, identity, reverse):
-    length, place = lax.axis_size(axis), lax.axis_index(axis)
-    everything = jax.tree.map(lambda part: lax.all_gather(part, axis), shard)
-    start = jax.tree.map(
-        lambda part, zero: jnp.broadcast_to(jnp.asarray(zero, part.dtype), part.shape),
-        shard,
-        identity,
-    )
-
-    def hop(k, before):
-        at = length - 1 - k if reverse else k
-        reached = at > place if reverse else at < place
-        new = combine(before, jax.tree.map(lambda part: part[at], everything))
-        return jax.tree.map(lambda a, b: jnp.where(reached, a, b), new, before)
-
-    return lax.fori_loop(0, length, hop, start)
-
-
-def nothing_yet(shard, identity):
-    return jax.tree.map(
-        lambda a, e: jnp.broadcast_to(jnp.asarray(e, a.dtype), a.shape), shard, identity
-    )
-
-
-def carried_in(shard, axes, combine, identity, reverse):
-    before = start = nothing_yet(shard, identity)
-    subtotal = shard
-    for axis in reversed(axes):
-        length, place = lax.axis_size(axis), lax.axis_index(axis)
-        pieces = jax.tree.map(lambda part: lax.all_gather(part, axis), subtotal)
-        inside, subtotal = start, start
-        for k in reversed(range(length)) if reverse else range(length):
-            passed = k > place if reverse else k < place
-            subtotal = combine(subtotal, jax.tree.map(lambda part: part[k], pieces))
-            inside = jax.tree.map(lambda new, old: jnp.where(passed, new, old), subtotal, inside)
-        before = combine(inside, before)
-    return before
-
-
-def rms_rows(values):
-    wide = values.astype(jnp.float32)
-    return wide * lax.rsqrt(jnp.mean(wide * wide, axis=-1, keepdims=True) + EPSILON)
-
-
-def short_filter(padded, taps):
-    wide = padded.astype(jnp.float32)
-    mixed = taps[0] * wide[:-2] + taps[1] * wide[1:-1] + taps[2] * wide[2:]
-    return jax.nn.silu(mixed).astype(jnp.bfloat16)
-
-
-def one_way(signal, step_size, rate, inward, outward, intersect):
-    sequence_extent, groups, ratio, width = signal.shape
-    states = inward.shape[2]
-    count = sequence_extent // BLOCK
-    blocks = signal.reshape(count, BLOCK, groups, ratio, width).astype(jnp.float32)
-    step_blocks = step_size.reshape(count, BLOCK, groups, ratio)
-    within = jnp.cumsum(-step_blocks * rate, axis=1)
-    final = within[:, -1]
-    scaling_factor = jnp.exp(final[:, None] - within) * step_blocks
-    inward_blocks = inward.reshape(count, BLOCK, groups, states).astype(jnp.float32)
-    outward_blocks = outward.reshape(count, BLOCK, groups, states).astype(jnp.float32)
-    block_states = jnp.einsum(
-        "cqgn,cqgrp->cgrpn",
-        inward_blocks,
-        blocks * scaling_factor[..., None],
-        precision=lax.Precision.HIGHEST,
-    )
-
-    def advance(state, inputs):
-        return (state * inputs[1][..., None, None] + inputs[0], state)
-
-    start_state = jnp.zeros((groups, ratio, width, states), jnp.float32)
-    last_state, before = lax.scan(advance, start_state, (block_states, jnp.exp(final)))
-    lower = (jnp.arange(BLOCK)[:, None] >= jnp.arange(BLOCK)[None, :])[None, :, :, None, None]
-    gaps = within[:, :, None] - within[:, None]
-    decay = jnp.where(lower, jnp.exp(jnp.where(lower, gaps, 0.0)), 0.0)
-    weights_mix = intersect[..., None] * decay * step_blocks[:, None]
-    diagonal = jnp.einsum("cqkgr,ckgrp->cqgrp", weights_mix, blocks, precision=lax.Precision.HIGHEST)
-    carried = (
-        jnp.einsum("cqgn,cgrpn->cqgrp", outward_blocks, before, precision=lax.Precision.HIGHEST)
-        * jnp.exp(within)[..., None]
-    )
-    running = jnp.cumsum(final, axis=0)
-    from_start = (within + (running - final)[:, None]).reshape(sequence_extent, groups, ratio)
-    outputs = (diagonal + carried).reshape(sequence_extent, groups, ratio, width)
-    return (
-        outputs,
-        from_start,
-        jnp.exp(running[-1]),
-        last_state,
-        outward_blocks.reshape(sequence_extent, groups, states),
-    )
-
-
-def read_in(outward_wide, incoming, from_start):
-    return (
-        jnp.einsum("lgn,grpn->lgrp", outward_wide, incoming, precision=lax.Precision.HIGHEST)
-        * jnp.exp(from_start)[..., None]
-    )
-
-
-def link(earlier, later):
-    return (earlier[0] * later[0], earlier[1] * later[0][..., None, None] + later[1])
-
-
-def combine_ways(ahead, behind, ahead_state, behind_state):
-    forward = ahead[0] + read_in(ahead[4], ahead_state, ahead[1])
-    backward = behind[0] + read_in(behind[4], behind_state, behind[1])
-    return forward + backward[::-1]
+LOG2E = 1.4426950408889634
+
+
+def dot_nt(a, b):
+    return lax.dot_general(a, b, (((1,), (1,)), ((), ())), preferred_element_type=jnp.float32)
+
+
+def dot_tn(a, b):
+    return lax.dot_general(a, b, (((0,), (0,)), ((), ())), preferred_element_type=jnp.float32)
+
+
+def dot(a, b, precision=None):
+    return lax.dot_general(
+        a, b, (((1,), (0,)), ((), ())), precision=precision, preferred_element_type=jnp.float32
+    )
+
+
+def iota(shape, dim):
+    return lax.broadcasted_iota(jnp.int32, shape, dim)
+
+
+def silu(v):
+    return v / (1.0 + jnp.exp(-v))
+
+
+def mixer_kernel(
+    shift,
+    mixed_ref,
+    gate_ref,
+    raw_ref,
+    taps_ref,
+    heads_ref,
+    gain_ref,
+    wo_hbm,
+    out_ref,
+    signal,
+    inward,
+    outward,
+    column,
+    rowwise,
+    reading,
+    states,
+    decays,
+    before,
+    inner,
+    totals,
+    arrived,
+    onward,
+    incoming,
+    mixed,
+    shards,
+    wo,
+    send,
+    recv,
+    local_sem,
+):
+    z, y, c, x = place()
+    me = z * 8 + y * 2 + c
+    blocks = gate_ref.shape[0] // BLOCK
+    half = signal.shape[1]
+    wide = 2 * half
+    groups = inward.shape[1] // STATE
+    ratio = half // HEAD_DIM // groups
+    heads = groups * ratio
+    span = ratio * HEAD_DIM
+
+    def stretch(n):
+        return {"z": n // 8, "y": lax.rem(n // 2, 4), "c": lax.rem(n, 2)}
+
+    barrier = pltpu.get_barrier_semaphore()
+
+    @pl.loop(1, 32)
+    def _(k):
+        pl.semaphore_signal(
+            barrier, inc=1, device_id=stretch(lax.rem(me + k, 32)), device_id_type=MESH
+        )
+
+    for k in range(1, 4):
+        pl.semaphore_signal(barrier, inc=1, device_id={"x": step(x, k)}, device_id_type=MESH)
+    load_wo = pltpu.make_async_copy(wo_hbm, wo, local_sem)
+    load_wo.start()
+
+    row, col = iota((BLOCK, BLOCK), 0), iota((BLOCK, BLOCK), 1)
+    lower = row >= col
+    triangle = jnp.where(lower, 1.0, 0.0)
+    spread = jnp.where(
+        iota((128, wide), 1) // HEAD_DIM == iota((128, wide), 0), 1.0, 0.0
+    ).astype(jnp.bfloat16)
+    forward_lane = iota((BLOCK, 128), 1) < heads
+
+    def rows_of(k):
+        return pl.ds(pl.multiple_of(k * BLOCK, BLOCK), BLOCK)
+
+    @pl.loop(0, blocks)
+    def _(k):
+        window = pl.ds(pl.multiple_of(k * BLOCK, BLOCK), BLOCK + 2 * HALO)
+        for at in range(0, mixed_ref.shape[1], 128):
+            cells = mixed_ref[window, at : at + 128].astype(jnp.float32)
+            tap = taps_ref[:, at : at + 128]
+            total = (
+                tap[0:1] * pltpu.roll(cells, 1, 0)
+                + tap[1:2] * cells
+                + tap[2:3] * pltpu.roll(cells, BLOCK + 2 * HALO - 1, 0)
+            )[HALO : HALO + BLOCK]
+            done = silu(total).astype(jnp.bfloat16)
+            if at < half:
+                signal[rows_of(k), at : at + 128] = done
+            elif at < half + inward.shape[1]:
+                inward[rows_of(k), at - half : at - half + 128] = done
+            else:
+                begin = at - half - inward.shape[1]
+                outward[rows_of(k), begin : begin + 128] = done
+
+        size = jax.nn.softplus(
+            raw_ref[rows_of(k), :].astype(jnp.float32) + heads_ref[0:1, :] - shift
+        )
+        logs = size * heads_ref[1:2, :]
+        through = dot(triangle, logs, lax.Precision.HIGHEST)
+        until = through - logs
+        whole = through[BLOCK - 1 : BLOCK, :]
+        logsize = jnp.log(size)
+        column[rows_of(k), :] = jnp.where(forward_lane, through, -until) * LOG2E
+        across = jnp.where(forward_lane, logsize - through, logsize + until) * LOG2E
+        turned = across.T
+        sizes = size.T
+        rowwise[k, 0 : 2 * heads, :] = turned[0 : 2 * heads]
+        rowwise[k, 2 * heads : 3 * heads, :] = sizes[0:heads] + sizes[heads : 2 * heads]
+        reading[rows_of(k), :] = jnp.exp(
+            jnp.where(forward_lane, through, whole - until)
+        ).astype(jnp.bfloat16)
+        weight = size * jnp.exp(jnp.where(forward_lane, whole - through, until))
+        decays[k] = dot(
+            jnp.broadcast_to(jnp.exp(whole), (8, 128)),
+            spread.astype(jnp.float32),
+            lax.Precision.HIGHEST,
+        )
+        weights = dot(weight.astype(jnp.bfloat16), spread)
+        for way in range(2):
+            for g in range(groups):
+                lanes = slice(g * span, (g + 1) * span)
+                placed = slice(way * half + g * span, way * half + (g + 1) * span)
+                content = (
+                    signal[rows_of(k), lanes].astype(jnp.float32) * weights[:, placed]
+                ).astype(jnp.bfloat16)
+                states[k, :, placed] = dot_tn(
+                    inward[rows_of(k), g * STATE : (g + 1) * STATE], content
+                )
+
+    @pl.loop(0, wide // 128)
+    def _(j):
+        lanes = pl.ds(pl.multiple_of(j * 128, 128), 128)
+        backward = j >= half // 128
+        total = jnp.zeros((STATE, 128), jnp.float32)
+        decay = jnp.ones((1, 128), jnp.float32)
+        for k in range(blocks):
+            at = jnp.where(backward, blocks - 1 - k, k)
+            part = decays[at, 0:1, lanes]
+            total = total * part + states[at, :, lanes]
+            decay = decay * part
+        high = decay.astype(jnp.bfloat16).astype(jnp.float32)
+        middle = (decay - high).astype(jnp.bfloat16).astype(jnp.float32)
+        low = decay - high - middle
+        place_row = iota((16, 128), 0)
+        tail = jnp.where(place_row == 0, high, jnp.where(place_row == 1, middle, low))
+        for q in range(4):
+            totals[4 * j + q, 0:32, :] = total[32 * q : 32 * q + 32].astype(jnp.bfloat16)
+            totals[4 * j + q, 32:48, :] = tail.astype(jnp.bfloat16)
+
+    pl.semaphore_wait(barrier, 34)
+
+    def outgoing(box, inbox, bank, k):
+        to = lax.rem(me + k, 32)
+        return pltpu.make_async_remote_copy(
+            src_ref=box.at[to],
+            dst_ref=inbox.at[me],
+            send_sem=send.at[bank, k],
+            recv_sem=recv.at[bank, me],
+            device_id=stretch(to),
+            device_id_type=MESH,
+        )
+
+    def expected(box, inbox, bank, k):
+        source = lax.rem(me + k, 32)
+        return pltpu.make_async_remote_copy(
+            src_ref=box.at[me],
+            dst_ref=inbox.at[source],
+            send_sem=send.at[bank, k],
+            recv_sem=recv.at[bank, source],
+            device_id=stretch(source),
+            device_id_type=MESH,
+        )
+
+    @pl.loop(1, 32)
+    def _(k):
+        outgoing(totals, arrived, 0, k).start()
+
+    arrived[me] = totals[me]
+
+    def within(k):
+        for g in range(groups):
+            inner_product = dot_nt(
+                outward[rows_of(k), g * STATE : (g + 1) * STATE],
+                inward[rows_of(k), g * STATE : (g + 1) * STATE],
+            )
+            cells = signal[rows_of(k), g * span : (g + 1) * span]
+            head_of = iota((BLOCK, span), 1) // HEAD_DIM
+            weights, content = [], []
+            for r in range(ratio):
+                h = g * ratio + r
+                below = column[rows_of(k), h : h + 1] + rowwise[k, h : h + 1, :]
+                above = (
+                    column[rows_of(k), heads + h : heads + h + 1]
+                    + rowwise[k, heads + h : heads + h + 1, :]
+                )
+                decay = jnp.exp2(jnp.where(lower, below, above))
+                both = jnp.where(
+                    row == col, rowwise[k, 2 * heads + h : 2 * heads + h + 1, :], decay
+                )
+                weights.append((inner_product * both).astype(jnp.bfloat16))
+                content.append(jnp.where(head_of == r, cells, jnp.zeros_like(cells)))
+            inner[rows_of(k), g * span : (g + 1) * span] = dot(
+                jnp.concatenate(weights, axis=1), jnp.concatenate(content, axis=0)
+            )
+
+    @pl.loop(0, blocks // 2)
+    def _(k):
+        within(k)
+
+    @pl.loop(1, 32)
+    def _(k):
+        expected(totals, arrived, 0, k).wait_recv()
+
+    flip = me >= 16
+
+    def hop(k, state):
+        at = jnp.where(flip, 31 - k, k)
+        onward[at] = state.astype(jnp.bfloat16)
+        message = arrived[at].astype(jnp.float32)
+        decay = message[32:33] + message[33:34] + message[34:35]
+        return state * decay + message[0:32]
+
+    lax.fori_loop(0, 32, hop, jnp.zeros((32, 128), jnp.float32))
+
+    @pl.loop(1, 32)
+    def _(k):
+        outgoing(onward, incoming, 1, k).start()
+
+    incoming[me] = onward[me]
+
+    @pl.loop(blocks // 2, blocks)
+    def _(k):
+        within(k)
+
+    @pl.loop(1, 32)
+    def _(k):
+        expected(onward, incoming, 1, k).wait_recv()
+
+    @pl.loop(0, wide // 128)
+    def _(j):
+        lanes = pl.ds(pl.multiple_of(j * 128, 128), 128)
+        backward = j >= half // 128
+        state = jnp.concatenate([incoming[4 * j + q] for q in range(4)], axis=0).astype(jnp.float32)
+        for k in range(blocks):
+            at = jnp.where(backward, blocks - 1 - k, k)
+            before[at, :, lanes] = state.astype(jnp.bfloat16)
+            state = state * decays[at, 0:1, lanes] + states[at, :, lanes]
+
+    def finish(k):
+        scale = dot(reading[rows_of(k), :], spread)
+        for g in range(groups):
+            lanes = slice(g * span, (g + 1) * span)
+            read = outward[rows_of(k), g * STATE : (g + 1) * STATE]
+            total = inner[rows_of(k), lanes]
+            for way in range(2):
+                placed = slice(way * half + g * span, way * half + (g + 1) * span)
+                total = total + dot(read, before[k, :, placed]) * scale[:, placed]
+            gated = total * silu(gate_ref[rows_of(k), lanes].astype(jnp.float32))
+            level = lax.rsqrt(jnp.mean(gated * gated, axis=-1, keepdims=True) + EPSILON)
+            mixed[rows_of(k), lanes] = (gated * level * gain_ref[:, lanes]).astype(jnp.bfloat16)
+
+    shard_rows = shards.shape[1]
+
+    def hand_over(k):
+        return pltpu.make_async_remote_copy(
+            src_ref=mixed.at[pl.ds(pl.multiple_of(step(x, k) * shard_rows, shard_rows), shard_rows)],
+            dst_ref=shards.at[x],
+            send_sem=send.at[2, k],
+            recv_sem=recv.at[2, x],
+            device_id={"x": step(x, k)},
+            device_id_type=MESH,
+        )
+
+    for k in (2, 1, 3, 0):
+
+        @pl.loop(0, 2)
+        def _(b):
+            finish(2 * step(x, k) + b)
+
+        if k:
+            hand_over(k).start()
+
+    shards[x] = mixed[pl.ds(pl.multiple_of(x * shard_rows, shard_rows), shard_rows), :]
+    load_wo.wait()
+    for k in (1, 3, 2):
+        source = step(x, k)
+        pltpu.make_async_remote_copy(
+            src_ref=mixed.at[pl.ds(0, shard_rows)],
+            dst_ref=shards.at[source],
+            send_sem=send.at[2, k],
+            recv_sem=recv.at[2, source],
+            device_id={"x": source},
+            device_id_type=MESH,
+        ).wait_recv()
+
+    @pl.loop(0, 8)
+    def _(k):
+        total = None
+        for at in range(4):
+            part = dot_nt(shards[at], wo[pl.ds(4 * k, 4), at].reshape(256, -1))
+            total = part if total is None else total + part
+        out_ref[:, pl.ds(pl.multiple_of(k * 256, 256), 256)] = total.astype(jnp.bfloat16)
+
+    @pl.loop(1, 32)
+    def _(k):
+        outgoing(totals, arrived, 0, k).wait_send()
+        outgoing(onward, incoming, 1, k).wait_send()
+
+    for k in (1, 2, 3):
+        hand_over(k).wait_send()
+
+
+def mix(mixed_in, gate, raw, taps, head_rows, out_gain, wo, shift):
+    rows, half = gate.shape
+    states = (mixed_in.shape[1] - half) // 2
+    blocks = rows // BLOCK
+    vmem = pl.BlockSpec(memory_space=pltpu.VMEM)
+    bf16, f32 = jnp.bfloat16, jnp.float32
+    return pl.pallas_call(
+        functools.partial(mixer_kernel, shift),
+        out_shape=jax.ShapeDtypeStruct((rows // 4, wo.shape[0] * wo.shape[2]), bf16),
+        in_specs=[vmem] * 6 + [pl.BlockSpec(memory_space=pl.ANY)],
+        out_specs=vmem,
+        scratch_shapes=[
+            pltpu.VMEM((rows, half), bf16),
+            pltpu.VMEM((rows, states), bf16),
+            pltpu.VMEM((rows, states), bf16),
+            pltpu.VMEM((rows, 128), f32),
+            pltpu.VMEM((blocks, 24, 128), f32),
+            pltpu.VMEM((rows, 128), bf16),
+            pltpu.VMEM((blocks, STATE, 2 * half), f32),
+            pltpu.VMEM((blocks, 8, 2 * half), f32),
+            pltpu.VMEM((blocks, STATE, 2 * half), bf16),
+            pltpu.VMEM((rows, half), f32),
+            pltpu.VMEM((32, 48, 128), bf16),
+            pltpu.VMEM((32, 48, 128), bf16),
+            pltpu.VMEM((32, 32, 128), bf16),
+            pltpu.VMEM((32, 32, 128), bf16),
+            pltpu.VMEM((rows, half), bf16),
+            pltpu.VMEM((4, rows // 4, half), bf16),
+            pltpu.VMEM(wo.shape, bf16),
+            pltpu.SemaphoreType.DMA((3, 32)),
+            pltpu.SemaphoreType.DMA((3, 32)),
+            pltpu.SemaphoreType.DMA,
+        ],
+        compiler_params=pltpu.CompilerParams(
+            collective_id=1, has_side_effects=True, vmem_limit_bytes=60 * 2**20
+        ),
+        name="mixer",
+    )(mixed_in, gate, raw, taps, head_rows, out_gain, wo)
 
 
 def local(
@@ -578,76 +851,23 @@
         ],
         axis=1,
     )
+    taps = jnp.concatenate([conv_value, conv_state_in, conv_state_out], axis=1)
+    head_rows = jnp.pad(
+        jnp.stack([step_offset.reshape(-1), -fading_speed.reshape(-1)]),
+        ((0, 0), (0, 128 - 2 * heads_local)),
+    )
     mixed_in, gate, raw, wo = gather_and_project(input_activations, norm_gain, a, w_gate, w_out.T)
-    sequence_extent = gate.shape[0]
-    stretch = lax.axis_index(SP)
-    row = lax.broadcasted_iota(jnp.int32, (sequence_extent + 2, 1), 0)
-    outside = ((row == 0) & (stretch == 0)) | (
-        (row == sequence_extent + 1) & (stretch == lax.axis_size(SP) - 1)
-    )
-    padded = jnp.where(outside, 0, mixed_in[HALO - 1 : 1 - HALO])
-    raw_forward, raw_backward = raw[:, :heads_local], raw[:, heads_local : 2 * heads_local]
-    taps = jnp.concatenate([conv_value, conv_state_in, conv_state_out], axis=1)
-    filtered = short_filter(padded, taps)
-    content_breadth = w_value.shape[1]
-    state_width = w_state_in.shape[1]
-    groups_local = state_width // STATE
-    ratio = heads_local // groups_local
-    signal = filtered[:, :content_breadth].reshape(sequence_extent, groups_local, ratio, HEAD_DIM)
-    inward = filtered[:, content_breadth : content_breadth + state_width].reshape(
-        sequence_extent, groups_local, STATE
-    )
-    outward = filtered[:, content_breadth + state_width :].reshape(
-        sequence_extent, groups_local, STATE
-    )
-    shift = math.log(sequence_extent * lax.axis_size(SP))
-    forward_step = jax.nn.softplus(
-        raw_forward.astype(jnp.float32) + step_offset[0] - shift
-    ).reshape(sequence_extent, groups_local, ratio)
-    backward_step = jax.nn.softplus(
-        raw_backward.astype(jnp.float32) + step_offset[1] - shift
-    ).reshape(sequence_extent, groups_local, ratio)
-    rates = fading_speed.reshape(2, groups_local, ratio)
-    count = sequence_extent // BLOCK
-    intersect = jnp.einsum(
-        "cqgn,ckgn->cqkg",
-        outward.reshape(count, BLOCK, groups_local, STATE),
-        inward.reshape(count, BLOCK, groups_local, STATE),
-        preferred_element_type=jnp.float32,
-    )
-    flipped = intersect[::-1, ::-1, ::-1]
-    ahead = one_way(signal, forward_step, rates[0], inward, outward, intersect)
-    behind = one_way(
-        signal[::-1], backward_step[::-1], rates[1], inward[::-1], outward[::-1], flipped
-    )
-    ahead_in = carried_in(
-        (ahead[2], ahead[3]),
-        SP,
-        link,
-        (jnp.ones_like(ahead[2]), jnp.zeros_like(ahead[3])),
-        False,
-    )
-    behind_in = carried_in(
-        (behind[2], behind[3]),
-        SP,
-        link,
-        (jnp.ones_like(behind[2]), jnp.zeros_like(behind[3])),
-        True,
-    )
-    combined = combine_ways(ahead, behind, ahead_in[1], behind_in[1])
-    gated = combined.reshape(sequence_extent, content_breadth) * jax.nn.silu(
-        gate.astype(jnp.float32)
-    )
-    grouped = rms_rows(
-        gated.reshape(sequence_extent, groups_local, content_breadth // groups_local)
-    ).reshape(sequence_extent, content_breadth)
-    mixed = (grouped * out_gain).astype(jnp.bfloat16)
-    everything = lax.all_to_all(
-        mixed.reshape(4, sequence_extent // 4, content_breadth), "x", split_axis=0, concat_axis=0
-    )
-    whole = wo.reshape(-1, 4, HEAD_DIM, content_breadth)
-    result = jnp.einsum("xtk,sxnk->tsn", everything, whole, preferred_element_type=jnp.float32)
-    return result.reshape(sequence_extent // 4, -1).astype(jnp.bfloat16)
+    shift = math.log(gate.shape[0] * lax.axis_size(SP))
+    return mix(
+        mixed_in,
+        gate,
+        raw,
+        taps,
+        head_rows,
+        out_gain.reshape(1, -1),
+        wo.reshape(-1, *wo.shape[3:]),
+        shift,
+    )
 
 
 def solution(mesh):

time: 373 us -> 140 us (0.38); the launches traced: 368 us -> 140 us
  other arithmetic: 104 us -> 2.57 us
  local copies, waits for them, and re-layouts: 74.6 us -> 6.31 us
  Pallas kernels: 80.6 us -> 131 us
  matrix products: 39.4 us -> 0 us
  blocking collectives: 37 us -> 0 us
  waiting for transfers between devices: 14.2 us -> 0 us
  between operations: 13.7 us -> 0.02 us
  starting transfers between devices: 4.28 us -> 0 us
    pallas_call x0 -> x1, Pallas kernels: none -> 50 us  [mix(): pl.pallas_call(functools.partial(mixer_kernel, shift), out_shape=jax.Shap...]
    another operation x6 -> x1, other arithmetic: 48.8 us -> 0.55 us  [local(): jnp.stack([step_offset.reshape(-1), -fading_speed.reshape(-1)])]
    dot_general x10 -> x0, matrix products: 39.4 us -> none  [the longest x2 11.6 us: one_way(): jnp.einsum('cqkgr,ckgrp->cqgrp', weights_mix, blocks, precision=lax.Preci...]
    all_gather x8 -> x0, blocking collectives: 37 us -> none  [carried_in(): pieces = jax.tree.map(lambda part: lax.all_gather(part, axis), subtotal)]
    rev x7 -> x0, local copies, waits for them, and re-layouts: 24.4 us -> none  [the longest x2 7.16 us: local(): flipped = intersect[::-1, ::-1, ::-1]]
    add x22 -> x0, other arithmetic: 22.5 us -> none  [the longest x16 16.6 us: advance(): return (state * inputs[1][..., None, None] + inputs[0], state)]
    dynamic_update_slice x16 -> x0, other arithmetic: 11.7 us -> none  [one_way(): lax.scan(advance, start_state, (block_states, jnp.exp(final)))]
    all_gather x4 -> x0, waiting for transfers between devices: 10.3 us -> none  [carried_in(): pieces = jax.tree.map(lambda part: lax.all_gather(part, axis), subtotal)]
  transfers between devices with their start and end apart: 5 -> 0, of which waited for: 2 -> 0; matrix products, arithmetic and copies ran while one was open for 24% -> 0% of each run, Pallas kernels for 0% -> 0%
where the time goes in v1:
time: 140 us
  Pallas kernels  131 us (94%)
  local copies, waits for them, and re-layouts  6.31 us (5%)
  other arithmetic  2.57 us (2%)
    pallas_call x1, Pallas kernels, gather_and_project(): pl.pallas_call(project_kernel, out_shape=(jax.ShapeDtypeStruct((4 * rows...  80.6 us
    pallas_call x1, Pallas kernels, mix(): pl.pallas_call(functools.partial(mixer_kernel, shift), out_shape=jax.Shap...  50 us
    unnamed x3, local copies, waits for them, and re-layouts  3.86 us

profile of v1, /device:TPU:1, one launch (start us, length us, event | category | flops | bytes accessed | tf_op | source)
XLA Modules:
  0.0 139.6 jit_solution(12802041603374898227)
XLA Ops:
  0.0 0.8 stack_reshape.3
  0.8 0.7 neg.13
  1.4 0.1 neg.14
  1.5 0.6 select_maximum_fusion.heads_ref
  2.1 0.8 copy.16
  2.9 0.8 copy.17
  3.6 1.3 pad_maximum_fusion.taps_ref
  5.0 1.6 %concatenate.6.a_ref = bf16[64,1152]{1,0:T(8,128)(2,1)} concatenate(bf16[64,512]{1,0:T(8,128)(2,1)} %param.18, bf16[64,256]{1,0:T(8,128)(2,1)} %param.19, bf16[64,256]{1,0:T(8,128)(2,1)} %param.20, bf16[64,8]{1,0:T(8,128)(2,1)S(1)} %copy.16, bf16[64,8]{1,0:T(8,128)(2,1)S(1)} %copy.17, bf16[64,112]{1,0:T(8,128)(2,1)S(1)} %broadcast_in_dim.3), dimensions={1} | concatenate | bytes 294912 | tf_op jit(solution)/shard_map/concatenate | solution.py:843
  6.6 80.6 %gather_project.1 = (bf16[1056,1024]{1,0:T(8,128)(2,1)}, bf16[1024,512]{1,0:T(8,128)(2,1)}, bf16[1024,128]{1,0:T(8,128)(2,1)}, bf16[4,4,2,4,64,512]{5,4,3,2,1,0:T(8,128)(2,1)}) custom-call(bf16[256,2048]{1,0:T(8,128)(2,1)} %tokens_ref.1, f32[1,2048]{1,0:T(1,128)} %bitcast.6, bf16[64,1152]{1,0:T(8,128)(2,1)} %concatenate.6.a_ref, bf16[64,512]{1,0:T(8,128)(2,1)} %g_ref.1, ...), custom_call_target="tpu_custom_call" | custom-call | tf_op jit(solution)/shard_map/gather_project/pallas_call | solution.py:413
  87.2 50.0 %mixer.1 = bf16[256,2048]{1,0:T(8,128)(2,1)} custom-call(bf16[1056,1024]{1,0:T(8,128)(2,1)} %get-tuple-element.9.mixed_ref, bf16[1024,512]{1,0:T(8,128)(2,1)} %get-tuple-element.10.gate_ref, bf16[1024,128]{1,0:T(8,128)(2,1)} %get-tuple-element.11.raw_ref, f32[3,1024]{1,0:T(4,128)} %pad_maximum_fusion.taps_ref, f32[2,128]{1,0:T(2,128)} %select_maximum_fusion.heads_ref, ...), custom_call_target="tpu_custom_call" | custom-call | tf_op jit(solution)/shard_map/mixer/pallas_call | solution.py:791
  137.3 2.3 %copy.19 = bf16[256,2048]{1,0:T(8,128)(2,1)} copy(bf16[256,2048]{1,0:T(8,128)(2,1)} %mixer.1) | data formatting | bytes 2097152
  (1 shorter events, 0.0 us)

commit v2 on v1

v2 whole, which is shorter than its diff:
```python
import functools
import math

import jax
import jax.numpy as jnp
from jax import lax
from jax.experimental import pallas as pl
from jax.experimental.pallas import tpu as pltpu
from jax.sharding import Mesh
from jax.sharding import PartitionSpec as P

HEAD_DIM = 64
STATE = 128
BLOCK = 128
SP = ("z", "y", "c")
SP_TP = ("z", "y", "c", "x")
EPSILON = 1e-06
MESH = pl.DeviceIdType.MESH
HALO = 16


def place():
    return [lax.axis_index(name) for name in ("z", "y", "c", "x")]


def step(at, by):
    return lax.rem(at + by + 4, 4)


def stretch_at(z, y, c, by):
    n = lax.rem(z * 8 + y * 2 + c + by + 32, 32)
    return {"z": n // 8, "y": lax.rem(n // 2, 4), "c": lax.rem(n, 2)}


class Wire:
    def __init__(self, send, recv):
        self.send, self.recv, self.count, self.sent = send, recv, 0, []

    def describe(self, source, target, to):
        k = self.count
        self.count += 1
        return pltpu.make_async_remote_copy(
            src_ref=source,
            dst_ref=target,
            send_sem=self.send.at[k],
            recv_sem=self.recv.at[k],
            device_id=to,
            device_id_type=MESH,
        )

    def go(self, source, to, target=None):
        copy = self.describe(source, source if target is None else target, to)
        copy.start()
        self.sent.append(copy)
        return copy

    def drain(self):
        for copy in self.sent:
            copy.wait_send()


class Ring:
    def __init__(self, wire, axis, at, block, low, high):
        self.wire, self.at = wire, at
        self.up, self.down = {axis: step(at, 1)}, {axis: step(at, 3)}
        self.block, self.low, self.high = block, low, high

    def start(self):
        self.a = self.wire.go(self.block(self.at), self.up)
        self.b = self.wire.go(self.block(self.at), self.down)

    def forward(self):
        self.a.wait_recv()
        self.c = self.wire.go(self.low(step(self.at, 3)), self.up)
        self.b.wait_recv()
        self.d = self.wire.go(self.high(step(self.at, 1)), self.down)

    def finish(self):
        self.c.wait_recv()
        self.d.wait_recv()


LOG2E = 1.4426950408889634


def dot_nt(a, b):
    return lax.dot_general(a, b, (((1,), (1,)), ((), ())), preferred_element_type=jnp.float32)


def dot_tn(a, b):
    return lax.dot_general(a, b, (((0,), (0,)), ((), ())), preferred_element_type=jnp.float32)


def dot(a, b, precision=None):
    return lax.dot_general(
        a, b, (((1,), (0,)), ((), ())), precision=precision, preferred_element_type=jnp.float32
    )


def iota(shape, dim):
    return lax.broadcasted_iota(jnp.int32, shape, dim)


def silu(v):
    return v / (1.0 + jnp.exp(-v))


def mixer_kernel(
    shift,
    tokens_hbm,
    norm_gain_ref,
    value_hbm,
    state_in_hbm,
    state_out_hbm,
    step_forward_ref,
    step_backward_ref,
    gate_hbm,
    w_out_hbm,
    tap_value_ref,
    tap_in_ref,
    tap_out_ref,
    heads_ref,
    gain_ref,
    out_ref,
    tokens,
    edges,
    normed,
    wv,
    ws,
    wg,
    wo,
    projected,
    gates,
    raw,
    signal,
    inward,
    outward,
    column,
    rowwise,
    reading,
    states,
    decays,
    before,
    inner,
    totals,
    arrived,
    onward,
    incoming,
    mixed,
    shards,
    relay,
    summed,
    send,
    recv,
    halo_send,
    halo_recv,
    state_send,
    state_recv,
    local_sem,
):
    z, y, c, x = place()
    me = z * 8 + y * 2 + c
    wire = Wire(send, recv)
    rows = tokens.shape[1]
    middle = rows // 2
    count = 4 * rows
    blocks = count // BLOCK
    half = signal.shape[1]
    wide = 2 * half
    groups = inward.shape[1] // STATE
    ratio = half // HEAD_DIM // groups
    heads = groups * ratio
    span = ratio * HEAD_DIM
    lead = inward.shape[1]
    partner = {"c": 1 - c}

    def stretch(n):
        return {"z": n // 8, "y": lax.rem(n // 2, 4), "c": lax.rem(n, 2)}

    own = [
        pltpu.make_async_copy(tokens_hbm, tokens.at[x], local_sem.at[0]),
        pltpu.make_async_copy(value_hbm, wv.at[z, y, c], local_sem.at[1]),
        pltpu.make_async_copy(state_in_hbm, ws.at[z, y, c, :, pl.ds(0, lead)], local_sem.at[2]),
        pltpu.make_async_copy(state_out_hbm, ws.at[z, y, c, :, pl.ds(lead, lead)], local_sem.at[3]),
        pltpu.make_async_copy(gate_hbm, wg.at[z, y, c], local_sem.at[4]),
        pltpu.make_async_copy(w_out_hbm, wo.at[z, y, c, x], local_sem.at[5]),
    ]
    for copy in own:
        copy.start()
    depth = step_forward_ref.shape[1]
    steps = jnp.concatenate(
        [
            step_forward_ref[...].astype(jnp.float32),
            step_backward_ref[...].astype(jnp.float32),
            jnp.zeros((128 - 2 * heads, depth), jnp.float32),
        ],
        axis=0,
    )
    steps = jnp.concatenate([steps, jnp.zeros((128, 128 - depth), jnp.float32)], axis=1).T
    ws[z, y, c, :, 2 * lead :] = steps[0:depth].astype(jnp.bfloat16)

    barrier = pltpu.get_barrier_semaphore()

    @pl.loop(1, 32)
    def _(k):
        pl.semaphore_signal(
            barrier, inc=1, device_id=stretch(lax.rem(me + k, 32)), device_id_type=MESH
        )

    for k in range(1, 4):
        others = [{"x": step(x, k)}]
        others += [dict(stretch_at(z, y, c, by), x=step(x, k)) for by in (1, 31)]
        for other in others:
            pl.semaphore_signal(barrier, inc=1, device_id=other, device_id_type=MESH)
    for copy in own:
        copy.wait()
    pl.semaphore_wait(barrier, 40)

    low, high = pl.ds(0, middle), pl.ds(middle, middle)
    up, down = {"x": step(x, 1)}, {"x": step(x, 3)}
    up_low = wire.go(tokens.at[x, low], up)
    down_high = wire.go(tokens.at[x, high], down)
    up_high = wire.go(tokens.at[x, high], up)
    down_low = wire.go(tokens.at[x, low], down)

    halos = [
        [
            pltpu.make_async_remote_copy(
                src_ref=tokens.at[x, pl.ds(offset, HALO)],
                dst_ref=edges.at[slot],
                send_sem=halo_send.at[4 * slot + k],
                recv_sem=halo_recv.at[slot],
                device_id=dict(stretch_at(z, y, c, by), x=k),
                device_id_type=MESH,
            )
            for k in range(4)
        ]
        for slot, (by, offset) in enumerate(((1, rows - HALO), (31, 0)))
    ]

    def first(buffer, axis, keep=()):
        def at(n, part):
            spot = (z, n, c) if axis == "y" else (n, y, c)
            if keep:
                start, size = keep
                return buffer.at[(*spot, pl.ds(start, size) if part is None else start + part)]
            return buffer.at[spot] if part is None else buffer.at[(*spot, pl.ds(32 * part, 32))]

        here = y if axis == "y" else z
        return Ring(
            wire, axis, here, lambda n: at(n, None), lambda n: at(n, 0), lambda n: at(n, 1)
        )

    def group(buffer, axis, n, part, keep):
        some = pl.ds(0, 4) if part is None else pl.ds(2 * part, 2)
        spot = (n, some, c) if axis == "z" else (some, n, c)
        return buffer.at[(*spot, pl.ds(*keep))] if keep else buffer.at[spot]

    def second(buffer, axis, keep=()):
        here = y if axis == "y" else z
        return Ring(
            wire,
            axis,
            here,
            lambda n: group(buffer, axis, n, None, keep),
            lambda n: group(buffer, axis, n, 0, keep),
            lambda n: group(buffer, axis, n, 1, keep),
        )

    pairs = {}

    def across(name, buffer, axis, by, keep=()):
        here = y if axis == "y" else z
        copy = wire.go(group(buffer, axis, step(here, by), None, keep), partner)
        pairs.setdefault(name, []).append(copy)

    v_first, s_first = first(wv, "y"), first(ws, "z")
    v_first.start()
    s_first.start()

    @pl.when(x == 3)
    def _():
        for copy in halos[0]:
            copy.start()

    @pl.when(x == 0)
    def _():
        for copy in halos[1]:
            copy.start()

    wo_x = Ring(
        wire,
        "x",
        x,
        lambda at: wo.at[z, y, c, at],
        lambda at: wo.at[z, y, c, at, pl.ds(0, 32)],
        lambda at: wo.at[z, y, c, at, pl.ds(32, 32)],
    )
    wo_x.start()

    def main_row(shard):
        return HALO + shard * rows

    def normalize(ref, size, to):
        @pl.loop(0, size // 16)
        def _(k):
            start = pl.multiple_of(k * 16, 16)
            cells = ref[pl.ds(start, 16), :].astype(jnp.float32)
            scale = lax.rsqrt(jnp.mean(cells * cells, axis=-1, keepdims=True) + EPSILON)
            normed[pl.ds(pl.multiple_of(to + start, 16), 16), :] = (
                cells * scale * norm_gain_ref[...]
            ).astype(jnp.bfloat16)

    def project(start, size):
        taken = pl.ds(start, size)

        @pl.loop(0, half // 256)
        def _(k):
            columns = pl.ds(pl.multiple_of(k * 256, 256), 256)
            projected[taken, columns] = dot(
                normed[taken, :], wv[:, :, :, :, columns].reshape(-1, 256)
            ).astype(jnp.bfloat16)

        @pl.loop(0, 2 * lead // 256)
        def _(k):
            columns = pl.ds(pl.multiple_of(k * 256, 256), 256)
            projected[taken, pl.ds(pl.multiple_of(half + k * 256, 256), 256)] = dot(
                normed[taken, :], ws[:, :, :, :, columns].reshape(-1, 256)
            ).astype(jnp.bfloat16)

    def project_shard(shard):
        project(pl.multiple_of(main_row(shard), 16), rows)
        raw[pl.ds(pl.multiple_of(shard * rows, rows), rows), :] = dot(
            normed[pl.ds(pl.multiple_of(main_row(shard), 16), rows), :],
            ws[:, :, :, :, 2 * lead :].reshape(-1, 128),
        ).astype(jnp.bfloat16)

    def project_gate(shard):
        @pl.loop(0, half // 256)
        def _(k):
            columns = pl.ds(pl.multiple_of(k * 256, 256), 256)
            gates[pl.ds(pl.multiple_of(shard * rows, rows), rows), columns] = silu(
                dot(
                    normed[pl.ds(pl.multiple_of(main_row(shard), 16), rows), :],
                    wg[:, :, :, :, columns].reshape(-1, 256),
                )
                .astype(jnp.bfloat16)
                .astype(jnp.float32)
            ).astype(jnp.bfloat16)

    normalize(tokens.at[x], rows, main_row(x))

    v_first.forward()
    s_first.forward()
    v_first.finish()
    v_second = second(wv, "z")
    v_second.start()
    across("v", wv, "z", 0)
    s_first.finish()
    s_second = second(ws, "y")
    s_second.start()
    across("s", ws, "y", 0)
    g_first = first(wg, "z")
    g_first.start()

    for slot in range(2):
        halos[slot][0].wait_recv()
    normalize(edges.at[0], HALO, 0)
    normalize(edges.at[1], HALO, main_row(4))

    up_low.wait_recv()
    far_low = wire.go(tokens.at[step(x, 3), low], up)
    down_high.wait_recv()
    far_high = wire.go(tokens.at[step(x, 1), high], down)
    normalize(tokens.at[step(x, 3), low], middle, main_row(step(x, 3)))
    normalize(tokens.at[step(x, 1), high], middle, main_row(step(x, 1)) + middle)

    v_second.forward()
    s_second.forward()
    for by in (3, 1):
        across("v", wv, "z", by)
        across("s", ws, "y", by)
    g_first.forward()
    v_second.finish()
    across("v", wv, "z", 2)
    s_second.finish()
    across("s", ws, "y", 2)
    g_first.finish()
    g_second = second(wg, "y")
    g_second.start()
    across("g", wg, "y", 0)
    for copy in pairs["v"] + pairs["s"]:
        copy.wait_recv()
    project_shard(x)

    up_high.wait_recv()
    down_low.wait_recv()
    wo_x.forward()
    normalize(tokens.at[step(x, 3), high], middle, main_row(step(x, 3)) + middle)
    normalize(tokens.at[step(x, 1), low], middle, main_row(step(x, 1)))
    wo_x.finish()
    lo_first, hi_first = first(wo, "y", (0, 2)), first(wo, "z", (2, 2))
    lo_first.start()
    hi_first.start()
    project_shard(step(x, 3))
    g_second.forward()
    across("g", wg, "y", 3)
    across("g", wg, "y", 1)
    project_shard(step(x, 1))

    @pl.when(me > 0)
    def _():
        project(0, HALO)

    @pl.when(me == 0)
    def _():
        projected[0:HALO, :] = jnp.zeros((HALO, wide), jnp.bfloat16)

    @pl.when(me < 31)
    def _():
        project(main_row(4), HALO)

    @pl.when(me == 31)
    def _():
        projected[main_row(4) :, :] = jnp.zeros((HALO, wide), jnp.bfloat16)

    lo_first.forward()
    hi_first.forward()

    row, col = iota((BLOCK, BLOCK), 0), iota((BLOCK, BLOCK), 1)
    lower = row >= col
    triangle = jnp.where(lower, 1.0, 0.0)
    spread = jnp.where(
        iota((128, wide), 1) // HEAD_DIM == iota((128, wide), 0), 1.0, 0.0
    ).astype(jnp.bfloat16)
    forward_lane = iota((BLOCK, 128), 1) < heads

    def rows_of(k):
        return pl.ds(pl.multiple_of(k * BLOCK, BLOCK), BLOCK)

    def prepare(k):
        window = pl.ds(pl.multiple_of(k * BLOCK, BLOCK), BLOCK + 2 * HALO)
        for at in range(0, wide, 128):
            if at < half:
                tap_ref, target, begin = tap_value_ref, signal, at
            elif at < half + lead:
                tap_ref, target, begin = tap_in_ref, inward, at - half
            else:
                tap_ref, target, begin = tap_out_ref, outward, at - half - lead
            cells = projected[window, at : at + 128].astype(jnp.float32)
            tap = tap_ref[:, begin : begin + 128]
            total = (
                tap[0:1] * pltpu.roll(cells, 1, 0)
                + tap[1:2] * cells
                + tap[2:3] * pltpu.roll(cells, BLOCK + 2 * HALO - 1, 0)
            )[HALO : HALO + BLOCK]
            target[rows_of(k), begin : begin + 128] = silu(total).astype(jnp.bfloat16)

        size = jax.nn.softplus(
            raw[rows_of(k), :].astype(jnp.float32) + heads_ref[0:1, :] - shift
        )
        logs = size * heads_ref[1:2, :]
        through = dot(triangle, logs, lax.Precision.HIGHEST)
        until = through - logs
        whole = through[BLOCK - 1 : BLOCK, :]
        logsize = jnp.log(size)
        column[rows_of(k), :] = jnp.where(forward_lane, through, -until) * LOG2E
        turned = (jnp.where(forward_lane, logsize - through, logsize + until) * LOG2E).T
        sizes = size.T
        rowwise[k, 0 : 2 * heads, :] = turned[0 : 2 * heads]
        rowwise[k, 2 * heads : 3 * heads, :] = sizes[0:heads] + sizes[heads : 2 * heads]
        reading[rows_of(k), :] = jnp.exp(
            jnp.where(forward_lane, through, whole - until)
        ).astype(jnp.bfloat16)
        weight = size * jnp.exp(jnp.where(forward_lane, whole - through, until))
        decays[k] = dot(
            jnp.broadcast_to(jnp.exp(whole), (8, 128)),
            spread.astype(jnp.float32),
            lax.Precision.HIGHEST,
        )
        weights = dot(weight.astype(jnp.bfloat16), spread)
        for way in range(2):
            for g in range(groups):
                lanes = slice(g * span, (g + 1) * span)
                placed = slice(way * half + g * span, way * half + (g + 1) * span)
                content = (
                    signal[rows_of(k), lanes].astype(jnp.float32) * weights[:, placed]
                ).astype(jnp.bfloat16)
                states[k, :, placed] = dot_tn(
                    inward[rows_of(k), g * STATE : (g + 1) * STATE], content
                )

    far = 2 * step(x, 2)

    @pl.loop(0, 4)
    def _(k):
        prepare(lax.rem(far + 3 + k, blocks))

    lo_first.finish()
    lo_second = second(wo, "z", (0, 2))
    lo_second.start()
    across("o", wo, "z", 0, (0, 2))
    hi_first.finish()
    hi_second = second(wo, "y", (2, 2))
    hi_second.start()
    across("o", wo, "y", 0, (2, 2))

    g_second.finish()
    across("g", wg, "y", 2)
    for copy in pairs["g"]:
        copy.wait_recv()
    project_gate(x)
    project_gate(step(x, 3))
    project_gate(step(x, 1))

    far_low.wait_recv()
    far_high.wait_recv()
    normalize(tokens.at[step(x, 2)], rows, main_row(step(x, 2)))
    project_shard(step(x, 2))

    @pl.loop(0, 4)
    def _(k):
        prepare(lax.rem(far + 7 + k, blocks))

    @pl.loop(0, wide // 128)
    def _(j):
        lanes = pl.ds(pl.multiple_of(j * 128, 128), 128)
        backward = j >= half // 128
        total = jnp.zeros((STATE, 128), jnp.float32)
        decay = jnp.ones((1, 128), jnp.float32)
        for k in range(blocks):
            at = jnp.where(backward, blocks - 1 - k, k)
            part = decays[at, 0:1, lanes]
            total = total * part + states[at, :, lanes]
            decay = decay * part
        upper = decay.astype(jnp.bfloat16).astype(jnp.float32)
        centre = (decay - upper).astype(jnp.bfloat16).astype(jnp.float32)
        rest = decay - upper - centre
        place_row = iota((16, 128), 0)
        tail = jnp.where(place_row == 0, upper, jnp.where(place_row == 1, centre, rest))
        for q in range(4):
            totals[4 * j + q, 0:32, :] = total[32 * q : 32 * q + 32].astype(jnp.bfloat16)
            totals[4 * j + q, 32:48, :] = tail.astype(jnp.bfloat16)

    def outgoing(box, inbox, bank, k):
        to = lax.rem(me + k, 32)
        return pltpu.make_async_remote_copy(
            src_ref=box.at[to],
            dst_ref=inbox.at[me],
            send_sem=state_send.at[bank, k],
            recv_sem=state_recv.at[bank, me],
            device_id=stretch(to),
            device_id_type=MESH,
        )

    def expected(box, inbox, bank, k):
        source = lax.rem(me + k, 32)
        return pltpu.make_async_remote_copy(
            src_ref=box.at[me],
            dst_ref=inbox.at[source],
            send_sem=state_send.at[bank, k],
            recv_sem=state_recv.at[bank, source],
            device_id=stretch(source),
            device_id_type=MESH,
        )

    @pl.loop(1, 32)
    def _(k):
        outgoing(totals, arrived, 0, k).start()

    arrived[me] = totals[me]

    lo_second.forward()
    hi_second.forward()
    for by in (3, 1):
        across("o", wo, "z", by, (0, 2))
        across("o", wo, "y", by, (2, 2))

    def within(k):
        for g in range(groups):
            inner_product = dot_nt(
                outward[rows_of(k), g * STATE : (g + 1) * STATE],
                inward[rows_of(k), g * STATE : (g + 1) * STATE],
            )
            cells = signal[rows_of(k), g * span : (g + 1) * span]
            head_of = iota((BLOCK, span), 1) // HEAD_DIM
            weights, content = [], []
            for r in range(ratio):
                h = g * ratio + r
                below = column[rows_of(k), h : h + 1] + rowwise[k, h : h + 1, :]
                above = (
                    column[rows_of(k), heads + h : heads + h + 1]
                    + rowwise[k, heads + h : heads + h + 1, :]
                )
                decay = jnp.exp2(jnp.where(lower, below, above))
                both = jnp.where(
                    row == col, rowwise[k, 2 * heads + h : 2 * heads + h + 1, :], decay
                )
                weights.append((inner_product * both).astype(jnp.bfloat16))
                content.append(jnp.where(head_of == r, cells, jnp.zeros_like(cells)))
            inner[rows_of(k), g * span : (g + 1) * span] = dot(
                jnp.concatenate(weights, axis=1), jnp.concatenate(content, axis=0)
            )

    project_gate(step(x, 2))

    @pl.loop(0, blocks // 2)
    def _(k):
        within(k)

    @pl.loop(1, 32)
    def _(k):
        expected(totals, arrived, 0, k).wait_recv()

    flip = me >= 16

    def hop(k, state):
        at = jnp.where(flip, 31 - k, k)
        onward[at] = state.astype(jnp.bfloat16)
        message = arrived[at].astype(jnp.float32)
        decay = message[32:33] + message[33:34] + message[34:35]
        return state * decay + message[0:32]

    lax.fori_loop(0, 32, hop, jnp.zeros((32, 128), jnp.float32))

    @pl.loop(1, 32)
    def _(k):
        outgoing(onward, incoming, 1, k).start()

    incoming[me] = onward[me]

    @pl.loop(blocks // 2, blocks)
    def _(k):
        within(k)

    @pl.loop(1, 32)
    def _(k):
        expected(onward, incoming, 1, k).wait_recv()

    @pl.loop(0, wide // 128)
    def _(j):
        lanes = pl.ds(pl.multiple_of(j * 128, 128), 128)
        backward = j >= half // 128
        state = jnp.concatenate([incoming[4 * j + q] for q in range(4)], axis=0).astype(jnp.float32)
        for k in range(blocks):
            at = jnp.where(backward, blocks - 1 - k, k)
            before[at, :, lanes] = state.astype(jnp.bfloat16)
            state = state * decays[at, 0:1, lanes] + states[at, :, lanes]

    def finish(k):
        scale = dot(reading[rows_of(k), :], spread)
        for g in range(groups):
            lanes = slice(g * span, (g + 1) * span)
            read = outward[rows_of(k), g * STATE : (g + 1) * STATE]
            total = inner[rows_of(k), lanes]
            for way in range(2):
                placed = slice(way * half + g * span, way * half + (g + 1) * span)
                total = total + dot(read, before[k, :, placed]) * scale[:, placed]
            gated = total * gates[rows_of(k), lanes].astype(jnp.float32)
            level = lax.rsqrt(jnp.mean(gated * gated, axis=-1, keepdims=True) + EPSILON)
            mixed[rows_of(k), lanes] = (gated * level * gain_ref[:, lanes]).astype(jnp.bfloat16)

    def finish_shard(shard):
        @pl.loop(0, 2)
        def _(b):
            finish(2 * shard + b)

    def part(shard, some):
        start, size = some
        return mixed.at[pl.ds(pl.multiple_of(shard * rows + start, middle), size)]

    finish_shard(step(x, 2))
    relay_up = wire.go(part(step(x, 2), (0, middle)), up, relay.at[0])
    relay_down = wire.go(part(step(x, 2), (middle, middle)), down, relay.at[1])
    finish_shard(step(x, 1))
    near_up = wire.go(part(step(x, 1), (0, rows)), up, shards.at[x])
    finish_shard(step(x, 3))
    near_down = wire.go(part(step(x, 3), (0, rows)), down, shards.at[x])
    lo_second.finish()
    across("o", wo, "z", 2, (0, 2))
    hi_second.finish()
    across("o", wo, "y", 2, (2, 2))
    finish_shard(x)
    shards[x] = mixed[pl.ds(pl.multiple_of(x * rows, rows), rows), :]
    relay_up.wait_recv()
    far_up = wire.go(relay.at[0], up, shards.at[step(x, 3), low])
    relay_down.wait_recv()
    far_down = wire.go(relay.at[1], down, shards.at[step(x, 1), high])
    for copy in pairs["o"]:
        copy.wait_recv()

    def contribute(at, begin, end):
        @pl.loop(0, 8)
        def _(k):
            columns = pl.ds(pl.multiple_of(k * 256, 256), 256)
            weight = wo[k // 2, pl.ds(2 * lax.rem(k, 2), 2), :, at].reshape(256, -1)
            total = dot_nt(shards[at], weight)
            if not begin:
                total = total + summed[:, columns]
            if end:
                out_ref[:, columns] = total.astype(out_ref.dtype)
            else:
                summed[:, columns] = total

    contribute(x, True, False)
    near_up.wait_recv()
    contribute(step(x, 3), False, False)
    near_down.wait_recv()
    contribute(step(x, 1), False, False)
    far_up.wait_recv()
    far_down.wait_recv()
    contribute(step(x, 2), False, True)

    wire.drain()

    @pl.loop(1, 32)
    def _(k):
        outgoing(totals, arrived, 0, k).wait_send()
        outgoing(onward, incoming, 1, k).wait_send()

    @pl.when(x == 3)
    def _():
        for copy in halos[0]:
            copy.wait_send()

    @pl.when(x == 0)
    def _():
        for copy in halos[1]:
            copy.wait_send()


COPIES = 80


def mix(
    tokens,
    norm_gain,
    w_gate,
    w_value,
    w_state_in,
    w_state_out,
    w_step_forward,
    w_step_backward,
    head_rows,
    conv_value,
    conv_state_in,
    conv_state_out,
    out_gain,
    w_out,
):
    rows, width = tokens.shape
    depth, half = w_value.shape
    states = w_state_in.shape[1]
    blocks = 4 * rows // BLOCK
    vmem, anywhere = pl.BlockSpec(memory_space=pltpu.VMEM), pl.BlockSpec(memory_space=pl.ANY)
    bf16, f32 = jnp.bfloat16, jnp.float32
    return pl.pallas_call(
        functools.partial(mixer_kernel, math.log(4 * rows * lax.axis_size(SP))),
        out_shape=jax.ShapeDtypeStruct((rows, width), OUT_TYPE),
        in_specs=[anywhere, vmem] + [anywhere] * 3 + [vmem] * 2 + [anywhere] * 2 + [vmem] * 5,
        out_specs=vmem,
        scratch_shapes=[
            pltpu.VMEM((4, rows, width), bf16),
            pltpu.VMEM((2, HALO, width), bf16),
            pltpu.VMEM((4 * rows + 2 * HALO, width), bf16),
            pltpu.VMEM((4, 4, 2, depth, half), bf16),
            pltpu.VMEM((4, 4, 2, depth, 2 * states + 128), bf16),
            pltpu.VMEM((4, 4, 2, depth, half), bf16),
            pltpu.VMEM((4, 4, 2, 4, depth, half), bf16),
            pltpu.VMEM((4 * rows + 2 * HALO, 2 * half), bf16),
            pltpu.VMEM((4 * rows, half), bf16),
            pltpu.VMEM((4 * rows, 128), bf16),
            pltpu.VMEM((4 * rows, half), bf16),
            pltpu.VMEM((4 * rows, states), bf16),
            pltpu.VMEM((4 * rows, states), bf16),
            pltpu.VMEM((4 * rows, 128), f32),
            pltpu.VMEM((blocks, 24, 128), f32),
            pltpu.VMEM((4 * rows, 128), bf16),
            pltpu.VMEM((blocks, STATE, 2 * half), f32),
            pltpu.VMEM((blocks, 8, 2 * half), f32),
            pltpu.VMEM((blocks, STATE, 2 * half), bf16),
            pltpu.VMEM((4 * rows, half), f32),
            pltpu.VMEM((32, 48, 128), bf16),
            pltpu.VMEM((32, 48, 128), bf16),
            pltpu.VMEM((32, 32, 128), bf16),
            pltpu.VMEM((32, 32, 128), bf16),
            pltpu.VMEM((4 * rows, half), bf16),
            pltpu.VMEM((4, rows, half), bf16),
            pltpu.VMEM((2, rows // 2, half), bf16),
            pltpu.VMEM((rows, width), f32),
            pltpu.SemaphoreType.DMA((COPIES,)),
            pltpu.SemaphoreType.DMA((COPIES,)),
            pltpu.SemaphoreType.DMA((8,)),
            pltpu.SemaphoreType.DMA((2,)),
            pltpu.SemaphoreType.DMA((2, 32)),
            pltpu.SemaphoreType.DMA((2, 32)),
            pltpu.SemaphoreType.DMA((6,)),
        ],
        compiler_params=pltpu.CompilerParams(
            collective_id=0, has_side_effects=True, vmem_limit_bytes=60 * 2**20
        ),
        name="mixer",
    )(
        tokens,
        norm_gain.reshape(1, -1),
        w_value,
        w_state_in,
        w_state_out,
        w_step_forward.T,
        w_step_backward.T,
        w_gate,
        w_out.T,
        conv_value,
        conv_state_in,
        conv_state_out,
        head_rows,
        out_gain.reshape(1, -1),
    )


OUT_TYPE = jnp.bfloat16


def local(
    input_activations,
    norm_gain,
    w_gate,
    w_value,
    w_state_in,
    w_state_out,
    w_step_forward,
    w_step_backward,
    step_offset,
    fading_speed,
    conv_value,
    conv_state_in,
    conv_state_out,
    out_gain,
    w_out,
):
    head_rows = jnp.pad(
        jnp.stack([step_offset.reshape(-1), -fading_speed.reshape(-1)]),
        ((0, 0), (0, 128 - step_offset.size)),
    )
    return mix(
        input_activations,
        norm_gain,
        w_gate,
        w_value,
        w_state_in,
        w_state_out,
        w_step_forward,
        w_step_backward,
        head_rows,
        conv_value,
        conv_state_in,
        conv_state_out,
        out_gain,
        w_out,
    )


def solution(mesh):
    torus = Mesh(mesh.devices.reshape(4, 4, 2, 4), SP_TP)
    return jax.shard_map(
        local,
        mesh=torus,
        in_specs=(
            P(SP_TP, None),
            P(),
            P(SP, "x"),
            P(SP, "x"),
            P(SP, "x"),
            P(SP, "x"),
            P(SP, "x"),
            P(SP, "x"),
            P(None, "x"),
            P(None, "x"),
            P(None, "x"),
            P(None, "x"),
            P(None, "x"),
            P("x"),
            P("x", SP),
        ),
        out_specs=P(SP_TP, None),
        check_vma=False,
    )
```

time: 140 us -> 122 us (0.87)
  Pallas kernels: 131 us -> 117 us
  local copies, waits for them, and re-layouts: 6.31 us -> 3.75 us
  other arithmetic: 2.57 us -> 0.57 us
    pallas_call x2 -> x1, Pallas kernels: 131 us -> 117 us  [mix(): pl.pallas_call(functools.partial(mixer_kernel, math.log(4 * rows * lax.ax...]
    concatenate x1 -> x0, local copies, waits for them, and re-layouts: 1.61 us -> none  [local(): jnp.concatenate([w_value, w_state_in, w_state_out, w_step_forward, w_step...]
    unnamed x3 -> x5, local copies, waits for them, and re-layouts: 3.86 us -> 3.58 us
where the time goes in v2:
time: 122 us
  Pallas kernels  117 us (96%)
  local copies, waits for them, and re-layouts  3.75 us (3%)
    pallas_call x1, Pallas kernels, mix(): pl.pallas_call(functools.partial(mixer_kernel, math.log(4 * rows * lax.ax...  117 us
    unnamed x5, local copies, waits for them, and re-layouts  3.58 us

profile of v2, /device:TPU:1, one launch (start us, length us, event | category | flops | bytes accessed | tf_op | source)
XLA Modules:
  0.0 121.8 jit_solution(17863844660633675720)
XLA Ops:
  0.0 0.0 copy-start.1
  0.0 0.7 copy-done.1
  0.7 0.0 copy-start
  0.7 0.1 stack_reshape.3
  0.8 0.6 copy-done
  1.4 0.1 neg.14
  1.4 0.6 select_maximum_fusion.heads_ref
  2.0 117.4 %mixer.1 = bf16[256,2048]{1,0:T(8,128)(2,1)} custom-call(bf16[256,2048]{1,0:T(8,128)(2,1)} %tokens_hbm.1, f32[1,2048]{1,0:T(1,128)} %bitcast.6, bf16[64,512]{1,0:T(8,128)(2,1)} %value_hbm.1, bf16[64,256]{1,0:T(8,128)(2,1)} %state_in_hbm.1, bf16[64,256]{1,0:T(8,128)(2,1)} %state_out_hbm.1, bf16[8,64]{1,0:T(8,128)(2,1)} %bitcast.7, bf16[8,64]{1,0:T(8,128)(2,1)} %bitcast.8, ...), custom_call_target="tpu_custom_call" | custom-call | tf_op jit(solution)/shard_map/mixer/pallas_call | solution.py:757
  119.5 2.3 %copy.17 = bf16[256,2048]{1,0:T(8,128)(2,1)} copy(bf16[256,2048]{1,0:T(8,128)(2,1)} %mixer.1) | data formatting | bytes 2097152
  (1 shorter events, 0.0 us)
Async XLA Ops:
  0.0 0.7 copy-start.1
  0.7 0.7 copy-start

commit v3 on v2

--- a/solution.py
+++ b/solution.py
@@ -102,26 +102,40 @@
 
 
 def silu(v):
-    return v / (1.0 + jnp.exp(-v))
+    part = 0.5 * v
+    return part + part * jnp.tanh(part)
 
 
 def mixer_kernel(
     shift,
     tokens_hbm,
-    norm_gain_ref,
     value_hbm,
     state_in_hbm,
     state_out_hbm,
+    gate_hbm,
+    w_out_hbm,
+    norm_gain_hbm,
+    step_forward_hbm,
+    step_backward_hbm,
+    tap_value_hbm,
+    tap_in_hbm,
+    tap_out_hbm,
+    offset_hbm,
+    speed_hbm,
+    gain_hbm,
+    out_ref,
+    norm_gain_ref,
     step_forward_ref,
     step_backward_ref,
-    gate_hbm,
-    w_out_hbm,
     tap_value_ref,
     tap_in_ref,
     tap_out_ref,
+    offset_ref,
+    speed_ref,
+    gain_ref,
     heads_ref,
-    gain_ref,
-    out_ref,
+    squares,
+    fades,
     tokens,
     edges,
     normed,
@@ -137,7 +151,6 @@
     outward,
     column,
     rowwise,
-    reading,
     states,
     decays,
     before,
@@ -152,8 +165,6 @@
     summed,
     send,
     recv,
-    halo_send,
-    halo_recv,
     state_send,
     state_recv,
     local_sem,
@@ -185,8 +196,30 @@
         pltpu.make_async_copy(gate_hbm, wg.at[z, y, c], local_sem.at[4]),
         pltpu.make_async_copy(w_out_hbm, wo.at[z, y, c, x], local_sem.at[5]),
     ]
+    small = (
+        (step_forward_hbm, step_forward_ref),
+        (step_backward_hbm, step_backward_ref),
+        (offset_hbm, offset_ref),
+        (speed_hbm, speed_ref),
+        (norm_gain_hbm, norm_gain_ref),
+        (tap_value_hbm, tap_value_ref),
+        (tap_in_hbm, tap_in_ref),
+        (tap_out_hbm, tap_out_ref),
+        (gain_hbm, gain_ref),
+    )
+    own += [
+        pltpu.make_async_copy(source, target, local_sem.at[6 + k])
+        for k, (source, target) in enumerate(small)
+    ]
     for copy in own:
         copy.start()
+    barrier = pltpu.get_barrier_semaphore()
+
+    near = [{axis: step(at, by)} for axis, at in (("x", x), ("y", y), ("z", z)) for by in (1, 3)]
+    for other in near + [partner]:
+        pl.semaphore_signal(barrier, inc=1, device_id=other, device_id_type=MESH)
+    for copy in own:
+        copy.wait()
     depth = step_forward_ref.shape[1]
     steps = jnp.concatenate(
         [
@@ -198,23 +231,28 @@
     )
     steps = jnp.concatenate([steps, jnp.zeros((128, 128 - depth), jnp.float32)], axis=1).T
     ws[z, y, c, :, 2 * lead :] = steps[0:depth].astype(jnp.bfloat16)
-
-    barrier = pltpu.get_barrier_semaphore()
-
-    @pl.loop(1, 32)
-    def _(k):
-        pl.semaphore_signal(
-            barrier, inc=1, device_id=stretch(lax.rem(me + k, 32)), device_id_type=MESH
-        )
-
-    for k in range(1, 4):
-        others = [{"x": step(x, k)}]
-        others += [dict(stretch_at(z, y, c, by), x=step(x, k)) for by in (1, 31)]
-        for other in others:
-            pl.semaphore_signal(barrier, inc=1, device_id=other, device_id_type=MESH)
-    for copy in own:
-        copy.wait()
-    pl.semaphore_wait(barrier, 40)
+    lines = jnp.concatenate(
+        [
+            jnp.concatenate([ref[w : w + 1, :] * sign for w in range(2)], axis=1)
+            for ref, sign in ((offset_ref, 1.0), (speed_ref, -1.0))
+        ],
+        axis=0,
+    )
+    lines = jnp.concatenate([lines, jnp.zeros((2, 128 - 2 * heads), jnp.float32)], axis=1)
+    heads_ref[...] = jnp.concatenate([lines, jnp.zeros((126, 128), jnp.float32)], axis=0).T[
+        0 : 2 * heads
+    ]
+    pl.semaphore_wait(barrier, 7)
+
+    wo_x = Ring(
+        wire,
+        "x",
+        x,
+        lambda at: wo.at[z, y, c, at],
+        lambda at: wo.at[z, y, c, at, pl.ds(0, 32)],
+        lambda at: wo.at[z, y, c, at, pl.ds(32, 32)],
+    )
+    wo_x.start()
 
     low, high = pl.ds(0, middle), pl.ds(middle, middle)
     up, down = {"x": step(x, 1)}, {"x": step(x, 3)}
@@ -222,21 +260,6 @@
     down_high = wire.go(tokens.at[x, high], down)
     up_high = wire.go(tokens.at[x, high], up)
     down_low = wire.go(tokens.at[x, low], down)
-
-    halos = [
-        [
-            pltpu.make_async_remote_copy(
-                src_ref=tokens.at[x, pl.ds(offset, HALO)],
-                dst_ref=edges.at[slot],
-                send_sem=halo_send.at[4 * slot + k],
-                recv_sem=halo_recv.at[slot],
-                device_id=dict(stretch_at(z, y, c, by), x=k),
-                device_id_type=MESH,
-            )
-            for k in range(4)
-        ]
-        for slot, (by, offset) in enumerate(((1, rows - HALO), (31, 0)))
-    ]
 
     def first(buffer, axis, keep=()):
         def at(n, part):
@@ -278,80 +301,94 @@
     v_first.start()
     s_first.start()
 
-    @pl.when(x == 3)
-    def _():
-        for copy in halos[0]:
-            copy.start()
-
-    @pl.when(x == 0)
-    def _():
-        for copy in halos[1]:
-            copy.start()
-
-    wo_x = Ring(
-        wire,
-        "x",
-        x,
-        lambda at: wo.at[z, y, c, at],
-        lambda at: wo.at[z, y, c, at, pl.ds(0, 32)],
-        lambda at: wo.at[z, y, c, at, pl.ds(32, 32)],
-    )
-    wo_x.start()
-
     def main_row(shard):
         return HALO + shard * rows
 
     def normalize(ref, size, to):
+        width = ref.shape[-1]
+
         @pl.loop(0, size // 16)
         def _(k):
-            start = pl.multiple_of(k * 16, 16)
-            cells = ref[pl.ds(start, 16), :].astype(jnp.float32)
-            scale = lax.rsqrt(jnp.mean(cells * cells, axis=-1, keepdims=True) + EPSILON)
-            normed[pl.ds(pl.multiple_of(to + start, 16), 16), :] = (
-                cells * scale * norm_gain_ref[...]
-            ).astype(jnp.bfloat16)
-
-    def project(start, size):
-        taken = pl.ds(start, size)
+            taken = pl.ds(pl.multiple_of(k * 16, 16), 16)
+            cells = ref[taken, :].astype(jnp.float32)
+            total = cells[:, 0:128] * cells[:, 0:128]
+            for at in range(128, width, 128):
+                total = total + cells[:, at : at + 128] * cells[:, at : at + 128]
+            squares[taken, :] = total
+
+        level = lax.rsqrt(
+            jnp.sum(squares[0:size, :], axis=-1, keepdims=True) * (1.0 / width) + EPSILON
+        )
+        squares[0:size, :] = jnp.broadcast_to(level, (size, 128))
+
+        @pl.loop(0, size // 16)
+        def _(k):
+            taken = pl.ds(pl.multiple_of(k * 16, 16), 16)
+            scale = squares[taken, :]
+            cells = ref[taken, :].astype(jnp.float32)
+            placed = pl.ds(pl.multiple_of(to + k * 16, 16), 16)
+            for at in range(0, width, 128):
+                normed[placed, at : at + 128] = (
+                    cells[:, at : at + 128] * scale * norm_gain_ref[:, at : at + 128]
+                ).astype(jnp.bfloat16)
+
+    shard_in = (x, step(x, 3), step(x, 1), step(x, 2))
+
+    def project(slots):
+        edge = not slots
+        begin, size = (slots[0] * rows, len(slots) * rows) if slots else (4 * rows, 2 * HALO)
+        taken = pl.ds(begin, size)
+
+        def put(values, columns):
+            for k, slot in enumerate(slots):
+                placed = pl.ds(pl.multiple_of(main_row(shard_in[slot]), 16), rows)
+                projected[placed, columns] = values[k * rows : (k + 1) * rows]
+            if edge:
+                projected[0:HALO, columns] = jnp.where(me > 0, values[0:HALO], 0).astype(
+                    values.dtype
+                )
+                projected[main_row(4) : main_row(4) + HALO, columns] = jnp.where(
+                    me < 31, values[HALO:], 0
+                ).astype(values.dtype)
+
+        for weights, total, start in ((wv, half, 0), (ws, 2 * lead, half)):
+
+            @pl.loop(0, total // 256)
+            def _(k):
+                columns = pl.ds(pl.multiple_of(k * 256, 256), 256)
+                put(
+                    dot(normed[taken, :], weights[:, :, :, :, columns].reshape(-1, 256)).astype(
+                        jnp.bfloat16
+                    ),
+                    pl.ds(pl.multiple_of(start + k * 256, 256), 256),
+                )
+
+        if edge:
+            return
+        values = dot(normed[taken, :], ws[:, :, :, :, 2 * lead :].reshape(-1, 128)).astype(
+            jnp.bfloat16
+        )
+        for k, slot in enumerate(slots):
+            placed = pl.ds(pl.multiple_of(shard_in[slot] * rows, rows), rows)
+            raw[placed, :] = values[k * rows : (k + 1) * rows]
+
+    def project_gate(slots):
+        taken = pl.ds(slots[0] * rows, len(slots) * rows)
 
         @pl.loop(0, half // 256)
         def _(k):
             columns = pl.ds(pl.multiple_of(k * 256, 256), 256)
-            projected[taken, columns] = dot(
-                normed[taken, :], wv[:, :, :, :, columns].reshape(-1, 256)
-            ).astype(jnp.bfloat16)
-
-        @pl.loop(0, 2 * lead // 256)
-        def _(k):
-            columns = pl.ds(pl.multiple_of(k * 256, 256), 256)
-            projected[taken, pl.ds(pl.multiple_of(half + k * 256, 256), 256)] = dot(
-                normed[taken, :], ws[:, :, :, :, columns].reshape(-1, 256)
-            ).astype(jnp.bfloat16)
-
-    def project_shard(shard):
-        project(pl.multiple_of(main_row(shard), 16), rows)
-        raw[pl.ds(pl.multiple_of(shard * rows, rows), rows), :] = dot(
-            normed[pl.ds(pl.multiple_of(main_row(shard), 16), rows), :],
-            ws[:, :, :, :, 2 * lead :].reshape(-1, 128),
-        ).astype(jnp.bfloat16)
-
-    def project_gate(shard):
-        @pl.loop(0, half // 256)
-        def _(k):
-            columns = pl.ds(pl.multiple_of(k * 256, 256), 256)
-            gates[pl.ds(pl.multiple_of(shard * rows, rows), rows), columns] = silu(
-                dot(
-                    normed[pl.ds(pl.multiple_of(main_row(shard), 16), rows), :],
-                    wg[:, :, :, :, columns].reshape(-1, 256),
-                )
-                .astype(jnp.bfloat16)
-                .astype(jnp.float32)
-            ).astype(jnp.bfloat16)
-
-    normalize(tokens.at[x], rows, main_row(x))
+            values = dot(normed[taken, :], wg[:, :, :, :, columns].reshape(-1, 256))
+            values = silu(values.astype(jnp.bfloat16).astype(jnp.float32)).astype(jnp.bfloat16)
+            for k, slot in enumerate(slots):
+                placed = pl.ds(pl.multiple_of(shard_in[slot] * rows, rows), rows)
+                gates[placed, columns] = values[k * rows : (k + 1) * rows]
+
+    normalize(tokens.at[x], rows, 0)
 
     v_first.forward()
     s_first.forward()
+    wo_x.forward()
     v_first.finish()
     v_second = second(wv, "z")
     v_second.start()
@@ -363,17 +400,19 @@
     g_first = first(wg, "z")
     g_first.start()
 
-    for slot in range(2):
-        halos[slot][0].wait_recv()
-    normalize(edges.at[0], HALO, 0)
-    normalize(edges.at[1], HALO, main_row(4))
-
     up_low.wait_recv()
-    far_low = wire.go(tokens.at[step(x, 3), low], up)
     down_high.wait_recv()
-    far_high = wire.go(tokens.at[step(x, 1), high], down)
-    normalize(tokens.at[step(x, 3), low], middle, main_row(step(x, 3)))
-    normalize(tokens.at[step(x, 1), high], middle, main_row(step(x, 1)) + middle)
+    far = [
+        wire.go(tokens.at[step(x, by), pl.ds(*some)], to)
+        for by, some, to in (
+            (3, (0, HALO), up),
+            (1, (rows - HALO, HALO), down),
+            (3, (HALO, middle - HALO), up),
+            (1, (middle, middle - HALO), down),
+        )
+    ]
+    normalize(tokens.at[step(x, 3), low], middle, rows)
+    normalize(tokens.at[step(x, 1), high], middle, 2 * rows + middle)
 
     v_second.forward()
     s_second.forward()
@@ -391,49 +430,47 @@
     across("g", wg, "y", 0)
     for copy in pairs["v"] + pairs["s"]:
         copy.wait_recv()
-    project_shard(x)
+    project((0,))
 
     up_high.wait_recv()
     down_low.wait_recv()
-    wo_x.forward()
-    normalize(tokens.at[step(x, 3), high], middle, main_row(step(x, 3)) + middle)
-    normalize(tokens.at[step(x, 1), low], middle, main_row(step(x, 1)))
     wo_x.finish()
+    normalize(tokens.at[step(x, 3), high], middle, rows + middle)
+    normalize(tokens.at[step(x, 1), low], middle, 2 * rows)
     lo_first, hi_first = first(wo, "y", (0, 2)), first(wo, "z", (2, 2))
     lo_first.start()
     hi_first.start()
-    project_shard(step(x, 3))
+    far[0].wait_recv()
+    far[1].wait_recv()
+    edge_in = [
+        wire.go(
+            tokens.at[shard, pl.ds(offset, HALO)],
+            stretch_at(z, y, c, by),
+            edges.at[pl.ds(slot * HALO, HALO)],
+        )
+        for slot, (shard, offset, by) in enumerate(((3, rows - HALO, 1), (0, 0, 31)))
+    ]
+    project((1, 2))
     g_second.forward()
     across("g", wg, "y", 3)
     across("g", wg, "y", 1)
-    project_shard(step(x, 1))
-
-    @pl.when(me > 0)
-    def _():
-        project(0, HALO)
-
-    @pl.when(me == 0)
-    def _():
-        projected[0:HALO, :] = jnp.zeros((HALO, wide), jnp.bfloat16)
-
-    @pl.when(me < 31)
-    def _():
-        project(main_row(4), HALO)
-
-    @pl.when(me == 31)
-    def _():
-        projected[main_row(4) :, :] = jnp.zeros((HALO, wide), jnp.bfloat16)
-
     lo_first.forward()
     hi_first.forward()
+    for copy in edge_in:
+        copy.wait_recv()
+    normalize(edges, 2 * HALO, 4 * rows)
+    project(())
 
     row, col = iota((BLOCK, BLOCK), 0), iota((BLOCK, BLOCK), 1)
     lower = row >= col
-    triangle = jnp.where(lower, 1.0, 0.0)
-    spread = jnp.where(
-        iota((128, wide), 1) // HEAD_DIM == iota((128, wide), 0), 1.0, 0.0
-    ).astype(jnp.bfloat16)
-    forward_lane = iota((BLOCK, 128), 1) < heads
+    triangle = jnp.where(row <= col, 1.0, 0.0)
+    forward_row = iota((2 * heads, BLOCK), 0) < heads
+
+    def spread(kind):
+        place_of = iota((128, wide), 1) // HEAD_DIM + 2 * heads * kind
+        return jnp.where(place_of == iota((128, wide), 0), 1.0, 0.0)
+
+    spread_weight = spread(2).astype(jnp.bfloat16)
 
     def rows_of(k):
         return pl.ds(pl.multiple_of(k * BLOCK, BLOCK), BLOCK)
@@ -449,36 +486,39 @@
                 tap_ref, target, begin = tap_out_ref, outward, at - half - lead
             cells = projected[window, at : at + 128].astype(jnp.float32)
             tap = tap_ref[:, begin : begin + 128]
+            here = slice(HALO, HALO + BLOCK)
             total = (
-                tap[0:1] * pltpu.roll(cells, 1, 0)
-                + tap[1:2] * cells
-                + tap[2:3] * pltpu.roll(cells, BLOCK + 2 * HALO - 1, 0)
-            )[HALO : HALO + BLOCK]
+                tap[0:1] * pltpu.roll(cells, 1, 0)[here]
+                + tap[1:2] * cells[here]
+                + tap[2:3] * pltpu.roll(cells, BLOCK + 2 * HALO - 1, 0)[here]
+            )
             target[rows_of(k), begin : begin + 128] = silu(total).astype(jnp.bfloat16)
 
         size = jax.nn.softplus(
-            raw[rows_of(k), :].astype(jnp.float32) + heads_ref[0:1, :] - shift
-        )
-        logs = size * heads_ref[1:2, :]
-        through = dot(triangle, logs, lax.Precision.HIGHEST)
+            raw[rows_of(k), :].astype(jnp.float32).T[0 : 2 * heads] + heads_ref[:, 0:1] - shift
+        )
+        logs = size * heads_ref[:, 1:2]
+        through = dot(logs, triangle, lax.Precision.HIGHEST)
         until = through - logs
-        whole = through[BLOCK - 1 : BLOCK, :]
+        whole = through[:, BLOCK - 1 : BLOCK]
         logsize = jnp.log(size)
-        column[rows_of(k), :] = jnp.where(forward_lane, through, -until) * LOG2E
-        turned = (jnp.where(forward_lane, logsize - through, logsize + until) * LOG2E).T
-        sizes = size.T
-        rowwise[k, 0 : 2 * heads, :] = turned[0 : 2 * heads]
-        rowwise[k, 2 * heads : 3 * heads, :] = sizes[0:heads] + sizes[heads : 2 * heads]
-        reading[rows_of(k), :] = jnp.exp(
-            jnp.where(forward_lane, through, whole - until)
-        ).astype(jnp.bfloat16)
-        weight = size * jnp.exp(jnp.where(forward_lane, whole - through, until))
-        decays[k] = dot(
-            jnp.broadcast_to(jnp.exp(whole), (8, 128)),
-            spread.astype(jnp.float32),
-            lax.Precision.HIGHEST,
-        )
-        weights = dot(weight.astype(jnp.bfloat16), spread)
+        rowwise[k, 0 : 2 * heads, :] = (
+            jnp.where(forward_row, logsize - through, logsize + until) * LOG2E
+        )
+        rowwise[k, 2 * heads : 3 * heads, :] = size[0:heads] + size[heads : 2 * heads]
+        turned = jnp.concatenate(
+            [
+                jnp.where(forward_row, through, -until) * LOG2E,
+                jnp.exp(jnp.where(forward_row, through, whole - until)),
+                size * jnp.exp(jnp.where(forward_row, whole - through, until)),
+                jnp.broadcast_to(jnp.exp(whole), (2 * heads, BLOCK)),
+                jnp.zeros((128 - 8 * heads, BLOCK), jnp.float32),
+            ],
+            axis=0,
+        ).T
+        column[rows_of(k), :] = turned
+        fades[k] = turned[0:8]
+        weights = dot(turned.astype(jnp.bfloat16), spread_weight)
         for way in range(2):
             for g in range(groups):
                 lanes = slice(g * span, (g + 1) * span)
@@ -490,11 +530,11 @@
                     inward[rows_of(k), g * STATE : (g + 1) * STATE], content
                 )
 
-    far = 2 * step(x, 2)
+    away = 2 * step(x, 2)
 
     @pl.loop(0, 4)
     def _(k):
-        prepare(lax.rem(far + 3 + k, blocks))
+        prepare(lax.rem(away + 3 + k, blocks))
 
     lo_first.finish()
     lo_second = second(wo, "z", (0, 2))
@@ -509,18 +549,24 @@
     across("g", wg, "y", 2)
     for copy in pairs["g"]:
         copy.wait_recv()
-    project_gate(x)
-    project_gate(step(x, 3))
-    project_gate(step(x, 1))
-
-    far_low.wait_recv()
-    far_high.wait_recv()
-    normalize(tokens.at[step(x, 2)], rows, main_row(step(x, 2)))
-    project_shard(step(x, 2))
+    project_gate((0, 1, 2))
+
+    far[2].wait_recv()
+    far[3].wait_recv()
+    normalize(tokens.at[step(x, 2)], rows, 3 * rows)
+    project((3,))
 
     @pl.loop(0, 4)
     def _(k):
-        prepare(lax.rem(far + 7 + k, blocks))
+        prepare(lax.rem(away + 7 + k, blocks))
+
+    over = dot(
+        jnp.concatenate([fades[k, 0:1, :] for k in range(blocks)], axis=0),
+        spread(3),
+        lax.Precision.HIGHEST,
+    )
+    for k in range(blocks):
+        decays[k] = jnp.broadcast_to(over[k : k + 1], (8, wide))
 
     @pl.loop(0, wide // 128)
     def _(j):
@@ -602,7 +648,7 @@
                 jnp.concatenate(weights, axis=1), jnp.concatenate(content, axis=0)
             )
 
-    project_gate(step(x, 2))
+    project_gate((3,))
 
     @pl.loop(0, blocks // 2)
     def _(k):
@@ -647,8 +693,10 @@
             before[at, :, lanes] = state.astype(jnp.bfloat16)
             state = state * decays[at, 0:1, lanes] + states[at, :, lanes]
 
+    spread_read = spread(1).astype(jnp.bfloat16)
+
     def finish(k):
-        scale = dot(reading[rows_of(k), :], spread)
+        scale = dot(column[rows_of(k), :].astype(jnp.bfloat16), spread_read)
         for g in range(groups):
             lanes = slice(g * span, (g + 1) * span)
             read = outward[rows_of(k), g * STATE : (g + 1) * STATE]
@@ -690,17 +738,16 @@
         copy.wait_recv()
 
     def contribute(at, begin, end):
-        @pl.loop(0, 8)
+        @pl.loop(0, 4)
         def _(k):
-            columns = pl.ds(pl.multiple_of(k * 256, 256), 256)
-            weight = wo[k // 2, pl.ds(2 * lax.rem(k, 2), 2), :, at].reshape(256, -1)
-            total = dot_nt(shards[at], weight)
+            lines = pl.ds(pl.multiple_of(k * 512, 512), 512)
+            total = dot_nt(wo[k, :, :, at].reshape(512, -1), shards[at])
             if not begin:
-                total = total + summed[:, columns]
+                total = total + summed[lines, :]
             if end:
-                out_ref[:, columns] = total.astype(out_ref.dtype)
+                out_ref[:, lines] = total.T.astype(out_ref.dtype)
             else:
-                summed[:, columns] = total
+                summed[lines, :] = total
 
     contribute(x, True, False)
     near_up.wait_recv()
@@ -717,16 +764,6 @@
     def _(k):
         outgoing(totals, arrived, 0, k).wait_send()
         outgoing(onward, incoming, 1, k).wait_send()
-
-    @pl.when(x == 3)
-    def _():
-        for copy in halos[0]:
-            copy.wait_send()
-
-    @pl.when(x == 0)
-    def _():
-        for copy in halos[1]:
-            copy.wait_send()
 
 
 COPIES = 80
@@ -741,7 +778,8 @@
     w_state_out,
     w_step_forward,
     w_step_backward,
-    head_rows,
+    step_offset,
+    fading_speed,
     conv_value,
     conv_state_in,
     conv_state_out,
@@ -757,11 +795,23 @@
     return pl.pallas_call(
         functools.partial(mixer_kernel, math.log(4 * rows * lax.axis_size(SP))),
         out_shape=jax.ShapeDtypeStruct((rows, width), OUT_TYPE),
-        in_specs=[anywhere, vmem] + [anywhere] * 3 + [vmem] * 2 + [anywhere] * 2 + [vmem] * 5,
+        in_specs=[anywhere] * 15,
         out_specs=vmem,
         scratch_shapes=[
+            pltpu.VMEM((1, width), f32),
+            pltpu.VMEM(w_step_forward.shape[::-1], bf16),
+            pltpu.VMEM(w_step_backward.shape[::-1], bf16),
+            pltpu.VMEM(conv_value.shape, f32),
+            pltpu.VMEM(conv_state_in.shape, f32),
+            pltpu.VMEM(conv_state_out.shape, f32),
+            pltpu.VMEM(step_offset.shape, f32),
+            pltpu.VMEM(fading_speed.shape, f32),
+            pltpu.VMEM((1, half), f32),
+            pltpu.VMEM((16, 128), f32),
+            pltpu.VMEM((rows, 128), f32),
+            pltpu.VMEM((blocks, 8, 128), f32),
             pltpu.VMEM((4, rows, width), bf16),
-            pltpu.VMEM((2, HALO, width), bf16),
+            pltpu.VMEM((2 * HALO, width), bf16),
             pltpu.VMEM((4 * rows + 2 * HALO, width), bf16),
             pltpu.VMEM((4, 4, 2, depth, half), bf16),
             pltpu.VMEM((4, 4, 2, depth, 2 * states + 128), bf16),
@@ -775,7 +825,6 @@
             pltpu.VMEM((4 * rows, states), bf16),
             pltpu.VMEM((4 * rows, 128), f32),
             pltpu.VMEM((blocks, 24, 128), f32),
-            pltpu.VMEM((4 * rows, 128), bf16),
             pltpu.VMEM((blocks, STATE, 2 * half), f32),
             pltpu.VMEM((blocks, 8, 2 * half), f32),
             pltpu.VMEM((blocks, STATE, 2 * half), bf16),
@@ -787,14 +836,12 @@
             pltpu.VMEM((4 * rows, half), bf16),
             pltpu.VMEM((4, rows, half), bf16),
             pltpu.VMEM((2, rows // 2, half), bf16),
-            pltpu.VMEM((rows, width), f32),
+            pltpu.VMEM((width, rows), f32),
             pltpu.SemaphoreType.DMA((COPIES,)),
             pltpu.SemaphoreType.DMA((COPIES,)),
-            pltpu.SemaphoreType.DMA((8,)),
-            pltpu.SemaphoreType.DMA((2,)),
             pltpu.SemaphoreType.DMA((2, 32)),
             pltpu.SemaphoreType.DMA((2, 32)),
-            pltpu.SemaphoreType.DMA((6,)),
+            pltpu.SemaphoreType.DMA((15,)),
         ],
         compiler_params=pltpu.CompilerParams(
             collective_id=0, has_side_effects=True, vmem_limit_bytes=60 * 2**20
@@ -802,18 +849,19 @@
         name="mixer",
     )(
         tokens,
-        norm_gain.reshape(1, -1),
         w_value,
         w_state_in,
         w_state_out,
+        w_gate,
+        w_out.T,
+        norm_gain.reshape(1, -1),
         w_step_forward.T,
         w_step_backward.T,
-        w_gate,
-        w_out.T,
         conv_value,
         conv_state_in,
         conv_state_out,
-        head_rows,
+        step_offset,
+        fading_speed,
         out_gain.reshape(1, -1),
     )
 
@@ -838,10 +886,6 @@
     out_gain,
     w_out,
 ):
-    head_rows = jnp.pad(
-        jnp.stack([step_offset.reshape(-1), -fading_speed.reshape(-1)]),
-        ((0, 0), (0, 128 - step_offset.size)),
-    )
     return mix(
         input_activations,
         norm_gain,
@@ -851,7 +895,8 @@
         w_state_out,
         w_step_forward,
         w_step_backward,
-        head_rows,
+        step_offset,
+        fading_speed,
         conv_value,
         conv_state_in,
         conv_state_out,

time: 122 us -> 98.8 us (0.81)
  Pallas kernels: 117 us -> 96.3 us
  local copies, waits for them, and re-layouts: 3.75 us -> 2.3 us
    pallas_call x1, Pallas kernels: 117 us -> 96.3 us  [mix(): pl.pallas_call(functools.partial(mixer_kernel, math.log(4 * rows * lax.ax...]
    unnamed x5 -> x1, local copies, waits for them, and re-layouts: 3.58 us -> 2.3 us
where the time goes in v3:
time: 98.8 us; the launch traced here: 98.6 us
  Pallas kernels  96.3 us (97%)
  local copies, waits for them, and re-layouts  2.3 us (2%)
    pallas_call x1, Pallas kernels, mix(): pl.pallas_call(functools.partial(mixer_kernel, math.log(4 * rows * lax.ax...  96.3 us
    unnamed x1, local copies, waits for them, and re-layouts  2.3 us

profile of v3, /device:TPU:1, one launch (start us, length us, event | category | flops | bytes accessed | tf_op | source)
XLA Modules:
  0.0 98.6 jit_solution(7681071140986856650)
XLA Ops:
  0.0 96.3 %mixer.1 = bf16[256,2048]{1,0:T(8,128)(2,1)} custom-call(bf16[256,2048]{1,0:T(8,128)(2,1)} %tokens_hbm.1, bf16[64,512]{1,0:T(8,128)(2,1)} %value_hbm.1, bf16[64,256]{1,0:T(8,128)(2,1)} %state_in_hbm.1, bf16[64,256]{1,0:T(8,128)(2,1)} %state_out_hbm.1, bf16[64,512]{1,0:T(8,128)(2,1)} %gate_hbm.1, bf16[64,512]{1,0:T(8,128)(2,1)} %bitcast.5, ...), custom_call_target="tpu_custom_call" | custom-call | tf_op jit(solution)/shard_map/mixer/pallas_call | solution.py:795
  96.3 2.3 %copy.17 = bf16[256,2048]{1,0:T(8,128)(2,1)} copy(bf16[256,2048]{1,0:T(8,128)(2,1)} %mixer.1) | data formatting | bytes 2097152

commit v4 on v3

--- a/solution.py
+++ b/solution.py
@@ -16,6 +16,7 @@
 SP_TP = ("z", "y", "c", "x")
 EPSILON = 1e-06
 MESH = pl.DeviceIdType.MESH
+VALUE, INWARD, OUTWARD, STEPS = range(4)
 HALO = 16
 
 
@@ -123,7 +124,7 @@
     offset_hbm,
     speed_hbm,
     gain_hbm,
-    out_ref,
+    out_hbm,
     norm_gain_ref,
     step_forward_ref,
     step_backward_ref,
@@ -136,6 +137,7 @@
     heads_ref,
     squares,
     fades,
+    out_ref,
     tokens,
     edges,
     normed,
@@ -258,8 +260,6 @@
     up, down = {"x": step(x, 1)}, {"x": step(x, 3)}
     up_low = wire.go(tokens.at[x, low], up)
     down_high = wire.go(tokens.at[x, high], down)
-    up_high = wire.go(tokens.at[x, high], up)
-    down_low = wire.go(tokens.at[x, low], down)
 
     def first(buffer, axis, keep=()):
         def at(n, part):
@@ -334,7 +334,7 @@
 
     shard_in = (x, step(x, 3), step(x, 1), step(x, 2))
 
-    def project(slots):
+    def project(slots, parts):
         edge = not slots
         begin, size = (slots[0] * rows, len(slots) * rows) if slots else (4 * rows, 2 * HALO)
         taken = pl.ds(begin, size)
@@ -351,26 +351,29 @@
                     me < 31, values[HALO:], 0
                 ).astype(values.dtype)
 
-        for weights, total, start in ((wv, half, 0), (ws, 2 * lead, half)):
-
-            @pl.loop(0, total // 256)
+        def product(weights, columns):
+            return dot(normed[taken, :], weights[:, :, :, :, columns].reshape(-1, 256)).astype(
+                jnp.bfloat16
+            )
+
+        if VALUE in parts:
+
+            @pl.loop(0, half // 256)
             def _(k):
                 columns = pl.ds(pl.multiple_of(k * 256, 256), 256)
-                put(
-                    dot(normed[taken, :], weights[:, :, :, :, columns].reshape(-1, 256)).astype(
-                        jnp.bfloat16
-                    ),
-                    pl.ds(pl.multiple_of(start + k * 256, 256), 256),
-                )
-
-        if edge:
-            return
-        values = dot(normed[taken, :], ws[:, :, :, :, 2 * lead :].reshape(-1, 128)).astype(
-            jnp.bfloat16
-        )
-        for k, slot in enumerate(slots):
-            placed = pl.ds(pl.multiple_of(shard_in[slot] * rows, rows), rows)
-            raw[placed, :] = values[k * rows : (k + 1) * rows]
+                put(product(wv, columns), columns)
+
+        if INWARD in parts:
+            put(product(ws, slice(0, lead)), slice(half, half + lead))
+        if OUTWARD in parts:
+            put(product(ws, slice(lead, 2 * lead)), slice(half + lead, wide))
+        if STEPS in parts:
+            values = dot(normed[taken, :], ws[:, :, :, :, 2 * lead :].reshape(-1, 128)).astype(
+                jnp.bfloat16
+            )
+            for k, slot in enumerate(slots):
+                placed = pl.ds(pl.multiple_of(shard_in[slot] * rows, rows), rows)
+                raw[placed, :] = values[k * rows : (k + 1) * rows]
 
     def project_gate(slots):
         taken = pl.ds(slots[0] * rows, len(slots) * rows)
@@ -387,8 +390,10 @@
     normalize(tokens.at[x], rows, 0)
 
     v_first.forward()
+    wo_x.forward()
+    up_high = wire.go(tokens.at[x, high], up)
+    down_low = wire.go(tokens.at[x, low], down)
     s_first.forward()
-    wo_x.forward()
     v_first.finish()
     v_second = second(wv, "z")
     v_second.start()
@@ -411,6 +416,10 @@
             (1, (middle, middle - HALO), down),
         )
     ]
+    wo_x.finish()
+    lo_first, hi_first = first(wo, "y", (0, 2)), first(wo, "z", (2, 2))
+    lo_first.start()
+    hi_first.start()
     normalize(tokens.at[step(x, 3), low], middle, rows)
     normalize(tokens.at[step(x, 1), high], middle, 2 * rows + middle)
 
@@ -428,18 +437,16 @@
     g_second = second(wg, "y")
     g_second.start()
     across("g", wg, "y", 0)
+    lo_first.forward()
+    hi_first.forward()
     for copy in pairs["v"] + pairs["s"]:
         copy.wait_recv()
-    project((0,))
+    project((0,), (VALUE, INWARD, OUTWARD, STEPS))
 
     up_high.wait_recv()
     down_low.wait_recv()
-    wo_x.finish()
     normalize(tokens.at[step(x, 3), high], middle, rows + middle)
     normalize(tokens.at[step(x, 1), low], middle, 2 * rows)
-    lo_first, hi_first = first(wo, "y", (0, 2)), first(wo, "z", (2, 2))
-    lo_first.start()
-    hi_first.start()
     far[0].wait_recv()
     far[1].wait_recv()
     edge_in = [
@@ -450,92 +457,6 @@
         )
         for slot, (shard, offset, by) in enumerate(((3, rows - HALO, 1), (0, 0, 31)))
     ]
-    project((1, 2))
-    g_second.forward()
-    across("g", wg, "y", 3)
-    across("g", wg, "y", 1)
-    lo_first.forward()
-    hi_first.forward()
-    for copy in edge_in:
-        copy.wait_recv()
-    normalize(edges, 2 * HALO, 4 * rows)
-    project(())
-
-    row, col = iota((BLOCK, BLOCK), 0), iota((BLOCK, BLOCK), 1)
-    lower = row >= col
-    triangle = jnp.where(row <= col, 1.0, 0.0)
-    forward_row = iota((2 * heads, BLOCK), 0) < heads
-
-    def spread(kind):
-        place_of = iota((128, wide), 1) // HEAD_DIM + 2 * heads * kind
-        return jnp.where(place_of == iota((128, wide), 0), 1.0, 0.0)
-
-    spread_weight = spread(2).astype(jnp.bfloat16)
-
-    def rows_of(k):
-        return pl.ds(pl.multiple_of(k * BLOCK, BLOCK), BLOCK)
-
-    def prepare(k):
-        window = pl.ds(pl.multiple_of(k * BLOCK, BLOCK), BLOCK + 2 * HALO)
-        for at in range(0, wide, 128):
-            if at < half:
-                tap_ref, target, begin = tap_value_ref, signal, at
-            elif at < half + lead:
-                tap_ref, target, begin = tap_in_ref, inward, at - half
-            else:
-                tap_ref, target, begin = tap_out_ref, outward, at - half - lead
-            cells = projected[window, at : at + 128].astype(jnp.float32)
-            tap = tap_ref[:, begin : begin + 128]
-            here = slice(HALO, HALO + BLOCK)
-            total = (
-                tap[0:1] * pltpu.roll(cells, 1, 0)[here]
-                + tap[1:2] * cells[here]
-                + tap[2:3] * pltpu.roll(cells, BLOCK + 2 * HALO - 1, 0)[here]
-            )
-            target[rows_of(k), begin : begin + 128] = silu(total).astype(jnp.bfloat16)
-
-        size = jax.nn.softplus(
-            raw[rows_of(k), :].astype(jnp.float32).T[0 : 2 * heads] + heads_ref[:, 0:1] - shift
-        )
-        logs = size * heads_ref[:, 1:2]
-        through = dot(logs, triangle, lax.Precision.HIGHEST)
-        until = through - logs
-        whole = through[:, BLOCK - 1 : BLOCK]
-        logsize = jnp.log(size)
-        rowwise[k, 0 : 2 * heads, :] = (
-            jnp.where(forward_row, logsize - through, logsize + until) * LOG2E
-        )
-        rowwise[k, 2 * heads : 3 * heads, :] = size[0:heads] + size[heads : 2 * heads]
-        turned = jnp.concatenate(
-            [
-                jnp.where(forward_row, through, -until) * LOG2E,
-                jnp.exp(jnp.where(forward_row, through, whole - until)),
-                size * jnp.exp(jnp.where(forward_row, whole - through, until)),
-                jnp.broadcast_to(jnp.exp(whole), (2 * heads, BLOCK)),
-                jnp.zeros((128 - 8 * heads, BLOCK), jnp.float32),
-            ],
-            axis=0,
-        ).T
-        column[rows_of(k), :] = turned
-        fades[k] = turned[0:8]
-        weights = dot(turned.astype(jnp.bfloat16), spread_weight)
-        for way in range(2):
-            for g in range(groups):
-                lanes = slice(g * span, (g + 1) * span)
-                placed = slice(way * half + g * span, way * half + (g + 1) * span)
-                content = (
-                    signal[rows_of(k), lanes].astype(jnp.float32) * weights[:, placed]
-                ).astype(jnp.bfloat16)
-                states[k, :, placed] = dot_tn(
-                    inward[rows_of(k), g * STATE : (g + 1) * STATE], content
-                )
-
-    away = 2 * step(x, 2)
-
-    @pl.loop(0, 4)
-    def _(k):
-        prepare(lax.rem(away + 3 + k, blocks))
-
     lo_first.finish()
     lo_second = second(wo, "z", (0, 2))
     lo_second.start()
@@ -544,21 +465,124 @@
     hi_second = second(wo, "y", (2, 2))
     hi_second.start()
     across("o", wo, "y", 0, (2, 2))
-
-    g_second.finish()
-    across("g", wg, "y", 2)
-    for copy in pairs["g"]:
+    project((1, 2), (VALUE, INWARD, OUTWARD, STEPS))
+    g_second.forward()
+    across("g", wg, "y", 3)
+    across("g", wg, "y", 1)
+    for copy in edge_in:
         copy.wait_recv()
-    project_gate((0, 1, 2))
+    normalize(edges, 2 * HALO, 4 * rows)
+    project((), (VALUE, INWARD, OUTWARD))
+
+    row, col = iota((BLOCK, BLOCK), 0), iota((BLOCK, BLOCK), 1)
+    lower = row >= col
+    triangle = jnp.where(row <= col, 1.0, 0.0)
+
+    def spread(kind):
+        place_of = iota((128, wide), 1) // HEAD_DIM + 2 * heads * kind
+        return jnp.where(place_of == iota((128, wide), 0), 1.0, 0.0)
+
+    spread_weight = spread(2).astype(jnp.bfloat16)
+
+    def rows_of(k):
+        return pl.ds(pl.multiple_of(k * BLOCK, BLOCK), BLOCK)
+
+    def filtered(k, begin, end):
+        window = pl.ds(pl.multiple_of(k * BLOCK, BLOCK), BLOCK + 2 * HALO)
+        for at in range(begin, end, 128):
+            if at < half:
+                tap_ref, target, start = tap_value_ref, signal, at
+            elif at < half + lead:
+                tap_ref, target, start = tap_in_ref, inward, at - half
+            else:
+                tap_ref, target, start = tap_out_ref, outward, at - half - lead
+            cells = projected[window, at : at + 128].astype(jnp.float32)
+            tap = tap_ref[:, start : start + 128]
+            here = slice(HALO, HALO + BLOCK)
+            total = (
+                tap[0:1] * pltpu.roll(cells, 1, 0)[here]
+                + tap[1:2] * cells[here]
+                + tap[2:3] * pltpu.roll(cells, BLOCK + 2 * HALO - 1, 0)[here]
+            )
+            target[rows_of(k), start : start + 128] = silu(total).astype(jnp.bfloat16)
+
+    def prepare(first_block):
+        some = [lax.rem(first_block + n, blocks) for n in range(4)]
+        both = 2 * heads
+        forward_row = lax.rem(iota((4 * both, BLOCK), 0), both) < heads
+        size = jax.nn.softplus(
+            jnp.concatenate(
+                [raw[rows_of(k), :].astype(jnp.float32).T[0:both] for k in some], axis=0
+            )
+            + jnp.concatenate([heads_ref[:, 0:1]] * 4, axis=0)
+            - shift
+        )
+        logs = size * jnp.concatenate([heads_ref[:, 1:2]] * 4, axis=0)
+        through = dot(logs, triangle, lax.Precision.HIGHEST)
+        until = through - logs
+        whole = through[:, BLOCK - 1 : BLOCK]
+        logsize = jnp.log(size)
+        lines = jnp.where(forward_row, logsize - through, logsize + until) * LOG2E
+        kinds = (
+            jnp.where(forward_row, through, -until) * LOG2E,
+            jnp.exp(jnp.where(forward_row, through, whole - until)),
+            size * jnp.exp(jnp.where(forward_row, whole - through, until)),
+            jnp.broadcast_to(jnp.exp(whole), (4 * both, BLOCK)),
+        )
+        turned = []
+        for n, k in enumerate(some):
+            own_rows = slice(n * both, (n + 1) * both)
+            rowwise[k, 0:both, :] = lines[own_rows]
+            rowwise[k, both : both + heads, :] = (
+                size[n * both : n * both + heads] + size[n * both + heads : (n + 1) * both]
+            )
+            block = jnp.concatenate(
+                [kind[own_rows] for kind in kinds]
+                + [jnp.zeros((128 - 4 * both, BLOCK), jnp.float32)],
+                axis=0,
+            ).T
+            column[rows_of(k), :] = block
+            fades[k] = block[0:8]
+            turned.append(block.astype(jnp.bfloat16))
+        turned = jnp.concatenate(turned, axis=0)
+        for g in range(groups):
+            across_in = [
+                inward[rows_of(k), g * STATE : (g + 1) * STATE].astype(jnp.float32).T.astype(
+                    jnp.bfloat16
+                )
+                for k in some
+            ]
+            cells = jnp.concatenate(
+                [signal[rows_of(k), g * span : (g + 1) * span] for k in some], axis=0
+            )
+            for way in range(2):
+                placed = slice(way * half + g * span, way * half + (g + 1) * span)
+                content = (
+                    cells.astype(jnp.float32) * dot(turned, spread_weight[:, placed])
+                ).astype(jnp.bfloat16)
+                for n, k in enumerate(some):
+                    states[k, :, placed] = dot(
+                        across_in[n], content[n * BLOCK : (n + 1) * BLOCK]
+                    )
+
+    away = 2 * step(x, 2)
+
+    @pl.loop(0, 4)
+    def _(k):
+        filtered(lax.rem(away + 3 + k, blocks), 0, wide)
+
+    prepare(away + 3)
 
     far[2].wait_recv()
     far[3].wait_recv()
     normalize(tokens.at[step(x, 2)], rows, 3 * rows)
-    project((3,))
+    project((3,), (VALUE, INWARD, STEPS))
 
     @pl.loop(0, 4)
     def _(k):
-        prepare(lax.rem(away + 7 + k, blocks))
+        filtered(lax.rem(away + 7 + k, blocks), 0, half + lead)
+
+    prepare(away + 7)
 
     over = dot(
         jnp.concatenate([fades[k, 0:1, :] for k in range(blocks)], axis=0),
@@ -616,11 +640,8 @@
 
     arrived[me] = totals[me]
 
-    lo_second.forward()
-    hi_second.forward()
-    for by in (3, 1):
-        across("o", wo, "z", by, (0, 2))
-        across("o", wo, "y", by, (2, 2))
+    g_second.finish()
+    across("g", wg, "y", 2)
 
     def within(k):
         for g in range(groups):
@@ -648,6 +669,21 @@
                 jnp.concatenate(weights, axis=1), jnp.concatenate(content, axis=0)
             )
 
+    lo_second.forward()
+    hi_second.forward()
+    for by in (3, 1):
+        across("o", wo, "z", by, (0, 2))
+        across("o", wo, "y", by, (2, 2))
+
+    project((3,), (OUTWARD,))
+
+    @pl.loop(0, 4)
+    def _(k):
+        filtered(lax.rem(away + 7 + k, blocks), half + lead, wide)
+
+    for copy in pairs["g"]:
+        copy.wait_recv()
+    project_gate((0, 1, 2))
     project_gate((3,))
 
     @pl.loop(0, blocks // 2)
@@ -737,6 +773,10 @@
     for copy in pairs["o"]:
         copy.wait_recv()
 
+    def leaving(k):
+        lines = pl.ds(pl.multiple_of(k * 512, 512), 512)
+        return pltpu.make_async_copy(out_ref.at[:, lines], out_hbm.at[:, lines], local_sem.at[k])
+
     def contribute(at, begin, end):
         @pl.loop(0, 4)
         def _(k):
@@ -746,6 +786,7 @@
                 total = total + summed[lines, :]
             if end:
                 out_ref[:, lines] = total.T.astype(out_ref.dtype)
+                leaving(k).start()
             else:
                 summed[lines, :] = total
 
@@ -764,6 +805,10 @@
     def _(k):
         outgoing(totals, arrived, 0, k).wait_send()
         outgoing(onward, incoming, 1, k).wait_send()
+
+    @pl.loop(0, 4)
+    def _(k):
+        leaving(k).wait()
 
 
 COPIES = 80
@@ -790,13 +835,13 @@
     depth, half = w_value.shape
     states = w_state_in.shape[1]
     blocks = 4 * rows // BLOCK
-    vmem, anywhere = pl.BlockSpec(memory_space=pltpu.VMEM), pl.BlockSpec(memory_space=pl.ANY)
+    anywhere = pl.BlockSpec(memory_space=pl.ANY)
     bf16, f32 = jnp.bfloat16, jnp.float32
     return pl.pallas_call(
         functools.partial(mixer_kernel, math.log(4 * rows * lax.axis_size(SP))),
         out_shape=jax.ShapeDtypeStruct((rows, width), OUT_TYPE),
         in_specs=[anywhere] * 15,
-        out_specs=vmem,
+        out_specs=pl.BlockSpec(memory_space=pltpu.HBM),
         scratch_shapes=[
             pltpu.VMEM((1, width), f32),
             pltpu.VMEM(w_step_forward.shape[::-1], bf16),
@@ -810,6 +855,7 @@
             pltpu.VMEM((16, 128), f32),
             pltpu.VMEM((rows, 128), f32),
             pltpu.VMEM((blocks, 8, 128), f32),
+            pltpu.VMEM((rows, width), OUT_TYPE),
             pltpu.VMEM((4, rows, width), bf16),
             pltpu.VMEM((2 * HALO, width), bf16),
             pltpu.VMEM((4 * rows + 2 * HALO, width), bf16),

time: 98.8 us -> 90.4 us (0.915)
  Pallas kernels: 96.3 us -> 87.9 us
    pallas_call x1, Pallas kernels: 96.3 us -> 87.9 us  [mix(): pl.pallas_call(functools.partial(mixer_kernel, math.log(4 * rows * lax.ax...]
where the time goes in v4:
time: 90.4 us; the launch traced here: 90.2 us
  Pallas kernels  87.9 us (97%)
  local copies, waits for them, and re-layouts  2.3 us (3%)
    pallas_call x1, Pallas kernels, mix(): pl.pallas_call(functools.partial(mixer_kernel, math.log(4 * rows * lax.ax...  87.9 us
    unnamed x1, local copies, waits for them, and re-layouts  2.3 us

profile of v4, /device:TPU:1, one launch (start us, length us, event | category | flops | bytes accessed | tf_op | source)
XLA Modules:
  0.0 90.2 jit_solution(10098288580587339706)
XLA Ops:
  0.0 87.9 %mixer.1 = bf16[256,2048]{1,0:T(8,128)(2,1)} custom-call(bf16[256,2048]{1,0:T(8,128)(2,1)} %tokens_hbm.1, bf16[64,512]{1,0:T(8,128)(2,1)} %value_hbm.1, bf16[64,256]{1,0:T(8,128)(2,1)} %state_in_hbm.1, bf16[64,256]{1,0:T(8,128)(2,1)} %state_out_hbm.1, bf16[64,512]{1,0:T(8,128)(2,1)} %gate_hbm.1, bf16[64,512]{1,0:T(8,128)(2,1)} %bitcast.5, ...), custom_call_target="tpu_custom_call" | custom-call | tf_op jit(solution)/shard_map/mixer/pallas_call | solution.py:840
  87.9 2.3 %copy.17 = bf16[256,2048]{1,0:T(8,128)(2,1)} copy(bf16[256,2048]{1,0:T(8,128)(2,1)} %mixer.1) | data formatting | bytes 2097152

commit v5 on v4

--- a/solution.py
+++ b/solution.py
@@ -34,51 +34,60 @@
 
 
 class Wire:
-    def __init__(self, send, recv):
-        self.send, self.recv, self.count, self.sent = send, recv, 0, []
-
-    def describe(self, source, target, to):
-        k = self.count
+    def __init__(self, flags, self_free):
+        self.flags, self.count, self.to, self.sent = flags, 0, self_free, []
+
+    def flag(self):
         self.count += 1
-        return pltpu.make_async_remote_copy(
+        return self.flags.at[self.count - 1]
+
+    def go(self, source, to, send, recv, target=None):
+        pltpu.make_async_remote_copy(
             src_ref=source,
-            dst_ref=target,
-            send_sem=self.send.at[k],
-            recv_sem=self.recv.at[k],
+            dst_ref=source if target is None else target,
+            send_sem=send,
+            recv_sem=recv,
             device_id=to,
             device_id_type=MESH,
+        ).start()
+
+    def span(self, ref, flag):
+        return pltpu.make_async_remote_copy(
+            src_ref=ref,
+            dst_ref=ref,
+            send_sem=flag,
+            recv_sem=flag,
+            device_id=self.to,
+            device_id_type=MESH,
         )
 
-    def go(self, source, to, target=None):
-        copy = self.describe(source, source if target is None else target, to)
-        copy.start()
-        self.sent.append(copy)
-        return copy
+    def landed(self, ref, flag):
+        self.span(ref, flag).wait_recv()
 
     def drain(self):
-        for copy in self.sent:
-            copy.wait_send()
+        for ref, flag in self.sent:
+            self.span(ref, flag).wait_send()
 
 
 class Ring:
-    def __init__(self, wire, axis, at, block, low, high):
+    def __init__(self, wire, axis, at, block, low, high, many):
         self.wire, self.at = wire, at
         self.up, self.down = {axis: step(at, 1)}, {axis: step(at, 3)}
-        self.block, self.low, self.high = block, low, high
+        self.block, self.low, self.high, self.many = block, low, high, many
+        self.out, self.near, self.away = wire.flag(), wire.flag(), wire.flag()
+        wire.sent.append((many(3), self.out))
 
     def start(self):
-        self.a = self.wire.go(self.block(self.at), self.up)
-        self.b = self.wire.go(self.block(self.at), self.down)
+        self.wire.go(self.block(self.at), self.up, self.out, self.near)
+        self.wire.go(self.block(self.at), self.down, self.out, self.near)
 
     def forward(self):
-        self.a.wait_recv()
-        self.c = self.wire.go(self.low(step(self.at, 3)), self.up)
-        self.b.wait_recv()
-        self.d = self.wire.go(self.high(step(self.at, 1)), self.down)
+        self.wire.landed(self.many(2), self.near)
+        self.wire.go(self.low(step(self.at, 3)), self.up, self.out, self.away)
+        self.wire.go(self.high(step(self.at, 1)), self.down, self.out, self.away)
 
     def finish(self):
-        self.c.wait_recv()
-        self.d.wait_recv()
+        self.wire.landed(self.many(1), self.away)
 
 
 LOG2E = 1.4426950408889634
@@ -165,15 +174,12 @@
     shards,
     relay,
     summed,
-    send,
-    recv,
-    state_send,
-    state_recv,
+    flags,
     local_sem,
 ):
     z, y, c, x = place()
     me = z * 8 + y * 2 + c
-    wire = Wire(send, recv)
+    wire = Wire(flags, {"c": 1 - c})
     rows = tokens.shape[1]
     middle = rows // 2
     count = 4 * rows
@@ -253,13 +259,17 @@
         lambda at: wo.at[z, y, c, at],
         lambda at: wo.at[z, y, c, at, pl.ds(0, 32)],
         lambda at: wo.at[z, y, c, at, pl.ds(32, 32)],
+        lambda n: wo.at[z, y, c, pl.ds(0, n)],
     )
     wo_x.start()
 
     low, high = pl.ds(0, middle), pl.ds(middle, middle)
     up, down = {"x": step(x, 1)}, {"x": step(x, 3)}
-    up_low = wire.go(tokens.at[x, low], up)
-    down_high = wire.go(tokens.at[x, high], down)
+    tokens_out, first_half, second_half = wire.flag(), wire.flag(), wire.flag()
+    far_ends, far_rest = wire.flag(), wire.flag()
+    wire.sent.append((tokens.at[pl.ds(0, 3)], tokens_out))
+    wire.go(tokens.at[x, low], up, tokens_out, first_half)
+    wire.go(tokens.at[x, high], down, tokens_out, first_half)
 
     def first(buffer, axis, keep=()):
         def at(n, part):
@@ -270,8 +280,13 @@
             return buffer.at[spot] if part is None else buffer.at[(*spot, pl.ds(32 * part, 32))]
 
         here = y if axis == "y" else z
+
+        def many(n):
+            spot = (z, pl.ds(0, n), c) if axis == "y" else (pl.ds(0, n), y, c)
+            return buffer.at[(*spot, pl.ds(*keep))] if keep else buffer.at[spot]
+
         return Ring(
-            wire, axis, here, lambda n: at(n, None), lambda n: at(n, 0), lambda n: at(n, 1)
+            wire, axis, here, lambda n: at(n, None), lambda n: at(n, 0), lambda n: at(n, 1), many
         )
 
     def group(buffer, axis, n, part, keep):
@@ -288,14 +303,20 @@
             lambda n: group(buffer, axis, n, None, keep),
             lambda n: group(buffer, axis, n, 0, keep),
             lambda n: group(buffer, axis, n, 1, keep),
+            lambda n: group(buffer, axis, pl.ds(0, n), None, keep),
         )
 
     pairs = {}
+    for name, buffer in (("v", wv), ("s", ws), ("g", wg), ("o", wo)):
+        pairs[name] = wire.flag(), wire.flag()
+        wire.sent.append((buffer.at[:, :, 1 - c], pairs[name][0]))
 
     def across(name, buffer, axis, by, keep=()):
         here = y if axis == "y" else z
-        copy = wire.go(group(buffer, axis, step(here, by), None, keep), partner)
-        pairs.setdefault(name, []).append(copy)
+        wire.go(group(buffer, axis, step(here, by), None, keep), partner, *pairs[name])
+
+    def crossed(name, buffer):
+        wire.landed(buffer.at[:, :, 1 - c], pairs[name][1])
 
     v_first, s_first = first(wv, "y"), first(ws, "z")
     v_first.start()
@@ -391,8 +412,8 @@
 
     v_first.forward()
     wo_x.forward()
-    up_high = wire.go(tokens.at[x, high], up)
-    down_low = wire.go(tokens.at[x, low], down)
+    wire.go(tokens.at[x, high], up, tokens_out, second_half)
+    wire.go(tokens.at[x, low], down, tokens_out, second_half)
     s_first.forward()
     v_first.finish()
     v_second = second(wv, "z")
@@ -405,17 +426,14 @@
     g_first = first(wg, "z")
     g_first.start()
 
-    up_low.wait_recv()
-    down_high.wait_recv()
-    far = [
-        wire.go(tokens.at[step(x, by), pl.ds(*some)], to)
-        for by, some, to in (
-            (3, (0, HALO), up),
-            (1, (rows - HALO, HALO), down),
-            (3, (HALO, middle - HALO), up),
-            (1, (middle, middle - HALO), down),
-        )
-    ]
+    wire.landed(tokens.at[0], first_half)
+    for by, start, to, flag in (
+        (3, (0, HALO), up, far_ends),
+        (1, (rows - HALO, HALO), down, far_ends),
+        (3, (HALO, middle - HALO), up, far_rest),
+        (1, (middle, middle - HALO), down, far_rest),
+    ):
+        wire.go(tokens.at[step(x, by), pl.ds(*start)], to, tokens_out, flag)
     wo_x.finish()
     lo_first, hi_first = first(wo, "y", (0, 2)), first(wo, "z", (2, 2))
     lo_first.start()
@@ -439,24 +457,24 @@
     across("g", wg, "y", 0)
     lo_first.forward()
     hi_first.forward()
-    for copy in pairs["v"] + pairs["s"]:
-        copy.wait_recv()
+    crossed("v", wv)
+    crossed("s", ws)
     project((0,), (VALUE, INWARD, OUTWARD, STEPS))
 
-    up_high.wait_recv()
-    down_low.wait_recv()
+    wire.landed(tokens.at[0], second_half)
     normalize(tokens.at[step(x, 3), high], middle, rows + middle)
     normalize(tokens.at[step(x, 1), low], middle, 2 * rows)
-    far[0].wait_recv()
-    far[1].wait_recv()
-    edge_in = [
+    wire.landed(edges, far_ends)
+    edge_out, edge_in = wire.flag(), wire.flag()
+    wire.sent.append((edges, edge_out))
+    for slot, (shard, offset, by) in enumerate(((3, rows - HALO, 1), (0, 0, 31))):
         wire.go(
             tokens.at[shard, pl.ds(offset, HALO)],
             stretch_at(z, y, c, by),
+            edge_out,
+            edge_in,
             edges.at[pl.ds(slot * HALO, HALO)],
         )
-        for slot, (shard, offset, by) in enumerate(((3, rows - HALO, 1), (0, 0, 31)))
-    ]
     lo_first.finish()
     lo_second = second(wo, "z", (0, 2))
     lo_second.start()
@@ -469,8 +487,7 @@
     g_second.forward()
     across("g", wg, "y", 3)
     across("g", wg, "y", 1)
-    for copy in edge_in:
-        copy.wait_recv()
+    wire.landed(edges, edge_in)
     normalize(edges, 2 * HALO, 4 * rows)
     project((), (VALUE, INWARD, OUTWARD))
 
@@ -573,8 +590,7 @@
 
     prepare(away + 3)
 
-    far[2].wait_recv()
-    far[3].wait_recv()
+    wire.landed(tokens.at[0, pl.ds(0, rows - 2 * HALO)], far_rest)
     normalize(tokens.at[step(x, 2)], rows, 3 * rows)
     project((3,), (VALUE, INWARD, STEPS))
 
@@ -612,31 +628,17 @@
             totals[4 * j + q, 0:32, :] = total[32 * q : 32 * q + 32].astype(jnp.bfloat16)
             totals[4 * j + q, 32:48, :] = tail.astype(jnp.bfloat16)
 
-    def outgoing(box, inbox, bank, k):
-        to = lax.rem(me + k, 32)
-        return pltpu.make_async_remote_copy(
-            src_ref=box.at[to],
-            dst_ref=inbox.at[me],
-            send_sem=state_send.at[bank, k],
-            recv_sem=state_recv.at[bank, me],
-            device_id=stretch(to),
-            device_id_type=MESH,
-        )
-
-    def expected(box, inbox, bank, k):
-        source = lax.rem(me + k, 32)
-        return pltpu.make_async_remote_copy(
-            src_ref=box.at[me],
-            dst_ref=inbox.at[source],
-            send_sem=state_send.at[bank, k],
-            recv_sem=state_recv.at[bank, source],
-            device_id=stretch(source),
-            device_id_type=MESH,
-        )
-
-    @pl.loop(1, 32)
-    def _(k):
-        outgoing(totals, arrived, 0, k).start()
+    state_flags = [wire.flag() for _ in range(4)]
+    wire.sent.append((totals.at[pl.ds(0, 31)], state_flags[0]))
+    wire.sent.append((onward.at[pl.ds(0, 31)], state_flags[2]))
+
+    def disperse(box, inbox, send, recv):
+        @pl.loop(0, 31)
+        def _(k):
+            to = lax.rem(me + lax.rem(k + 15, 31) + 1, 32)
+            wire.go(box.at[to], stretch(to), send, recv, inbox.at[me])
+
+    disperse(totals, arrived, *state_flags[:2])
 
     arrived[me] = totals[me]
 
@@ -681,18 +683,12 @@
     def _(k):
         filtered(lax.rem(away + 7 + k, blocks), half + lead, wide)
 
-    for copy in pairs["g"]:
-        copy.wait_recv()
-    project_gate((0, 1, 2))
-    project_gate((3,))
 
     @pl.loop(0, blocks // 2)
     def _(k):
         within(k)
 
-    @pl.loop(1, 32)
-    def _(k):
-        expected(totals, arrived, 0, k).wait_recv()
+    wire.landed(arrived.at[pl.ds(0, 31)], state_flags[1])
 
     flip = me >= 16
 
@@ -705,19 +701,19 @@
 
     lax.fori_loop(0, 32, hop, jnp.zeros((32, 128), jnp.float32))
 
-    @pl.loop(1, 32)
-    def _(k):
-        outgoing(onward, incoming, 1, k).start()
+    disperse(onward, incoming, *state_flags[2:])
 
     incoming[me] = onward[me]
+
+    crossed("g", wg)
+    project_gate((0, 1, 2))
+    project_gate((3,))
 
     @pl.loop(blocks // 2, blocks)
     def _(k):
         within(k)
 
-    @pl.loop(1, 32)
-    def _(k):
-        expected(onward, incoming, 1, k).wait_recv()
+    wire.landed(incoming.at[pl.ds(0, 31)], state_flags[3])
 
     @pl.loop(0, wide // 128)
     def _(j):
@@ -753,25 +749,26 @@
         start, size = some
         return mixed.at[pl.ds(pl.multiple_of(shard * rows + start, middle), size)]
 
-    finish_shard(step(x, 2))
-    relay_up = wire.go(part(step(x, 2), (0, middle)), up, relay.at[0])
-    relay_down = wire.go(part(step(x, 2), (middle, middle)), down, relay.at[1])
+    mixed_out, relayed, from_below, from_above, from_far = [wire.flag() for _ in range(5)]
+    wire.sent.append((shards, mixed_out))
+    finish(2 * step(x, 2))
+    wire.go(part(step(x, 2), (0, middle)), up, mixed_out, relayed, relay.at[0])
+    finish(2 * step(x, 2) + 1)
+    wire.go(part(step(x, 2), (middle, middle)), down, mixed_out, relayed, relay.at[1])
     finish_shard(step(x, 1))
-    near_up = wire.go(part(step(x, 1), (0, rows)), up, shards.at[x])
+    wire.go(part(step(x, 1), (0, rows)), up, mixed_out, from_below, shards.at[x])
     finish_shard(step(x, 3))
-    near_down = wire.go(part(step(x, 3), (0, rows)), down, shards.at[x])
+    wire.go(part(step(x, 3), (0, rows)), down, mixed_out, from_above, shards.at[x])
     lo_second.finish()
     across("o", wo, "z", 2, (0, 2))
     hi_second.finish()
     across("o", wo, "y", 2, (2, 2))
     finish_shard(x)
     shards[x] = mixed[pl.ds(pl.multiple_of(x * rows, rows), rows), :]
-    relay_up.wait_recv()
-    far_up = wire.go(relay.at[0], up, shards.at[step(x, 3), low])
-    relay_down.wait_recv()
-    far_down = wire.go(relay.at[1], down, shards.at[step(x, 1), high])
-    for copy in pairs["o"]:
-        copy.wait_recv()
+    wire.landed(relay, relayed)
+    wire.go(relay.at[0], up, mixed_out, from_far, shards.at[step(x, 3), low])
+    wire.go(relay.at[1], down, mixed_out, from_far, shards.at[step(x, 1), high])
+    crossed("o", wo)
 
     def leaving(k):
         lines = pl.ds(pl.multiple_of(k * 512, 512), 512)
@@ -791,27 +788,21 @@
                 summed[lines, :] = total
 
     contribute(x, True, False)
-    near_up.wait_recv()
+    wire.landed(shards.at[0], from_below)
     contribute(step(x, 3), False, False)
-    near_down.wait_recv()
+    wire.landed(shards.at[0], from_above)
     contribute(step(x, 1), False, False)
-    far_up.wait_recv()
-    far_down.wait_recv()
+    wire.landed(shards.at[0], from_far)
     contribute(step(x, 2), False, True)
 
     wire.drain()
-
-    @pl.loop(1, 32)
-    def _(k):
-        outgoing(totals, arrived, 0, k).wait_send()
-        outgoing(onward, incoming, 1, k).wait_send()
 
     @pl.loop(0, 4)
     def _(k):
         leaving(k).wait()
 
 
-COPIES = 80
+FLAGS = 57
 
 
 def mix(
@@ -883,10 +874,7 @@
             pltpu.VMEM((4, rows, half), bf16),
             pltpu.VMEM((2, rows // 2, half), bf16),
             pltpu.VMEM((width, rows), f32),
-            pltpu.SemaphoreType.DMA((COPIES,)),
-            pltpu.SemaphoreType.DMA((COPIES,)),
-            pltpu.SemaphoreType.DMA((2, 32)),
-            pltpu.SemaphoreType.DMA((2, 32)),
+            pltpu.SemaphoreType.DMA((FLAGS,)),
             pltpu.SemaphoreType.DMA((15,)),
         ],
         compiler_params=pltpu.CompilerParams(

time: 90.4 us -> 87.1 us (0.963)
  Pallas kernels: 87.9 us -> 84.6 us
    pallas_call x1, Pallas kernels: 87.9 us -> 84.6 us  [mix(): pl.pallas_call(functools.partial(mixer_kernel, math.log(4 * rows * lax.ax...]
where the time goes in v5:
time: 87.1 us; the launch traced here: 86.9 us
  Pallas kernels  84.6 us (97%)
  local copies, waits for them, and re-layouts  2.3 us (3%)
    pallas_call x1, Pallas kernels, mix(): pl.pallas_call(functools.partial(mixer_kernel, math.log(4 * rows * lax.ax...  84.6 us
    unnamed x1, local copies, waits for them, and re-layouts  2.3 us

profile of v5, /device:TPU:1, one launch (start us, length us, event | category | flops | bytes accessed | tf_op | source)
XLA Modules:
  0.0 86.9 jit_solution(8475769879470865210)
XLA Ops:
  0.0 84.6 %mixer.1 = bf16[256,2048]{1,0:T(8,128)(2,1)} custom-call(bf16[256,2048]{1,0:T(8,128)(2,1)} %tokens_hbm.1, bf16[64,512]{1,0:T(8,128)(2,1)} %value_hbm.1, bf16[64,256]{1,0:T(8,128)(2,1)} %state_in_hbm.1, bf16[64,256]{1,0:T(8,128)(2,1)} %state_out_hbm.1, bf16[64,512]{1,0:T(8,128)(2,1)} %gate_hbm.1, bf16[64,512]{1,0:T(8,128)(2,1)} %bitcast.5, ...), custom_call_target="tpu_custom_call" | custom-call | tf_op jit(solution)/shard_map/mixer/pallas_call | solution.py:831
  84.6 2.3 %copy.17 = bf16[256,2048]{1,0:T(8,128)(2,1)} copy(bf16[256,2048]{1,0:T(8,128)(2,1)} %mixer.1) | data formatting | bytes 2097152

commit v6 on v5

--- a/solution.py
+++ b/solution.py
@@ -133,7 +133,7 @@
     offset_hbm,
     speed_hbm,
     gain_hbm,
-    out_hbm,
+    out_ref,
     norm_gain_ref,
     step_forward_ref,
     step_backward_ref,
@@ -146,7 +146,6 @@
     heads_ref,
     squares,
     fades,
-    out_ref,
     tokens,
     edges,
     normed,
@@ -328,9 +327,9 @@
     def normalize(ref, size, to):
         width = ref.shape[-1]
 
-        @pl.loop(0, size // 16)
+        @pl.loop(0, size // 32, unroll=2)
         def _(k):
-            taken = pl.ds(pl.multiple_of(k * 16, 16), 16)
+            taken = pl.ds(pl.multiple_of(k * 32, 32), 32)
             cells = ref[taken, :].astype(jnp.float32)
             total = cells[:, 0:128] * cells[:, 0:128]
             for at in range(128, width, 128):
@@ -342,12 +341,12 @@
         )
         squares[0:size, :] = jnp.broadcast_to(level, (size, 128))
 
-        @pl.loop(0, size // 16)
+        @pl.loop(0, size // 32, unroll=2)
         def _(k):
-            taken = pl.ds(pl.multiple_of(k * 16, 16), 16)
+            taken = pl.ds(pl.multiple_of(k * 32, 32), 32)
             scale = squares[taken, :]
             cells = ref[taken, :].astype(jnp.float32)
-            placed = pl.ds(pl.multiple_of(to + k * 16, 16), 16)
+            placed = pl.ds(pl.multiple_of(to + k * 32, 16), 32)
             for at in range(0, width, 128):
                 normed[placed, at : at + 128] = (
                     cells[:, at : at + 128] * scale * norm_gain_ref[:, at : at + 128]
@@ -770,20 +769,15 @@
     wire.go(relay.at[1], down, mixed_out, from_far, shards.at[step(x, 1), high])
     crossed("o", wo)
 
-    def leaving(k):
-        lines = pl.ds(pl.multiple_of(k * 512, 512), 512)
-        return pltpu.make_async_copy(out_ref.at[:, lines], out_hbm.at[:, lines], local_sem.at[k])
-
     def contribute(at, begin, end):
-        @pl.loop(0, 4)
+        @pl.loop(0, 2)
         def _(k):
-            lines = pl.ds(pl.multiple_of(k * 512, 512), 512)
-            total = dot_nt(wo[k, :, :, at].reshape(512, -1), shards[at])
+            lines = pl.ds(pl.multiple_of(k * 1024, 1024), 1024)
+            total = dot_nt(wo[pl.ds(2 * k, 2), :, :, at].reshape(1024, -1), shards[at])
             if not begin:
                 total = total + summed[lines, :]
             if end:
                 out_ref[:, lines] = total.T.astype(out_ref.dtype)
-                leaving(k).start()
             else:
                 summed[lines, :] = total
 
@@ -796,10 +790,6 @@
     contribute(step(x, 2), False, True)
 
     wire.drain()
-
-    @pl.loop(0, 4)
-    def _(k):
-        leaving(k).wait()
 
 
 FLAGS = 57
@@ -830,9 +820,9 @@
     bf16, f32 = jnp.bfloat16, jnp.float32
     return pl.pallas_call(
         functools.partial(mixer_kernel, math.log(4 * rows * lax.axis_size(SP))),
-        out_shape=jax.ShapeDtypeStruct((rows, width), OUT_TYPE),
+        out_shape=pltpu.VMEM((rows, width), OUT_TYPE),
         in_specs=[anywhere] * 15,
-        out_specs=pl.BlockSpec(memory_space=pltpu.HBM),
+        out_specs=pl.BlockSpec(memory_space=pltpu.VMEM),
         scratch_shapes=[
             pltpu.VMEM((1, width), f32),
             pltpu.VMEM(w_step_forward.shape[::-1], bf16),
@@ -846,7 +836,6 @@
             pltpu.VMEM((16, 128), f32),
             pltpu.VMEM((rows, 128), f32),
             pltpu.VMEM((blocks, 8, 128), f32),
-            pltpu.VMEM((rows, width), OUT_TYPE),
             pltpu.VMEM((4, rows, width), bf16),
             pltpu.VMEM((2 * HALO, width), bf16),
             pltpu.VMEM((4 * rows + 2 * HALO, width), bf16),

time: 87.1 us -> 84.5 us (0.970)
  local copies, waits for them, and re-layouts: 2.3 us -> 0.97 us
  Pallas kernels: 84.6 us -> 83.4 us
    unnamed x1, local copies, waits for them, and re-layouts: 2.3 us -> 0.97 us
    pallas_call x1, Pallas kernels: 84.6 us -> 83.4 us  [mix(): pl.pallas_call(functools.partial(mixer_kernel, math.log(4 * rows * lax.ax...]
where the time goes in v6:
time: 84.5 us; the launch traced here: 84.3 us
  Pallas kernels  83.4 us (99%)
  local copies, waits for them, and re-layouts  0.97 us (1%)
    pallas_call x1, Pallas kernels, mix(): pl.pallas_call(functools.partial(mixer_kernel, math.log(4 * rows * lax.ax...  83.4 us

profile of v6, /device:TPU:1, one launch (start us, length us, event | category | flops | bytes accessed | tf_op | source)
XLA Modules:
  0.0 84.3 jit_solution(6349292448699323883)
XLA Ops:
  0.0 83.4 %mixer.1 = bf16[256,2048]{1,0:T(8,128)(2,1)S(1)} custom-call(bf16[256,2048]{1,0:T(8,128)(2,1)} %tokens_hbm.1, bf16[64,512]{1,0:T(8,128)(2,1)} %value_hbm.1, bf16[64,256]{1,0:T(8,128)(2,1)} %state_in_hbm.1, bf16[64,256]{1,0:T(8,128)(2,1)} %state_out_hbm.1, bf16[64,512]{1,0:T(8,128)(2,1)} %gate_hbm.1, bf16[64,512]{1,0:T(8,128)(2,1)} %bitcast.5, ...), custom_call_target="tpu_custom_call" | custom-call | tf_op jit(solution)/shard_map/mixer/pallas_call | solution.py:821
  83.4 1.0 %copy.17 = bf16[256,2048]{1,0:T(8,128)(2,1)} copy(bf16[256,2048]{1,0:T(8,128)(2,1)S(1)} %mixer.1) | data formatting | bytes 2097152

commit v7 on v6

--- a/solution.py
+++ b/solution.py
@@ -16,7 +16,7 @@
 SP_TP = ("z", "y", "c", "x")
 EPSILON = 1e-06
 MESH = pl.DeviceIdType.MESH
-VALUE, INWARD, OUTWARD, STEPS = range(4)
+VALUE, INWARD, OUTWARD, STEPS, VALUE_FIRST, VALUE_SECOND = range(6)
 HALO = 16
 
 
@@ -383,6 +383,10 @@
                 columns = pl.ds(pl.multiple_of(k * 256, 256), 256)
                 put(product(wv, columns), columns)
 
+        for name, start in ((VALUE_FIRST, 0), (VALUE_SECOND, half // 2)):
+            if name in parts:
+                columns = slice(start, start + half // 2)
+                put(product(wv, columns), columns)
         if INWARD in parts:
             put(product(ws, slice(0, lead)), slice(half, half + lead))
         if OUTWARD in parts:
@@ -522,8 +526,11 @@
             )
             target[rows_of(k), start : start + 128] = silu(total).astype(jnp.bfloat16)
 
-    def prepare(first_block):
-        some = [lax.rem(first_block + n, blocks) for n in range(4)]
+    def four(first_block):
+        return [lax.rem(first_block + n, blocks) for n in range(4)]
+
+    def prepare_steps(first_block):
+        some = four(first_block)
         both = 2 * heads
         forward_row = lax.rem(iota((4 * both, BLOCK), 0), both) < heads
         size = jax.nn.softplus(
@@ -545,7 +552,6 @@
             size * jnp.exp(jnp.where(forward_row, whole - through, until)),
             jnp.broadcast_to(jnp.exp(whole), (4 * both, BLOCK)),
         )
-        turned = []
         for n, k in enumerate(some):
             own_rows = slice(n * both, (n + 1) * both)
             rowwise[k, 0:both, :] = lines[own_rows]
@@ -559,9 +565,13 @@
             ).T
             column[rows_of(k), :] = block
             fades[k] = block[0:8]
-            turned.append(block.astype(jnp.bfloat16))
-        turned = jnp.concatenate(turned, axis=0)
-        for g in range(groups):
+
+    def prepare_states(first_block, chosen):
+        some = four(first_block)
+        turned = jnp.concatenate(
+            [column[rows_of(k), :].astype(jnp.bfloat16) for k in some], axis=0
+        )
+        for g in chosen:
             across_in = [
                 inward[rows_of(k), g * STATE : (g + 1) * STATE].astype(jnp.float32).T.astype(
                     jnp.bfloat16
@@ -587,17 +597,20 @@
     def _(k):
         filtered(lax.rem(away + 3 + k, blocks), 0, wide)
 
-    prepare(away + 3)
+    prepare_steps(away + 3)
+    prepare_states(away + 3, range(groups))
 
     wire.landed(tokens.at[0, pl.ds(0, rows - 2 * HALO)], far_rest)
     normalize(tokens.at[step(x, 2)], rows, 3 * rows)
-    project((3,), (VALUE, INWARD, STEPS))
+    project((3,), (STEPS, INWARD, VALUE_FIRST))
 
     @pl.loop(0, 4)
     def _(k):
-        filtered(lax.rem(away + 7 + k, blocks), 0, half + lead)
-
-    prepare(away + 7)
+        filtered(lax.rem(away + 7 + k, blocks), 0, half // 2)
+        filtered(lax.rem(away + 7 + k, blocks), half, half + lead)
+
+    prepare_steps(away + 7)
+    prepare_states(away + 7, (0,))
 
     over = dot(
         jnp.concatenate([fades[k, 0:1, :] for k in range(blocks)], axis=0),
@@ -607,38 +620,73 @@
     for k in range(blocks):
         decays[k] = jnp.broadcast_to(over[k : k + 1], (8, wide))
 
-    @pl.loop(0, wide // 128)
-    def _(j):
-        lanes = pl.ds(pl.multiple_of(j * 128, 128), 128)
-        backward = j >= half // 128
-        total = jnp.zeros((STATE, 128), jnp.float32)
-        decay = jnp.ones((1, 128), jnp.float32)
-        for k in range(blocks):
-            at = jnp.where(backward, blocks - 1 - k, k)
-            part = decays[at, 0:1, lanes]
-            total = total * part + states[at, :, lanes]
-            decay = decay * part
-        upper = decay.astype(jnp.bfloat16).astype(jnp.float32)
-        centre = (decay - upper).astype(jnp.bfloat16).astype(jnp.float32)
-        rest = decay - upper - centre
-        place_row = iota((16, 128), 0)
-        tail = jnp.where(place_row == 0, upper, jnp.where(place_row == 1, centre, rest))
-        for q in range(4):
-            totals[4 * j + q, 0:32, :] = total[32 * q : 32 * q + 32].astype(jnp.bfloat16)
-            totals[4 * j + q, 32:48, :] = tail.astype(jnp.bfloat16)
-
-    state_flags = [wire.flag() for _ in range(4)]
-    wire.sent.append((totals.at[pl.ds(0, 31)], state_flags[0]))
-    wire.sent.append((onward.at[pl.ds(0, 31)], state_flags[2]))
-
-    def disperse(box, inbox, send, recv):
-        @pl.loop(0, 31)
-        def _(k):
-            to = lax.rem(me + lax.rem(k + 15, 31) + 1, 32)
-            wire.go(box.at[to], stretch(to), send, recv, inbox.at[me])
-
-    disperse(totals, arrived, *state_flags[:2])
-
+    tiles = span // 128
+    ways = half // 128
+
+    def tile_of(g, n):
+        return n // tiles * ways + g * tiles + lax.rem(n, tiles)
+
+    def total_up(g):
+        @pl.loop(0, 2 * tiles)
+        def _(n):
+            j = tile_of(g, n)
+            lanes = pl.ds(pl.multiple_of(j * 128, 128), 128)
+            backward = n >= tiles
+            total = jnp.zeros((STATE, 128), jnp.float32)
+            decay = jnp.ones((1, 128), jnp.float32)
+            for k in range(blocks):
+                at = jnp.where(backward, blocks - 1 - k, k)
+                part = decays[at, 0:1, lanes]
+                total = total * part + states[at, :, lanes]
+                decay = decay * part
+            upper = decay.astype(jnp.bfloat16).astype(jnp.float32)
+            centre = (decay - upper).astype(jnp.bfloat16).astype(jnp.float32)
+            rest = decay - upper - centre
+            place_row = iota((16, 128), 0)
+            tail = jnp.where(place_row == 0, upper, jnp.where(place_row == 1, centre, rest))
+            for q in range(4):
+                totals[4 * j + q, 0:32, :] = total[32 * q : 32 * q + 32].astype(jnp.bfloat16)
+                totals[4 * j + q, 32:48, :] = tail.astype(jnp.bfloat16)
+
+    totals_out = [wire.flag() for _ in range(groups)]
+    totals_in, onward_out = wire.flag(), wire.flag()
+    onward_in = [wire.flag() for _ in range(groups)]
+    wire.sent.append((onward.at[pl.ds(0, 31)], onward_out))
+    mine = lax.rem(me // (4 * tiles), groups)
+    share = 32 // groups
+
+    def each_of(g, act):
+        @pl.when(mine == g)
+        def _():
+            act(share - 1)
+
+        @pl.when(mine != g)
+        def _():
+            act(share)
+
+    def disperse_totals(g):
+        @pl.loop(0, 2 * tiles)
+        def _(n):
+            for q in range(4):
+                to = 4 * tile_of(g, n) + q
+
+                @pl.when(to != me)
+                def _():
+                    wire.go(
+                        totals.at[to], stretch(to), totals_out[g], totals_in, arrived.at[me]
+                    )
+
+    total_up(0)
+    disperse_totals(0)
+    project((3,), (VALUE_SECOND,))
+
+    @pl.loop(0, 4)
+    def _(k):
+        filtered(lax.rem(away + 7 + k, blocks), half // 2, half)
+
+    prepare_states(away + 7, (1,))
+    total_up(1)
+    disperse_totals(1)
     arrived[me] = totals[me]
 
     g_second.finish()
@@ -687,7 +735,7 @@
     def _(k):
         within(k)
 
-    wire.landed(arrived.at[pl.ds(0, 31)], state_flags[1])
+    wire.landed(arrived.at[pl.ds(0, 31)], totals_in)
 
     flip = me >= 16
 
@@ -700,7 +748,15 @@
 
     lax.fori_loop(0, 32, hop, jnp.zeros((32, 128), jnp.float32))
 
-    disperse(onward, incoming, *state_flags[2:])
+    for g in range(groups):
+
+        @pl.when(mine == g)
+        def _():
+            @pl.loop(0, 31)
+            def _(k):
+                to = lax.rem(me + lax.rem(k + 15, 31) + 1, 32)
+                wire.go(onward.at[to], stretch(to), onward_out, onward_in[g], incoming.at[me])
+
 
     incoming[me] = onward[me]
 
@@ -712,61 +768,88 @@
     def _(k):
         within(k)
 
-    wire.landed(incoming.at[pl.ds(0, 31)], state_flags[3])
-
-    @pl.loop(0, wide // 128)
-    def _(j):
-        lanes = pl.ds(pl.multiple_of(j * 128, 128), 128)
-        backward = j >= half // 128
-        state = jnp.concatenate([incoming[4 * j + q] for q in range(4)], axis=0).astype(jnp.float32)
-        for k in range(blocks):
-            at = jnp.where(backward, blocks - 1 - k, k)
-            before[at, :, lanes] = state.astype(jnp.bfloat16)
-            state = state * decays[at, 0:1, lanes] + states[at, :, lanes]
-
     spread_read = spread(1).astype(jnp.bfloat16)
 
-    def finish(k):
-        scale = dot(column[rows_of(k), :].astype(jnp.bfloat16), spread_read)
-        for g in range(groups):
-            lanes = slice(g * span, (g + 1) * span)
-            read = outward[rows_of(k), g * STATE : (g + 1) * STATE]
-            total = inner[rows_of(k), lanes]
-            for way in range(2):
-                placed = slice(way * half + g * span, way * half + (g + 1) * span)
-                total = total + dot(read, before[k, :, placed]) * scale[:, placed]
-            gated = total * gates[rows_of(k), lanes].astype(jnp.float32)
-            level = lax.rsqrt(jnp.mean(gated * gated, axis=-1, keepdims=True) + EPSILON)
-            mixed[rows_of(k), lanes] = (gated * level * gain_ref[:, lanes]).astype(jnp.bfloat16)
-
-    def finish_shard(shard):
+    def carry(g):
+        each_of(g, lambda n: wire.landed(incoming.at[pl.ds(0, n)], onward_in[g]))
+
+        @pl.loop(0, 2 * tiles)
+        def _(n):
+            j = tile_of(g, n)
+            lanes = pl.ds(pl.multiple_of(j * 128, 128), 128)
+            backward = n >= tiles
+            state = jnp.concatenate([incoming[4 * j + q] for q in range(4)], axis=0).astype(
+                jnp.float32
+            )
+            for k in range(blocks):
+                at = jnp.where(backward, blocks - 1 - k, k)
+                before[at, :, lanes] = state.astype(jnp.bfloat16)
+                state = state * decays[at, 0:1, lanes] + states[at, :, lanes]
+
+    def finish(k, g):
+        lanes = slice(g * span, (g + 1) * span)
+        read = outward[rows_of(k), g * STATE : (g + 1) * STATE]
+        scale = column[rows_of(k), :].astype(jnp.bfloat16)
+        total = inner[rows_of(k), lanes]
+        for way in range(2):
+            placed = slice(way * half + g * span, way * half + (g + 1) * span)
+            total = total + dot(read, before[k, :, placed]) * dot(scale, spread_read[:, placed])
+        gated = total * gates[rows_of(k), lanes].astype(jnp.float32)
+        level = lax.rsqrt(jnp.mean(gated * gated, axis=-1, keepdims=True) + EPSILON)
+        mixed[rows_of(k), lanes] = (gated * level * gain_ref[:, lanes]).astype(jnp.bfloat16)
+
+    def finish_shard(shard, g):
         @pl.loop(0, 2)
         def _(b):
-            finish(2 * shard + b)
-
-    def part(shard, some):
+            finish(2 * shard + b, g)
+
+    def lanes_of(g):
+        return pl.ds(g * span, span)
+
+    def part(shard, some, g):
         start, size = some
-        return mixed.at[pl.ds(pl.multiple_of(shard * rows + start, middle), size)]
-
-    mixed_out, relayed, from_below, from_above, from_far = [wire.flag() for _ in range(5)]
+        return mixed.at[
+            pl.ds(pl.multiple_of(shard * rows + start, middle), size), lanes_of(g)
+        ]
+
+    mixed_out, from_below, from_above, from_far = [wire.flag() for _ in range(4)]
+    relayed = [wire.flag() for _ in range(groups)]
     wire.sent.append((shards, mixed_out))
-    finish(2 * step(x, 2))
-    wire.go(part(step(x, 2), (0, middle)), up, mixed_out, relayed, relay.at[0])
-    finish(2 * step(x, 2) + 1)
-    wire.go(part(step(x, 2), (middle, middle)), down, mixed_out, relayed, relay.at[1])
-    finish_shard(step(x, 1))
-    wire.go(part(step(x, 1), (0, rows)), up, mixed_out, from_below, shards.at[x])
-    finish_shard(step(x, 3))
-    wire.go(part(step(x, 3), (0, rows)), down, mixed_out, from_above, shards.at[x])
-    lo_second.finish()
-    across("o", wo, "z", 2, (0, 2))
-    hi_second.finish()
-    across("o", wo, "y", 2, (2, 2))
-    finish_shard(x)
+
+    def hand_on(g):
+        wire.landed(relay.at[:, :, lanes_of(g)], relayed[g])
+        for half_at, to, target in (
+            (0, up, shards.at[step(x, 3), low, lanes_of(g)]),
+            (1, down, shards.at[step(x, 1), high, lanes_of(g)]),
+        ):
+            wire.go(relay.at[half_at, :, lanes_of(g)], to, mixed_out, from_far, target)
+
+    for g in range(groups):
+        carry(g)
+        for half_at, to in ((0, up), (1, down)):
+            finish(2 * step(x, 2) + half_at, g)
+            wire.go(
+                part(step(x, 2), (half_at * middle, middle), g),
+                to,
+                mixed_out,
+                relayed[g],
+                relay.at[half_at, :, lanes_of(g)],
+            )
+        for by, to, flag in ((1, up, from_below), (3, down, from_above)):
+            finish_shard(step(x, by), g)
+            wire.go(
+                part(step(x, by), (0, rows), g), to, mixed_out, flag, shards.at[x, :, lanes_of(g)]
+            )
+        if g == 0:
+            lo_second.finish()
+            across("o", wo, "z", 2, (0, 2))
+            hi_second.finish()
+            across("o", wo, "y", 2, (2, 2))
+        finish_shard(x, g)
+        if g:
+            hand_on(g - 1)
     shards[x] = mixed[pl.ds(pl.multiple_of(x * rows, rows), rows), :]
-    wire.landed(relay, relayed)
-    wire.go(relay.at[0], up, mixed_out, from_far, shards.at[step(x, 3), low])
-    wire.go(relay.at[1], down, mixed_out, from_far, shards.at[step(x, 1), high])
+    hand_on(groups - 1)
     crossed("o", wo)
 
     def contribute(at, begin, end):
@@ -790,9 +873,11 @@
     contribute(step(x, 2), False, True)
 
     wire.drain()
-
-
-FLAGS = 57
+    for g in range(groups):
+        each_of(g, lambda n: wire.span(totals.at[pl.ds(0, n)], totals_out[g]).wait_send())
+
+
+FLAGS = 60
 
 
 def mix(

time: 84.5 us -> 83.5 us (0.988)
  Pallas kernels: 83.4 us -> 82.4 us
    pallas_call x1, Pallas kernels: 83.4 us -> 82.4 us  [mix(): pl.pallas_call(functools.partial(mixer_kernel, math.log(4 * rows * lax.ax...]
where the time goes in v7:
time: 83.5 us; the launch traced here: 83.3 us
  Pallas kernels  82.4 us (99%)
  local copies, waits for them, and re-layouts  0.97 us (1%)
    pallas_call x1, Pallas kernels, mix(): pl.pallas_call(functools.partial(mixer_kernel, math.log(4 * rows * lax.ax...  82.4 us

profile of v7, /device:TPU:1, one launch (start us, length us, event | category | flops | bytes accessed | tf_op | source)
XLA Modules:
  0.0 83.3 jit_solution(14660364006239623080)
XLA Ops:
  0.0 82.4 %mixer.1 = bf16[256,2048]{1,0:T(8,128)(2,1)S(1)} custom-call(bf16[256,2048]{1,0:T(8,128)(2,1)} %tokens_hbm.1, bf16[64,512]{1,0:T(8,128)(2,1)} %value_hbm.1, bf16[64,256]{1,0:T(8,128)(2,1)} %state_in_hbm.1, bf16[64,256]{1,0:T(8,128)(2,1)} %state_out_hbm.1, bf16[64,512]{1,0:T(8,128)(2,1)} %gate_hbm.1, bf16[64,512]{1,0:T(8,128)(2,1)} %bitcast.5, ...), custom_call_target="tpu_custom_call" | custom-call | tf_op jit(solution)/shard_map/mixer/pallas_call | solution.py:906
  82.4 1.0 %copy.17 = bf16[256,2048]{1,0:T(8,128)(2,1)} copy(bf16[256,2048]{1,0:T(8,128)(2,1)S(1)} %mixer.1) | data formatting | bytes 2097152

commit v8 on v7

--- a/solution.py
+++ b/solution.py
@@ -595,10 +595,10 @@
 
     @pl.loop(0, 4)
     def _(k):
-        filtered(lax.rem(away + 3 + k, blocks), 0, wide)
+        filtered(lax.rem(away + 3 + k, blocks), 0, half + lead)
 
     prepare_steps(away + 3)
-    prepare_states(away + 3, range(groups))
+    prepare_states(away + 3, (0,))
 
     wire.landed(tokens.at[0, pl.ds(0, rows - 2 * HALO)], far_rest)
     normalize(tokens.at[step(x, 2)], rows, 3 * rows)
@@ -610,8 +610,6 @@
         filtered(lax.rem(away + 7 + k, blocks), half, half + lead)
 
     prepare_steps(away + 7)
-    prepare_states(away + 7, (0,))
-
     over = dot(
         jnp.concatenate([fades[k, 0:1, :] for k in range(blocks)], axis=0),
         spread(3),
@@ -619,6 +617,7 @@
     )
     for k in range(blocks):
         decays[k] = jnp.broadcast_to(over[k : k + 1], (8, wide))
+    prepare_states(away + 7, (0,))
 
     tiles = span // 128
     ways = half // 128
@@ -684,13 +683,12 @@
     def _(k):
         filtered(lax.rem(away + 7 + k, blocks), half // 2, half)
 
+    prepare_states(away + 3, (1,))
     prepare_states(away + 7, (1,))
     total_up(1)
     disperse_totals(1)
     arrived[me] = totals[me]
 
-    g_second.finish()
-    across("g", wg, "y", 2)
 
     def within(k):
         for g in range(groups):
@@ -718,17 +716,11 @@
                 jnp.concatenate(weights, axis=1), jnp.concatenate(content, axis=0)
             )
 
-    lo_second.forward()
-    hi_second.forward()
-    for by in (3, 1):
-        across("o", wo, "z", by, (0, 2))
-        across("o", wo, "y", by, (2, 2))
-
     project((3,), (OUTWARD,))
 
-    @pl.loop(0, 4)
+    @pl.loop(0, blocks)
     def _(k):
-        filtered(lax.rem(away + 7 + k, blocks), half + lead, wide)
+        filtered(k, half + lead, wide)
 
 
     @pl.loop(0, blocks // 2)
@@ -760,13 +752,22 @@
 
     incoming[me] = onward[me]
 
+    g_second.finish()
+    across("g", wg, "y", 2)
+
+    @pl.loop(blocks // 2, blocks)
+    def _(k):
+        within(k)
+
+    lo_second.forward()
+    hi_second.forward()
+    for by in (3, 1):
+        across("o", wo, "z", by, (0, 2))
+        across("o", wo, "y", by, (2, 2))
+
     crossed("g", wg)
     project_gate((0, 1, 2))
     project_gate((3,))
-
-    @pl.loop(blocks // 2, blocks)
-    def _(k):
-        within(k)
 
     spread_read = spread(1).astype(jnp.bfloat16)
 
@@ -840,18 +841,14 @@
             wire.go(
                 part(step(x, by), (0, rows), g), to, mixed_out, flag, shards.at[x, :, lanes_of(g)]
             )
-        if g == 0:
-            lo_second.finish()
-            across("o", wo, "z", 2, (0, 2))
-            hi_second.finish()
-            across("o", wo, "y", 2, (2, 2))
         finish_shard(x, g)
         if g:
             hand_on(g - 1)
+    lo_second.finish()
+    across("o", wo, "z", 2, (0, 2))
+    hi_second.finish()
+    across("o", wo, "y", 2, (2, 2))
     shards[x] = mixed[pl.ds(pl.multiple_of(x * rows, rows), rows), :]
-    hand_on(groups - 1)
-    crossed("o", wo)
-
     def contribute(at, begin, end):
         @pl.loop(0, 2)
         def _(k):
@@ -864,7 +861,10 @@
             else:
                 summed[lines, :] = total
 
+    hand_on(groups - 1)
+    crossed("o", wo)
     contribute(x, True, False)
+
     wire.landed(shards.at[0], from_below)
     contribute(step(x, 3), False, False)
     wire.landed(shards.at[0], from_above)

time: 83.5 us -> 81.4 us (0.975)
  Pallas kernels: 82.4 us -> 80.3 us
    pallas_call x1, Pallas kernels: 82.4 us -> 80.3 us  [mix(): pl.pallas_call(functools.partial(mixer_kernel, math.log(4 * rows * lax.ax...]
where the time goes in v8:
time: 81.4 us; the launch traced here: 81.3 us
  Pallas kernels  80.3 us (99%)
  local copies, waits for them, and re-layouts  0.97 us (1%)
    pallas_call x1, Pallas kernels, mix(): pl.pallas_call(functools.partial(mixer_kernel, math.log(4 * rows * lax.ax...  80.3 us

profile of v8, /device:TPU:1, one launch (start us, length us, event | category | flops | bytes accessed | tf_op | source)
XLA Modules:
  0.0 81.3 jit_solution(13536717311946347400)
XLA Ops:
  0.0 80.3 %mixer.1 = bf16[256,2048]{1,0:T(8,128)(2,1)S(1)} custom-call(bf16[256,2048]{1,0:T(8,128)(2,1)} %tokens_hbm.1, bf16[64,512]{1,0:T(8,128)(2,1)} %value_hbm.1, bf16[64,256]{1,0:T(8,128)(2,1)} %state_in_hbm.1, bf16[64,256]{1,0:T(8,128)(2,1)} %state_out_hbm.1, bf16[64,512]{1,0:T(8,128)(2,1)} %gate_hbm.1, bf16[64,512]{1,0:T(8,128)(2,1)} %bitcast.5, ...), custom_call_target="tpu_custom_call" | custom-call | tf_op jit(solution)/shard_map/mixer/pallas_call | solution.py:906
  80.3 1.0 %copy.17 = bf16[256,2048]{1,0:T(8,128)(2,1)} copy(bf16[256,2048]{1,0:T(8,128)(2,1)S(1)} %mixer.1) | data formatting | bytes 2097152
